TPU v7x, 32 devices: a whole 2x2x4 slice. The times are simulated.
32 devices in a mesh: sp: 8 (over z, y), tp: 4 (over x, core).
Axes of the slice: x: 2, y: 2, z: 4, core: 2. Of those that a mesh axis runs over, the one named last changes fastest.
Arguments:
- queries: bfloat16 [4096, 512], P('sp', 'tp'), may hold values from -6 to 6
- key_matrix: bfloat16 [4096, 512], P('sp', 'tp'), may hold values from -6 to 6
- value_matrix: bfloat16 [4096, 1024], P('sp', 'tp'), may hold values from -6 to 6
- channel_decay_input: bfloat16 [4096, 512], P('sp', 'tp')
- head_decay_offset: float32 [4096, 8], P('sp', 'tp'), may hold values from -1 to 0
- output_gate_input: bfloat16 [4096, 1024], P('sp', 'tp'), may hold values from -6 to 6
- head_norm_gain: float32 [128], replicated, may hold values from 0.1 to 1.9
- residual: bfloat16 [4096, 2048], P(('sp', 'tp')), may hold values from -6 to 6
- mixer_output_weight: bfloat16 [1024, 2048], replicated, may hold values from -0.1875 to 0.1875
- expert_norm_gain: float32 [2048], replicated, may hold values from 0.1 to 1.9
- routes: int32 [4096, 4], P(('sp', 'tp')), may hold values from 0 to 63, all different within a row; in each aligned block of 128 rows (0 to 127, 128 to 255, ...) at most 16 rows name the same one
- chosen_router_scores: float32 [4096, 4], P(('sp', 'tp')), may hold values from 0.1 to 1
- routed_gate_weight: bfloat16 [64, 2048, 512], P(('sp', 'tp')), may hold values from -0.125 to 0.125
- routed_up_weight: bfloat16 [64, 2048, 512], P(('sp', 'tp')), may hold values from -0.125 to 0.125
- routed_down_weight: bfloat16 [64, 512, 2048], P(('sp', 'tp')), may hold values from -0.25 to 0.25
- common_gate_weight: bfloat16 [2048, 512], replicated, may hold values from -0.125 to 0.125
- common_up_weight: bfloat16 [2048, 512], replicated, may hold values from -0.125 to 0.125
- common_down_weight: bfloat16 [512, 2048], replicated, may hold values from -0.25 to 0.25
Outputs:
- layer_out: bfloat16 [4096, 2048], P(('sp', 'tp'))
Inputs may be any that keep to these rules, and one draw needn't show every extreme that they name: `routes`: each row names 4 different experts. In each aligned block of 128 rows (the rows of one device) no expert is named by more than 16 rows, a bound that some block reaches.
All inputs are finite; a program needn't handle non-finite values.
Results may differ from a plain program's by a relative error of at most 0.017.
Values may be sent and summed in bfloat16 or wider, within the bound.
No kernel may reach another device: no remote copies, remote signals or barrier semaphores. Data moves between devices by JAX's collectives and lax.ppermute only.
A program may use at most 128 MiB of HBM per device.

v0:
```python
import jax
import jax.numpy as jnp
from jax import lax
from jax.sharding import PartitionSpec as P

D = 2048
KEY_CHANNELS = 64
VDIM = 128
BLOCK = 64
TOP_K = 4


eps_norm = 1e-06
decay_running = 16.0
routed_scale = 2.5


def carried_in(part, axis, combine, identity):
    place = lax.axis_index(axis)
    gathered = jax.tree.map(lambda a: lax.all_gather(a, axis), part)
    state = jax.tree.map(lambda a, e: jnp.zeros_like(a) + jnp.asarray(e, a.dtype), part, identity)

    def one(hop, state):
        return combine(
            state, jax.tree.map(lambda a: lax.dynamic_index_in_dim(a, hop, 0, False), gathered)
        )

    return lax.fori_loop(0, place, one, state)


def expert_block(picked_rows, gate_weight, up_weight, down_weight):
    gate_pre = jnp.dot(picked_rows, gate_weight, preferred_element_type=jnp.float32)
    up_pre = jnp.dot(picked_rows, up_weight, preferred_element_type=jnp.float32)
    hidden = (jax.nn.silu(gate_pre) * up_pre).astype(jnp.bfloat16)
    return jnp.dot(hidden, down_weight, preferred_element_type=jnp.float32)


def apply_experts(arrived, routed_gate_weight, routed_up_weight, routed_down_weight):
    gate_pre = jnp.einsum(
        "sech,ehf->secf", arrived, routed_gate_weight, preferred_element_type=jnp.float32
    )
    up_pre = jnp.einsum(
        "sech,ehf->secf", arrived, routed_up_weight, preferred_element_type=jnp.float32
    )
    hidden = (jax.nn.silu(gate_pre) * up_pre).astype(jnp.bfloat16)
    return jnp.einsum(
        "secf,efh->sech", hidden, routed_down_weight, preferred_element_type=jnp.float32
    ).astype(jnp.bfloat16)


def chain_join(earlier, latter):
    return (earlier[0] * latter[0], latter[0][..., None] * earlier[1] + latter[1])


def on_device(
    queries,
    key_matrix,
    value_matrix,
    channel_decay_input,
    head_decay_offset,
    output_gate_input,
    head_norm_gain,
    residual,
    mixer_output_weight,
    expert_norm_gain,
    routes,
    chosen_router_scores,
    routed_gate_weight,
    routed_up_weight,
    routed_down_weight,
    common_gate_weight,
    common_up_weight,
    common_down_weight,
):
    device_heads = head_decay_offset.shape[1]
    seq_rows = queries.shape[0]
    blocks = seq_rows // BLOCK

    def split_local(values, columns):
        return (
            values.astype(jnp.float32)
            .reshape(blocks, BLOCK, device_heads, columns)
            .transpose(2, 0, 1, 3)
        )

    decay_spike_columns = jnp.repeat(head_decay_offset, KEY_CHANNELS, axis=1)
    decay_logarithm = (
        jax.nn.log_sigmoid(channel_decay_input.astype(jnp.float32)) / decay_running
        + decay_spike_columns
    )
    within = jnp.cumsum(split_local(decay_logarithm, KEY_CHANNELS), axis=2)
    block_end = within[:, :, -1, :]
    q_heads = split_local(queries, KEY_CHANNELS) * KEY_CHANNELS ** (-0.5)
    k_heads = split_local(key_matrix, KEY_CHANNELS)
    v_heads = split_local(value_matrix, VDIM)
    q_decay = q_heads * jnp.exp(within)
    k_grow = k_heads * jnp.exp(-within)
    k_tail = k_heads * jnp.exp(block_end[:, :, None, :] - within)
    causal = jnp.tril(jnp.ones((BLOCK, BLOCK), dtype=bool))
    scores = jnp.where(causal, jnp.einsum("hnid,hnjd->hnij", q_decay, k_grow), 0.0)
    inside = jnp.einsum("hnij,hnje->hnie", scores, v_heads)
    block_state = jnp.einsum("hncd,hnce->hnde", k_tail, v_heads)
    inclusive = jnp.cumsum(block_end, axis=1)
    exclusive = inclusive - block_end
    before = jnp.arange(blocks)[:, None] > jnp.arange(blocks)[None, :]
    spread = jnp.exp(
        jnp.where(
            before[None, :, :, None], exclusive[:, :, None, :] - inclusive[:, None, :, :], -jnp.inf
        )
    )
    local_start = jnp.einsum("hnmd,hmde->hnde", spread, block_state)
    total_log = inclusive[:, -1, :]
    tail_weight = jnp.exp(total_log[:, None, :] - inclusive)
    device_state = jnp.einsum("hnd,hnde->hde", tail_weight, block_state)
    device_decay = jnp.exp(total_log)
    identity = (jnp.ones_like(device_decay), jnp.zeros_like(device_state))
    _, carried = carried_in((device_decay, device_state), "sp", chain_join, identity)
    entering = local_start + jnp.exp(exclusive)[..., None] * carried[:, None, :, :]
    output = inside + jnp.einsum("hncd,hnde->hnce", q_decay, entering)
    output = output.transpose(1, 2, 0, 3).reshape(seq_rows, device_heads, VDIM)
    inv_rms = lax.rsqrt(jnp.mean(output * output, axis=-1, keepdims=True) + eps_norm)
    normed_heads = (output * inv_rms * head_norm_gain).reshape(seq_rows, device_heads * VDIM)
    gated_output = (normed_heads * jax.nn.silu(output_gate_input.astype(jnp.float32))).astype(
        jnp.bfloat16
    )
    tok_count = residual.shape[0]
    stacked = gated_output.reshape(lax.axis_size("tp"), tok_count, gated_output.shape[1])
    projected = jnp.dot(
        lax.all_to_all(stacked, "tp", split_axis=0, concat_axis=2, tiled=True)[0],
        mixer_output_weight,
        preferred_element_type=jnp.float32,
    )[None][0]
    middle = (residual.astype(jnp.float32) + projected).astype(jnp.bfloat16)
    middle_wide = middle.astype(jnp.float32)
    norm_scale = lax.rsqrt(jnp.mean(middle_wide * middle_wide, axis=-1, keepdims=True) + eps_norm)
    normed = (middle_wide * norm_scale * expert_norm_gain).astype(jnp.bfloat16)
    weights = (
        routed_scale * chosen_router_scores / jnp.sum(chosen_router_scores, axis=-1, keepdims=True)
    )
    devices = lax.axis_size("sp") * lax.axis_size("tp")
    exp_dev = routed_gate_weight.shape[0]
    experts_all = exp_dev * devices
    cap_slots = 2 * TOP_K * tok_count // experts_all
    flat_expert = routes.reshape(-1)
    one_hot = (flat_expert[:, None] == jnp.arange(experts_all, dtype=jnp.int32)[None, :]).astype(
        jnp.int32
    )
    slot_index = jnp.sum((jnp.cumsum(one_hot, axis=0) - 1) * one_hot, axis=1)
    destination = flat_expert * cap_slots + slot_index
    buffer_rows = experts_all * cap_slots
    row_owner = jnp.arange(flat_expert.shape[0], dtype=jnp.int32) // TOP_K
    source_row = jnp.full((buffer_rows,), tok_count, jnp.int32).at[destination].set(row_owner)
    normed_pad = jnp.concatenate([normed, jnp.zeros((1, D), jnp.bfloat16)], axis=0)
    outgoing = normed_pad[source_row].reshape(devices, exp_dev, cap_slots, D)
    produced = apply_experts(
        lax.all_to_all(outgoing, ("sp", "tp"), split_axis=0, concat_axis=0, tiled=True),
        routed_gate_weight,
        routed_up_weight,
        routed_down_weight,
    )
    returned = lax.all_to_all(produced, ("sp", "tp"), split_axis=0, concat_axis=0, tiled=True)
    flat_back = returned.reshape(buffer_rows, D)
    gathered = flat_back[destination].reshape(tok_count, TOP_K, D)
    routed = jnp.sum(weights[:, :, None] * gathered, axis=1)
    shared = expert_block(normed, common_gate_weight, common_up_weight, common_down_weight)
    return (middle_wide + routed + shared).astype(jnp.bfloat16)


def solution(mesh):
    placed = (
        P("sp", "tp"),
        P("sp", "tp"),
        P("sp", "tp"),
        P("sp", "tp"),
        P("sp", "tp"),
        P("sp", "tp"),
        P(),
        P(("sp", "tp"), None),
        P(),
        P(),
        P(("sp", "tp"), None),
        P(("sp", "tp"), None),
        P(("sp", "tp"), None, None),
        P(("sp", "tp"), None, None),
        P(("sp", "tp"), None, None),
        P(),
        P(),
        P(),
    )
    return jax.shard_map(
        on_device, mesh=mesh, in_specs=placed, out_specs=P(("sp", "tp"), None), check_vma=False
    )
```

profile of v0, /device:TPU:0, one launch (start us, length us, event | category | flops | bytes accessed | tf_op | source)
XLA Modules:
  0.0 336.8 jit_solution(10941217069375739230)
XLA Ops:
  0.0 1.2 copy.45
  2.2 1.0 copy.46
  3.2 1.1 fusion.35
  8.5 1.1 reshape.193
  9.7 2.0 reshape.194
  11.8 2.0 bitcast_multiply_fusion.3
  14.7 33.0 %all-gather.1 = f32[16,64,128]{2,1,0:T(8,128)S(1)} all-gather(f32[2,64,128]{2,1,0:T(8,128)S(1)} %bitcast.150), channel_id=3, replica_groups=mesh['sp'=8,'tp'=4] {'sp'}, dimensions={0}, use_global_device_ids=true | all-gather | bytes 589824 | tf_op jit(solution)/shard_map/all_gather | solution.py:20
  47.8 20.7 %all-gather = f32[16,1,64]{2,1,0:T(1,128)S(1)} all-gather(f32[2,1,64]{2,1,0:T(1,128)S(1)} %copy-done.12), channel_id=2, replica_groups=mesh['sp'=8,'tp'=4] {'sp'}, dimensions={0}, use_global_device_ids=true | all-gather | bytes 4608 | tf_op jit(solution)/shard_map/all_gather | solution.py:20
  68.5 1.4 copy.53
  69.9 1.4 copy.56
  71.7 1.5 fusion.27
  73.2 1.0 multiply_reduce_fusion.2
  74.4 1.5 copy.59
  77.5 3.4 %all-to-all-start = ((bf16[4,128,256]{1,2,0:T(8,128)(2,1)}), bf16[4,128,256]{1,2,0:T(8,128)(2,1)S(1)}, u32[]{:S(2)}, u32[]{:S(2)}) async-start(bf16[4,128,256]{1,2,0:T(8,128)(2,1)} %copy.61), calls=%async_computation | async-start | bytes 524288 | tf_op jit(solution)/shard_map/all_to_all | solution.py:129
  81.3 1.2 reduce-window.6
  83.1 2.4 scatter_custom_fusion
  85.6 1.3 all-to-all-done
  86.9 3.1 multiply_reduce_fusion.1
  90.0 1.0 copy-done.1
  91.2 6.0 %gather_fusion = bf16[1024,2048]{1,0:T(8,128)(2,1)} fusion(bf16[129,2048]{1,0:T(8,128)(2,1)S(1)} %concatenate.3, s32[1024]{0:T(1024)S(1)} %fusion.75), kind=kCustom, calls=%fused_computation | custom fusion | bytes 8392704 | tf_op jit(solution)/shard_map/gather | solution.py:154
  97.2 96.9 %all_to_all.25 = bf16[32,2,16,2048]{3,2,1,0:T(8,128)(2,1)S(1)} all-to-all(bf16[32,2,16,2048]{3,2,1,0:T(8,128)(2,1)} %bitcast.143), channel_id=1, replica_groups=mesh['sp'=8,'tp'=4] {'sp','tp'}, dimensions={0} | all-to-all | bytes 8388608 | tf_op jit(solution)/shard_map/all_to_all | solution.py:156
  194.1 2.0 copy-done.4
  196.1 3.7 %fusion.4 = f32[2,32,16,512]{3,2,1,0:T(8,128)} fusion(bf16[2,2048,512]{2,1,0:T(8,128)(2,1)S(1)} %copy-done.13, bf16[32,2,16,2048]{3,2,1,0:T(8,128)(2,1)S(1)} %all_to_all.25), kind=kOutput, calls=%fused_computation.9 | convolution fusion | flops 2147483648 | bytes 10485760 | tf_op jit(solution)/shard_map/sech,ehf->secf/dot_general | solution.py:39
  199.8 11.8 %convert_bitcast_fusion = bf16[32,2,16,2048]{3,2,0,1:T(8,128)(2,1)} fusion(bf16[2,512,2048]{2,1,0:T(8,128)(2,1)} %param.34, f32[2,32,16,512]{3,2,1,0:T(8,128)} %fusion.4, bf16[2,2048,512]{2,1,0:T(8,128)(2,1)} %param.33, bf16[32,2,16,2048]{3,2,1,0:T(8,128)(2,1)} %copy-done.4), kind=kOutput, calls=%fused_computation.12 | convolution fusion | flops 4300210176 | bytes 18874368 | tf_op jit(solution)/shard_map/secf,efh->sech/dot_general | solution.py:46
  211.6 4.7 %copy.69 = bf16[32,2,16,2048]{3,2,1,0:T(8,128)(2,1)} copy(bf16[32,2,16,2048]{3,2,0,1:T(8,128)(2,1)} %convert_bitcast_fusion) | data formatting | bytes 8388608 | tf_op jit(solution)/shard_map/convert_element_type | solution.py:48
  216.3 3.9 %all-to-all-start.2 = ((bf16[32,2,16,2048]{3,2,1,0:T(8,128)(2,1)}), bf16[32,2,16,2048]{3,2,1,0:T(8,128)(2,1)}, u32[]{:S(2)}, u32[]{:S(2)}) async-start(bf16[32,2,16,2048]{3,2,1,0:T(8,128)(2,1)} %copy.69), calls=%async_computation.2 | async-start | bytes 8388608 | tf_op jit(solution)/shard_map/all_to_all | solution.py:161
  220.5 2.0 fusion.86
  222.5 91.5 %all-to-all-done.2 = bf16[32,2,16,2048]{3,2,1,0:T(8,128)(2,1)} async-done(((bf16[32,2,16,2048]{3,2,1,0:T(8,128)(2,1)}), bf16[32,2,16,2048]{3,2,1,0:T(8,128)(2,1)}, u32[]{:S(2)}, u32[]{:S(2)}) %all-to-all-start.2) | async-done | bytes 4194336 | tf_op jit(solution)/shard_map/all_to_all | solution.py:161
  314.0 8.0 %gather_fusion.1 = bf16[512,2048]{1,0:T(8,128)(2,1)} fusion(bf16[1024,2048]{1,0:T(8,128)(2,1)} %bitcast.37, s32[1024]{0:T(1024)S(1)} %pad_clamp_fusion), kind=kCustom, calls=%fused_computation.1 | custom fusion | bytes 4196352 | tf_op jit(solution)/shard_map/gather | solution.py:163
  322.0 4.8 %reshape.159 = f32[128,4,2048]{2,1,0:T(4,128)} reshape(bf16[512,2048]{1,0:T(8,128)(2,1)} %gather_fusion.1) | data formatting | bytes 6291456 | tf_op jit(solution)/shard_map/convert_element_type | solution.py:164
  326.7 6.4 %multiply_reduce_fusion = f32[128,2048]{1,0:T(8,128)} fusion(f32[128,4,2048]{2,1,0:T(4,128)} %reshape.159, f32[128,4]{1,0:T(8,128)S(1)} %copy.62), kind=kLoop, calls=%fused_computation.11 | loop fusion | flops 1835008 | bytes 5244928 | tf_op jit(solution)/shard_map/reduce_sum | solution.py:164
  333.1 3.7 %fusion.12 = bf16[128,2048]{1,0:T(8,128)(2,1)} fusion(bf16[512,2048]{1,0:T(8,128)(2,1)S(1)} %copy-done, bf16[128,2048]{1,0:T(8,128)(2,1)} %copy-done.3, bf16[2048,512]{1,0:T(8,128)(2,1)} %param.36, f32[128,2048]{1,0:T(8,128)S(1)} %copy-done.2, f32[128,2048]{1,0:T(8,128)} %multiply_reduce_fusion, f32[128,512]{1,0:T(8,128)S(1)} %fusion.86), kind=kOutput, calls=%fused_computation.19 | convolution fusion | flops 538050560 | bytes 7602176 | tf_op jit(solution)/shard_map/dot_general | solution.py:35
  (74 shorter events, 9.8 us)
Async XLA Ops:
  0.0 333.1 %copy-start = (bf16[512,2048]{1,0:T(8,128)(2,1)S(1)}, bf16[512,2048]{1,0:T(8,128)(2,1)}, u32[]{:S(2)}) copy-start(bf16[512,2048]{1,0:T(8,128)(2,1)} %param.37) | copy-start | bytes 6291460
  0.0 11.7 %copy-start.6 = (bf16[512,256]{1,0:T(8,128)(2,1)S(1)}, bf16[512,256]{1,0:T(8,128)(2,1)}, u32[]{:S(2)}) copy-start(bf16[512,256]{1,0:T(8,128)(2,1)} %param.22) | copy-start | bytes 786436
  9.7 4.4 %copy-start.8 = (bf16[2,8,64,1]{1,3,2,0:T(2,128)(2,1)S(1)}, bf16[2,8,64,1]{1,3,2,0:T(2,128)(2,1)}, u32[]{:S(2)}) copy-start(bf16[2,8,64,1]{1,3,2,0:T(2,128)(2,1)} %copy.70) | copy-start | bytes 6148
  11.8 36.0 %copy-start.12 = (f32[2,1,64]{2,1,0:T(1,128)S(1)}, f32[2,1,64]{2,1,0:T(1,128)}, u32[]{:S(2)}) copy-start(f32[2,1,64]{2,1,0:T(1,128)} %get-tuple-element.64) | copy-start | bytes 1540
  14.0 0.7 copy-start.5
  68.5 7.4 %copy-start.14 = (f32[128]{0:T(128)S(1)}, f32[128]{0:T(128)}, u32[]{:S(2)}) copy-start(f32[128]{0:T(128)} %param.26) | copy-start | bytes 1540
  71.7 4.8 %copy-start.7 = (bf16[512,256]{1,0:T(8,128)(2,1)S(1)}, bf16[512,256]{1,0:T(8,128)(2,1)}, u32[]{:S(2)}) copy-start(bf16[512,256]{1,0:T(8,128)(2,1)} %param.25) | copy-start | bytes 786436
  71.7 9.2 %copy-start.10 = (s32[128,4]{0,1:T(4,128)S(1)}, s32[128,4]{0,1:T(4,128)}, u32[]{:S(2)}) copy-start(s32[128,4]{0,1:T(4,128)} %param.30) | copy-start | bytes 6148
  76.6 14.3 %copy-start.9 = (f32[2048]{0:T(1024)S(1)}, f32[2048]{0:T(1024)}, u32[]{:S(2)}) copy-start(f32[2048]{0:T(1024)} %param.29) | copy-start | bytes 24580
  77.5 9.4 %all-to-all-start = ((bf16[4,128,256]{1,2,0:T(8,128)(2,1)}), bf16[4,128,256]{1,2,0:T(8,128)(2,1)S(1)}, u32[]{:S(2)}, u32[]{:S(2)}) async-start(bf16[4,128,256]{1,2,0:T(8,128)(2,1)} %copy.61), calls=%async_computation | async-start | bytes 524288 | tf_op jit(solution)/shard_map/all_to_all | solution.py:129
  90.0 1.0 copy-start.1
  91.1 129.3 %copy-start.3 = (bf16[128,2048]{1,0:T(8,128)(2,1)}, bf16[128,2048]{1,0:T(8,128)(2,1)S(1)}, u32[]{:S(2)}) copy-start(bf16[128,2048]{1,0:T(8,128)(2,1)S(1)} %multiply_convert_fusion) | copy-start | bytes 1572868
  97.2 98.9 %copy-start.13 = (bf16[2,2048,512]{2,1,0:T(8,128)(2,1)S(1)}, bf16[2,2048,512]{2,1,0:T(8,128)(2,1)}, u32[]{:S(2)}) copy-start(bf16[2,2048,512]{2,1,0:T(8,128)(2,1)} %param.32) | copy-start | bytes 12582916
  194.1 2.0 copy-start.4
  216.3 4.0 %copy-start.11 = (f32[128,4]{0,1:T(4,128)S(1)}, f32[128,4]{0,1:T(4,128)}, u32[]{:S(2)}) copy-start(f32[128,4]{0,1:T(4,128)} %param.31) | copy-start | bytes 6148
  216.3 97.6 %all-to-all-start.2 = ((bf16[32,2,16,2048]{3,2,1,0:T(8,128)(2,1)}), bf16[32,2,16,2048]{3,2,1,0:T(8,128)(2,1)}, u32[]{:S(2)}, u32[]{:S(2)}) async-start(bf16[32,2,16,2048]{3,2,1,0:T(8,128)(2,1)} %copy.69), calls=%async_computation.2 | async-start | bytes 8388608 | tf_op jit(solution)/shard_map/all_to_all | solution.py:161
  326.7 6.4 %copy-start.2 = (f32[128,2048]{1,0:T(8,128)S(1)}, f32[128,2048]{1,0:T(8,128)}, u32[]{:S(2)}) copy-start(f32[128,2048]{1,0:T(8,128)} %copy-done.1) | copy-start | bytes 3145732
where the time goes:
time: 338 us; the launch traced here: 337 us
  blocking collectives  151 us (45%)
  waiting for transfers between devices  92.8 us (27%)
  local copies, waits for them, and re-layouts  43.2 us (13%)
  matrix products  27.7 us (8%)
  other arithmetic  14.9 us (4%)
  starting transfers between devices  7.35 us (2%)
    all_to_all x1, blocking collectives, on_device(): lax.all_to_all(outgoing, ('sp', 'tp'), split_axis=0, concat_axis=0, tiled...  96.9 us
    all_to_all x1, waiting for transfers between devices, on_device(): lax.all_to_all(produced, ('sp', 'tp'), split_axis=0, concat_axis=0, tiled...  91.5 us
    all_gather x2, blocking collectives, carried_in(): gathered = jax.tree.map(lambda a: lax.all_gather(a, axis), part)  53.7 us
    dot_general x1, matrix products, apply_experts(): jnp.einsum('secf,efh->sech', hidden, routed_down_weight, preferred_elemen...  11.8 us
    gather x1, local copies, waits for them, and re-layouts, on_device(): gathered = flat_back[destination].reshape(tok_count, TOP_K, D)  8 us
  transfers between devices with their start and end apart: 2, of which 2 were waited for; matrix products, arithmetic and copies ran while one was open for 2% of the time, Pallas kernels for 0%

commit v1 on v0

v1 whole, which is shorter than its diff:
```python
import jax
import jax.numpy as jnp
from jax import lax
from jax.experimental import pallas as pl
from jax.experimental.pallas import tpu as pltpu
from jax.sharding import PartitionSpec as P

KEY_CHANNELS = 64
BLOCK = 64
TOP_K = 4
MSG_PAD = 16

eps_norm = 1e-06
decay_running = 16.0
routed_scale = 2.5


def lane_head(shape):
    return lax.broadcasted_iota(jnp.int32, shape, 1) // KEY_CHANNELS


def state_kernel(k_ref, v_ref, c_ref, o_ref, within_ref, starts_ref, msg_ref):
    rows, width = k_ref.shape
    heads = o_ref.shape[1]
    vdim = v_ref.shape[1] // heads
    x = c_ref[...].astype(jnp.float32)
    decay = (jnp.minimum(x, 0.0) - jnp.log1p(jnp.exp(-jnp.abs(x)))) / decay_running
    head_of = lane_head((rows, width))
    spike = jnp.zeros((rows, width), jnp.float32)
    for h in range(heads):
        spike = jnp.where(head_of == h, o_ref[:, h : h + 1], spike)
    decay = decay + spike
    lower = lax.broadcasted_iota(jnp.int32, (BLOCK, BLOCK), 0) >= lax.broadcasted_iota(
        jnp.int32, (BLOCK, BLOCK), 1
    )
    lower = lower.astype(jnp.float32)
    state_head = lane_head((vdim, width))
    state = jnp.zeros((vdim, width), jnp.float32)
    total = jnp.zeros((1, width), jnp.float32)
    for n in range(rows // BLOCK):
        at = slice(n * BLOCK, (n + 1) * BLOCK)
        within = jnp.dot(
            lower,
            decay[at],
            precision=lax.Precision.HIGHEST,
            preferred_element_type=jnp.float32,
        )
        within_ref[at, :] = within
        starts_ref[n] = state
        last = within[BLOCK - 1 : BLOCK]
        tail = (k_ref[at, :].astype(jnp.float32) * jnp.exp(last - within)).astype(jnp.bfloat16)
        added = jnp.zeros((vdim, width), jnp.float32)
        for h in range(heads):
            one = lax.dot_general(
                v_ref[at, h * vdim : (h + 1) * vdim],
                tail,
                (((0,), (0,)), ((), ())),
                preferred_element_type=jnp.float32,
            )
            added = jnp.where(state_head == h, one, added)
        state = state * jnp.exp(last) + added
        total = total + last
    factor = jnp.exp(total)
    high = factor.astype(jnp.bfloat16).astype(jnp.float32)
    low = factor - high
    row = lax.broadcasted_iota(jnp.int32, (MSG_PAD, width), 0)
    tail_rows = jnp.where(row == 0, high, jnp.where(row == 1, low, 0.0)).astype(jnp.bfloat16)
    state = state.astype(jnp.bfloat16)
    for j in range(msg_ref.shape[0]):
        msg_ref[j, :vdim, :] = state
        msg_ref[j, vdim:, :] = tail_rows


def mixer_kernel(
    place_ref, q_ref, k_ref, v_ref, within_ref, starts_ref, msg_ref, gate_ref, gain_ref, out_ref
):
    rows, width = k_ref.shape
    heads = width // KEY_CHANNELS
    vdim = v_ref.shape[1] // heads

    def hop(j, carried):
        message = msg_ref[j].astype(jnp.float32)
        factor = message[vdim : vdim + 1] + message[vdim + 1 : vdim + 2]
        return carried * factor + message[:vdim]

    carried = lax.fori_loop(0, place_ref[0], hop, jnp.zeros((vdim, width), jnp.float32))
    head_of = lane_head((BLOCK, width))
    causal = lax.broadcasted_iota(jnp.int32, (heads * BLOCK, BLOCK), 0) % BLOCK >= (
        lax.broadcasted_iota(jnp.int32, (heads * BLOCK, BLOCK), 1)
    )
    gain = gain_ref[...]
    before = jnp.zeros((1, width), jnp.float32)
    for n in range(rows // BLOCK):
        at = slice(n * BLOCK, (n + 1) * BLOCK)
        within = within_ref[at, :]
        queries = q_ref[at, :].astype(jnp.float32) * (KEY_CHANNELS**-0.5) * jnp.exp(within)
        grown = (k_ref[at, :].astype(jnp.float32) * jnp.exp(-within)).astype(jnp.bfloat16)
        split = jnp.concatenate(
            [jnp.where(head_of == h, queries, 0.0) for h in range(heads)], axis=0
        ).astype(jnp.bfloat16)
        scores = lax.dot_general(
            split, grown, (((1,), (1,)), ((), ())), preferred_element_type=jnp.float32
        )
        scores = jnp.where(causal, scores, 0.0).astype(jnp.bfloat16)
        entering = (starts_ref[n] + jnp.exp(before) * carried).astype(jnp.bfloat16)
        crossed = lax.dot_general(
            split, entering, (((1,), (1,)), ((), ())), preferred_element_type=jnp.float32
        )
        for h in range(heads):
            cols = slice(h * vdim, (h + 1) * vdim)
            own = slice(h * BLOCK, (h + 1) * BLOCK)
            output = crossed[own] + jnp.dot(
                scores[own], v_ref[at, cols], preferred_element_type=jnp.float32
            )
            scale = lax.rsqrt(jnp.mean(output * output, axis=-1, keepdims=True) + eps_norm)
            gate = gate_ref[at, cols].astype(jnp.float32)
            out_ref[at, cols] = (
                output * scale * gain * (gate / (1.0 + jnp.exp(-gate)))
            ).astype(jnp.bfloat16)
        before = before + within[BLOCK - 1 : BLOCK]


def mixer(queries, keys, values, channel_decay_input, head_decay_offset, gates, gain):
    rows, width = keys.shape
    vdim = gain.shape[0]
    seq = lax.axis_size("sp")
    within, starts, message = pl.pallas_call(
        state_kernel,
        out_shape=(
            jax.ShapeDtypeStruct((rows, width), jnp.float32),
            jax.ShapeDtypeStruct((rows // BLOCK, vdim, width), jnp.float32),
            jax.ShapeDtypeStruct((seq, vdim + MSG_PAD, width), jnp.bfloat16),
        ),
        name="mixer_state",
    )(keys, values, channel_decay_input, head_decay_offset)
    arrived = lax.all_to_all(message, "sp", split_axis=0, concat_axis=0, tiled=True)
    vmem = pl.BlockSpec(memory_space=pltpu.VMEM)
    return pl.pallas_call(
        mixer_kernel,
        in_specs=[pl.BlockSpec(memory_space=pltpu.SMEM)] + [vmem] * 8,
        out_specs=vmem,
        out_shape=jax.ShapeDtypeStruct(values.shape, jnp.bfloat16),
        name="mixer_output",
    )(
        lax.axis_index("sp").astype(jnp.int32).reshape(1),
        queries,
        keys,
        values,
        within,
        starts,
        arrived,
        gates,
        gain.reshape(1, vdim),
    )


def shared_block(rows, gate_weight, up_weight, down_weight):
    gate_pre = jnp.dot(rows, gate_weight, preferred_element_type=jnp.float32)
    up_pre = jnp.dot(rows, up_weight, preferred_element_type=jnp.float32)
    hidden = (jax.nn.silu(gate_pre) * up_pre).astype(jnp.bfloat16)
    return jnp.dot(hidden, down_weight, preferred_element_type=jnp.float32)


def apply_experts(arrived, routed_gate_weight, routed_up_weight, routed_down_weight):
    gate_pre = jnp.einsum(
        "sech,ehf->secf", arrived, routed_gate_weight, preferred_element_type=jnp.float32
    )
    up_pre = jnp.einsum(
        "sech,ehf->secf", arrived, routed_up_weight, preferred_element_type=jnp.float32
    )
    hidden = (jax.nn.silu(gate_pre) * up_pre).astype(jnp.bfloat16)
    return jnp.einsum(
        "secf,efh->sech", hidden, routed_down_weight, preferred_element_type=jnp.float32
    ).astype(jnp.bfloat16)


def slot_tables(chosen, weights, first_expert, slots, cap):
    tokens = chosen.shape[0]
    slot = lax.broadcasted_iota(jnp.int32, (tokens, slots), 1)
    expert = (first_expert + slot // cap).astype(jnp.float32)
    named = jnp.zeros((tokens, slots), jnp.float32)
    weight = jnp.zeros((tokens, slots), jnp.float32)
    for k in range(TOP_K):
        hit = chosen[:, k : k + 1] == expert
        named = jnp.where(hit, 1.0, named)
        weight = jnp.where(hit, weights[:, k : k + 1], weight)
    earlier = jnp.tril(jnp.ones((tokens, tokens), jnp.bfloat16), -1)
    rank = jnp.dot(earlier, named.astype(jnp.bfloat16), preferred_element_type=jnp.float32)
    held = (named > 0) & (rank == (slot % cap).astype(jnp.float32))
    weight = jnp.where(held, weight, 0.0)
    high = weight.astype(jnp.bfloat16)
    low = (weight - high.astype(jnp.float32)).astype(jnp.bfloat16)
    return held.astype(jnp.bfloat16), high, low


def pack(held, rows):
    return lax.dot_general(
        held, rows, (((0,), (0,)), ((), ())), preferred_element_type=jnp.float32
    ).astype(jnp.bfloat16)


def weigh(high, low, results):
    return jnp.dot(high, results, preferred_element_type=jnp.float32) + jnp.dot(
        low, results, preferred_element_type=jnp.float32
    )


def on_device(
    queries,
    key_matrix,
    value_matrix,
    channel_decay_input,
    head_decay_offset,
    output_gate_input,
    head_norm_gain,
    residual,
    mixer_output_weight,
    expert_norm_gain,
    routes,
    chosen_router_scores,
    routed_gate_weight,
    routed_up_weight,
    routed_down_weight,
    common_gate_weight,
    common_up_weight,
    common_down_weight,
):
    seq, heads_axis = lax.axis_size("sp"), lax.axis_size("tp")
    axes = ("sp", "tp")
    devices = seq * heads_axis
    half = devices // 2
    halves = [list(range(half)), list(range(half, devices))]
    swap = [(i, (i + seq // 2) % seq) for i in range(seq)]
    tok_count, width = residual.shape
    exp_dev = routed_gate_weight.shape[0]
    cap = 2 * TOP_K * tok_count // (exp_dev * devices)
    slots = exp_dev * half * cap
    first_expert = (lax.axis_index("sp") // (seq // 2)) * (exp_dev * half)

    weights = (
        routed_scale * chosen_router_scores / jnp.sum(chosen_router_scores, axis=-1, keepdims=True)
    )
    chosen = jnp.concatenate([routes.astype(jnp.float32), weights], axis=1)
    chosen_far = lax.ppermute(chosen, "sp", swap)
    held_near, high_near, low_near = slot_tables(
        chosen[:, :TOP_K], chosen[:, TOP_K:], first_expert, slots, cap
    )
    held_far, high_far, low_far = slot_tables(
        chosen_far[:, :TOP_K], chosen_far[:, TOP_K:], first_expert, slots, cap
    )

    gated = mixer(
        queries,
        key_matrix,
        value_matrix,
        channel_decay_input,
        head_decay_offset,
        output_gate_input,
        head_norm_gain,
    )
    stacked = gated.reshape(heads_axis, tok_count, gated.shape[1])
    projected = jnp.dot(
        lax.all_to_all(stacked, "tp", split_axis=0, concat_axis=2, tiled=True)[0],
        mixer_output_weight,
        preferred_element_type=jnp.float32,
    )
    middle = (residual.astype(jnp.float32) + projected).astype(jnp.bfloat16)
    middle_wide = middle.astype(jnp.float32)
    norm_scale = lax.rsqrt(jnp.mean(middle_wide * middle_wide, axis=-1, keepdims=True) + eps_norm)
    normed = (middle_wide * norm_scale * expert_norm_gain).astype(jnp.bfloat16)

    def spread(rows):
        return lax.all_to_all(
            rows.reshape(half, exp_dev * cap, width),
            axes,
            split_axis=0,
            concat_axis=0,
            axis_index_groups=halves,
            tiled=True,
        )

    def experts(arrived):
        return apply_experts(
            arrived.reshape(half, exp_dev, cap, width),
            routed_gate_weight,
            routed_up_weight,
            routed_down_weight,
        ).reshape(slots, width)

    normed_far = lax.ppermute(normed, "sp", swap)
    arrived_near = spread(pack(held_near, normed))
    arrived_far = spread(pack(held_far, normed_far))
    shared = shared_block(normed, common_gate_weight, common_up_weight, common_down_weight)
    done_near = experts(arrived_near)
    done_far = experts(arrived_far)
    back_far = spread(done_far).reshape(slots, width)
    far = weigh(high_far, low_far, back_far).astype(jnp.bfloat16)
    from_far = lax.ppermute(far, "sp", swap)
    back_near = spread(done_near).reshape(slots, width)
    routed = weigh(high_near, low_near, back_near) + from_far.astype(jnp.float32)
    return (middle_wide + routed + shared).astype(jnp.bfloat16)


def solution(mesh):
    placed = (
        P("sp", "tp"),
        P("sp", "tp"),
        P("sp", "tp"),
        P("sp", "tp"),
        P("sp", "tp"),
        P("sp", "tp"),
        P(),
        P(("sp", "tp"), None),
        P(),
        P(),
        P(("sp", "tp"), None),
        P(("sp", "tp"), None),
        P(("sp", "tp"), None, None),
        P(("sp", "tp"), None, None),
        P(("sp", "tp"), None, None),
        P(),
        P(),
        P(),
    )
    return jax.shard_map(
        on_device, mesh=mesh, in_specs=placed, out_specs=P(("sp", "tp"), None), check_vma=False
    )
```

time: 338 us -> 227 us (0.67)
  blocking collectives: 151 us -> 0 us
  local copies, waits for them, and re-layouts: 43.2 us -> 12.4 us
  starting transfers between devices: 7.35 us -> 34 us
  matrix products: 27.7 us -> 53.1 us
  waiting for transfers between devices: 92.8 us -> 116 us
  other arithmetic: 14.9 us -> 3.08 us
  Pallas kernels: 0 us -> 6.96 us
    all_to_all x1 -> x0, blocking collectives: 96.9 us -> none  [on_device(): lax.all_to_all(outgoing, ('sp', 'tp'), split_axis=0, concat_axis=0, tiled...]
    all_gather x2 -> x0, blocking collectives: 53.7 us -> none  [carried_in(): gathered = jax.tree.map(lambda a: lax.all_gather(a, axis), part)]
    ppermute x0 -> x3, waiting for transfers between devices: none -> 23.8 us  [the longest x1 23.8 us: on_device(): normed_far = lax.ppermute(normed, 'sp', swap)]
    all_to_all x1 -> x5, starting transfers between devices: 3.94 us -> 26.1 us  [the longest x4 18.8 us: spread(): lax.all_to_all(rows.reshape(half, exp_dev * cap, width), axes, split_axis...]
    dot_general x7 -> x10, matrix products: 9.12 us -> 23.5 us  [the longest x2 6.31 us: pack(): lax.dot_general(held, rows, (((0,), (0,)), ((), ())), preferred_element_t...]
    gather x2 -> x0, local copies, waits for them, and re-layouts: 14 us -> none  [the longest x1 8 us: on_device(): gathered = flat_back[destination].reshape(tok_count, TOP_K, D)]
    pallas_call x0 -> x2, Pallas kernels: none -> 6.96 us  [the longest x1 3.91 us: mixer(): pl.pallas_call(state_kernel, out_shape=(jax.ShapeDtypeStruct((rows, width...]
    reduce_sum x2 -> x0, other arithmetic: 6.53 us -> none  [the longest x1 6.41 us: on_device(): routed = jnp.sum(weights[:, :, None] * gathered, axis=1)]
  transfers between devices with their start and end apart: 2 -> 9, of which waited for: 2 -> 7; matrix products, arithmetic and copies ran while one was open for 2% -> 26% of each run, Pallas kernels for 0% -> 1%
where the time goes in v1:
time: 227 us; the launch traced here: 226 us
  waiting for transfers between devices  116 us (51%)
  matrix products  53.1 us (23%)
  starting transfers between devices  34 us (15%)
  local copies, waits for them, and re-layouts  12.4 us (5%)
  Pallas kernels  6.96 us (3%)
  other arithmetic  3.08 us (1%)
    all_to_all x4, waiting for transfers between devices, spread(): lax.all_to_all(rows.reshape(half, exp_dev * cap, width), axes, split_axis...  81.8 us
    ppermute x1, waiting for transfers between devices, on_device(): normed_far = lax.ppermute(normed, 'sp', swap)  23.8 us
    all_to_all x4, starting transfers between devices, spread(): lax.all_to_all(rows.reshape(half, exp_dev * cap, width), axes, split_axis...  18.8 us
    dot_general x2, matrix products, apply_experts(): jnp.einsum('secf,efh->sech', hidden, routed_down_weight, preferred_elemen...  16.3 us
    dot_general x2, matrix products, apply_experts(): jnp.einsum('sech,ehf->secf', arrived, routed_gate_weight, preferred_eleme...  10.1 us
    all_to_all x1, starting transfers between devices, mixer(): lax.all_to_all(message, 'sp', split_axis=0, concat_axis=0, tiled=True)  7.31 us
    convert_element_type x2, local copies, waits for them, and re-layouts, apply_experts(): return jnp.einsum('secf,efh->sech', hidden, routed_down_weight, preferred...  6.38 us
    dot_general x2, matrix products, pack(): lax.dot_general(held, rows, (((0,), (0,)), ((), ())), preferred_element_t...  6.31 us
  transfers between devices with their start and end apart: 9, of which 7 were waited for; matrix products, arithmetic and copies ran while one was open for 26% of the time, Pallas kernels for 1%

profile of v1, /device:TPU:0, one launch (start us, length us, event | category | flops | bytes accessed | tf_op | source)
XLA Modules:
  0.0 226.2 jit_solution(14491984630922561111)
XLA Ops:
  1.7 3.9 %mixer_state.1 = (f32[512,128]{1,0:T(8,128)}, f32[8,128,128]{2,1,0:T(8,128)}, bf16[8,144,128]{2,1,0:T(8,128)(2,1)}) custom-call(bf16[512,128]{1,0:T(8,128)(2,1)} %k_ref.3, bf16[512,256]{1,0:T(8,128)(2,1)} %v_ref.3, bf16[512,128]{1,0:T(8,128)(2,1)} %c_ref.1, f32[512,2]{1,0:T(8,128)} %copy.20.o_ref), custom_call_target="tpu_custom_call" | custom-call | tf_op jit(solution)/shard_map/mixer_state/pallas_call | solution.py:127
  5.6 7.3 %all-to-all-start = ((bf16[8,144,128]{2,1,0:T(8,128)(2,1)}), bf16[8,144,128]{2,1,0:T(8,128)(2,1)S(1)}, u32[]{:S(2)}, u32[]{:S(2)}) async-start(bf16[8,144,128]{2,1,0:T(8,128)(2,1)} %get-tuple-element.10), calls=%async_computation | async-start | bytes 589824 | tf_op jit(solution)/shard_map/all_to_all | solution.py:136
  15.0 3.0 %collective-permute-start = (f32[128,8]{0,1:T(8,128)S(1)}, f32[128,8]{0,1:T(8,128)S(1)}, u32[]{:S(2)}, u32[]{:S(2)}) collective-permute-start(f32[128,8]{0,1:T(8,128)S(1)} %pad_maximum_fusion), channel_id=1, source_target_pairs={{0,16},{4,20},{8,24},{12,28},{16,0},{20,4},{24,8},{28,12},{1,17},{... | collective-permute-start | bytes 12296 | tf_op jit(solution)/shard_map/ppermute | solution.py:244
  18.0 4.7 %all-to-all-done.msg_ref = bf16[8,144,128]{2,1,0:T(8,128)(2,1)S(1)} async-done(((bf16[8,144,128]{2,1,0:T(8,128)(2,1)}), bf16[8,144,128]{2,1,0:T(8,128)(2,1)S(1)}, u32[]{:S(2)}, u32[]{:S(2)}) %all-to-all-start) | async-done | bytes 294944 | tf_op jit(solution)/shard_map/all_to_all | solution.py:136
  23.4 3.1 %mixer_output.1 = bf16[512,256]{1,0:T(8,128)(2,1)} custom-call(s32[1]{0:T(128)} %bitcast.place_ref, bf16[512,128]{1,0:T(8,128)(2,1)} %q_ref.1, bf16[512,128]{1,0:T(8,128)(2,1)} %k_ref.3, bf16[512,256]{1,0:T(8,128)(2,1)} %v_ref.3, f32[512,128]{1,0:T(8,128)} %get-tuple-element.8.within_ref, f32[8,128,128]{2,1,0:T(8,128)} %get-tuple-element.9.starts_ref, ...), custom_call_target="tpu_custom_call" | custom-call | tf_op jit(solution)/shard_map/mixer_output/pallas_call | solution.py:138
  26.4 1.8 copy.21
  28.2 3.4 %all-to-all-start.1 = ((bf16[4,128,256]{1,2,0:T(8,128)(2,1)}), bf16[4,128,256]{1,2,0:T(8,128)(2,1)S(1)}, u32[]{:S(2)}, u32[]{:S(2)}) async-start(bf16[4,128,256]{1,2,0:T(8,128)(2,1)} %copy.21), calls=%async_computation.1 | async-start | bytes 524288 | tf_op jit(solution)/shard_map/all_to_all | solution.py:263
  31.7 5.9 %all-to-all-done.1 = bf16[4,128,256]{1,2,0:T(8,128)(2,1)S(1)} async-done(((bf16[4,128,256]{1,2,0:T(8,128)(2,1)}), bf16[4,128,256]{1,2,0:T(8,128)(2,1)S(1)}, u32[]{:S(2)}, u32[]{:S(2)}) %all-to-all-start.1) | async-done | bytes 262176 | tf_op jit(solution)/shard_map/all_to_all | solution.py:263
  37.6 3.1 %multiply_reduce_fusion = (f32[128]{0:T(128)S(1)}, f32[128,2048]{1,0:T(8,128)S(1)}) fusion(bf16[128,1024]{0,1:T(8,128)(2,1)S(1)} %bitcast.140, bf16[1024,2048]{1,0:T(8,128)(2,1)} %param.26, bf16[128,2048]{1,0:T(8,128)(2,1)} %param.25), kind=kOutput, calls=%fused_computation.45 | convolution fusion | flops 538443648 | bytes 6029824 | tf_op jit(solution)/shard_map/dot_general | solution.py:262
  43.8 23.8 %collective-permute-done.1 = bf16[128,2048]{1,0:T(8,128)(2,1)} collective-permute-done((bf16[128,2048]{1,0:T(8,128)(2,1)}, bf16[128,2048]{1,0:T(8,128)(2,1)}, u32[]{:S(2)}, u32[]{:S(2)}) %collective-permute-start.1) | collective-permute-done | bytes 524320 | tf_op jit(solution)/shard_map/ppermute | solution.py:290
  67.6 3.1 %convolution_convert_fusion = bf16[512,2048]{1,0:T(8,128)(2,1)} fusion(pred[128,512]{1,0:T(32,128)(4,1)S(1)} %fusion.74, bf16[128,2048]{1,0:T(8,128)(2,1)} %collective-permute-done.1), kind=kOutput, calls=%fused_computation.14 | convolution fusion | flops 269484032 | bytes 2686976 | tf_op jit(solution)/shard_map/dot_general | solution.py:197
  70.7 4.4 %all-to-all-start.4 = ((bf16[16,32,2048]{2,1,0:T(8,128)(2,1)}), bf16[16,32,2048]{2,1,0:T(8,128)(2,1)}, u32[]{:S(2)}, u32[]{:S(2)}) async-start(bf16[16,32,2048]{2,1,0:T(8,128)(2,1)} %bitcast.137), calls=%async_computation.4 | async-start | bytes 4194304 | tf_op jit(solution)/shard_map/all_to_all | solution.py:273
  76.2 3.2 %convolution_convert_fusion.1 = bf16[512,2048]{1,0:T(8,128)(2,1)} fusion(pred[128,512]{1,0:T(32,128)(4,1)S(1)} %fusion.73, bf16[128,2048]{1,0:T(8,128)(2,1)} %multiply_convert_fusion), kind=kOutput, calls=%fused_computation.15 | convolution fusion | flops 269484032 | bytes 2686976 | tf_op jit(solution)/shard_map/dot_general | solution.py:197
  79.3 24.9 %all-to-all-done.4 = bf16[16,32,2048]{2,1,0:T(8,128)(2,1)} async-done(((bf16[16,32,2048]{2,1,0:T(8,128)(2,1)}), bf16[16,32,2048]{2,1,0:T(8,128)(2,1)}, u32[]{:S(2)}, u32[]{:S(2)}) %all-to-all-start.4) | async-done | bytes 2097184 | tf_op jit(solution)/shard_map/all_to_all | solution.py:273
  104.3 4.5 %all-to-all-start.2 = ((bf16[16,32,2048]{2,1,0:T(8,128)(2,1)}), bf16[16,32,2048]{2,1,0:T(8,128)(2,1)}, u32[]{:S(2)}, u32[]{:S(2)}) async-start(bf16[16,32,2048]{2,1,0:T(8,128)(2,1)} %bitcast.139), calls=%async_computation.2 | async-start | bytes 4194304 | tf_op jit(solution)/shard_map/all_to_all | solution.py:273
  108.8 5.0 %fusion.36 = f32[16,2,16,512]{3,2,0,1:T(8,128)} fusion(bf16[2,2048,512]{2,1,0:T(8,128)(2,1)} %param.30, bf16[16,2,16,2048]{3,2,1,0:T(8,128)(2,1)} %bitcast.36), kind=kOutput, calls=%fused_computation.29 | convolution fusion | flops 1073741824 | bytes 7340032 | tf_op jit(solution)/shard_map/sech,ehf->secf/dot_general | solution.py:165
  113.8 8.1 %fusion.18 = bf16[16,2,16,2048]{3,2,0,1:T(8,128)(2,1)} fusion(bf16[2,512,2048]{2,1,0:T(8,128)(2,1)} %param.32, bf16[2,2048,512]{2,1,0:T(8,128)(2,1)} %param.31, bf16[16,2,16,2048]{3,2,1,0:T(8,128)(2,1)} %bitcast.36, f32[16,2,16,512]{3,2,0,1:T(8,128)} %fusion.36), kind=kOutput, calls=%fused_computation.16 | convolution fusion | flops 2150105088 | bytes 13631488 | tf_op jit(solution)/shard_map/secf,efh->sech/dot_general | solution.py:172
  121.9 3.2 %copy.25 = bf16[16,2,16,2048]{3,2,1,0:T(8,128)(2,1)} copy(bf16[16,2,16,2048]{3,2,0,1:T(8,128)(2,1)} %fusion.18) | data formatting | bytes 4194304 | tf_op jit(solution)/shard_map/convert_element_type | solution.py:174
  125.1 12.7 %all-to-all-done.2 = bf16[16,32,2048]{2,1,0:T(8,128)(2,1)} async-done(((bf16[16,32,2048]{2,1,0:T(8,128)(2,1)}), bf16[16,32,2048]{2,1,0:T(8,128)(2,1)}, u32[]{:S(2)}, u32[]{:S(2)}) %all-to-all-start.2) | async-done | bytes 2097184 | tf_op jit(solution)/shard_map/all_to_all | solution.py:273
  137.9 5.0 %all-to-all-start.5 = ((bf16[16,32,2048]{2,1,0:T(8,128)(2,1)}), bf16[16,32,2048]{2,1,0:T(8,128)(2,1)}, u32[]{:S(2)}, u32[]{:S(2)}) async-start(bf16[16,32,2048]{2,1,0:T(8,128)(2,1)} %bitcast.138), calls=%async_computation.5 | async-start | bytes 4194304 | tf_op jit(solution)/shard_map/all_to_all | solution.py:273
  142.8 5.0 %fusion.31 = f32[16,2,16,512]{3,2,0,1:T(8,128)} fusion(bf16[2,2048,512]{2,1,0:T(8,128)(2,1)} %param.30, bf16[16,2,16,2048]{3,2,1,0:T(8,128)(2,1)} %bitcast.15), kind=kOutput, calls=%fused_computation.28 | convolution fusion | flops 1073741824 | bytes 7340032 | tf_op jit(solution)/shard_map/sech,ehf->secf/dot_general | solution.py:165
  147.9 8.2 %fusion.21 = bf16[16,2,16,2048]{3,2,0,1:T(8,128)(2,1)} fusion(bf16[2,512,2048]{2,1,0:T(8,128)(2,1)} %param.32, bf16[2,2048,512]{2,1,0:T(8,128)(2,1)} %param.31, bf16[16,2,16,2048]{3,2,1,0:T(8,128)(2,1)} %bitcast.15, f32[16,2,16,512]{3,2,0,1:T(8,128)} %fusion.31), kind=kOutput, calls=%fused_computation.17 | convolution fusion | flops 2150105088 | bytes 13631488 | tf_op jit(solution)/shard_map/secf,efh->sech/dot_general | solution.py:172
  156.0 3.2 %copy.23 = bf16[16,2,16,2048]{3,2,1,0:T(8,128)(2,1)} copy(bf16[16,2,16,2048]{3,2,0,1:T(8,128)(2,1)} %fusion.21) | data formatting | bytes 4194304 | tf_op jit(solution)/shard_map/convert_element_type | solution.py:174
  159.2 12.7 %all-to-all-done.5 = bf16[16,32,2048]{2,1,0:T(8,128)(2,1)} async-done(((bf16[16,32,2048]{2,1,0:T(8,128)(2,1)}), bf16[16,32,2048]{2,1,0:T(8,128)(2,1)}, u32[]{:S(2)}, u32[]{:S(2)}) %all-to-all-start.5) | async-done | bytes 2097184 | tf_op jit(solution)/shard_map/all_to_all | solution.py:273
  171.9 4.9 %all-to-all-start.3 = ((bf16[16,32,2048]{2,1,0:T(8,128)(2,1)}), bf16[16,32,2048]{2,1,0:T(8,128)(2,1)}, u32[]{:S(2)}, u32[]{:S(2)}) async-start(bf16[16,32,2048]{2,1,0:T(8,128)(2,1)} %bitcast.136), calls=%async_computation.3 | async-start | bytes 4194304 | tf_op jit(solution)/shard_map/all_to_all | solution.py:273
  177.5 2.2 fusion.147
  179.8 2.2 fusion.116
  182.0 3.0 %fusion.26 = bf16[128,2048]{1,0:T(8,128)(2,1)} fusion(f32[128,2048]{1,0:T(8,128)S(1)} %fusion.116, bf16[512,2048]{1,0:T(8,128)(2,1)} %bitcast.44, pred[128,512]{1,0:T(32,128)(4,1)S(1)} %fusion.74, f32[128]{0:T(128)S(1)} %copy-done.4, f32[128]{0:T(128)S(1)} %copy-done.5, f32[128]{0:T(128)S(1)} %copy-done.6, f32[128]{0:T(128)S(1)} %copy-done.3, ...), kind=kOutput, calls=%fused_computation.23 | convolution fusion | flops 270008320 | bytes 3744260 | tf_op jit(solution)/shard_map/dot_general | solution.py:203
  185.5 31.4 %all-to-all-done.3 = bf16[16,32,2048]{2,1,0:T(8,128)(2,1)} async-done(((bf16[16,32,2048]{2,1,0:T(8,128)(2,1)}), bf16[16,32,2048]{2,1,0:T(8,128)(2,1)}, u32[]{:S(2)}, u32[]{:S(2)}) %all-to-all-start.3) | async-done | bytes 2097184 | tf_op jit(solution)/shard_map/all_to_all | solution.py:273
  216.9 2.2 fusion.119
  219.2 3.2 %convolution_add_fusion.1 = f32[128,2048]{1,0:T(8,128)} fusion(f32[128,2048]{1,0:T(8,128)S(1)} %fusion.119, bf16[512,2048]{1,0:T(8,128)(2,1)} %bitcast.26, pred[128,512]{1,0:T(32,128)(4,1)S(1)} %fusion.73, f32[128]{0:T(128)S(1)} %copy-done.24, f32[128]{0:T(128)S(1)} %copy-done.25, f32[128]{0:T(128)S(1)} %copy-done.26, f32[128]{0:T(128)S(1)} %copy-done.23, ...), kind=kOutput, calls=%fused_computation.19 | convolution fusion | flops 269746176 | bytes 4268548 | tf_op jit(solution)/shard_map/dot_general | solution.py:203
  222.3 3.8 %add_convert_fusion = bf16[128,2048]{1,0:T(8,128)(2,1)} fusion(f32[128,2048]{1,0:T(8,128)S(1)} %get-tuple-element.28, f32[128,2048]{1,0:T(8,128)} %convolution_add_fusion.1, bf16[128,2048]{1,0:T(8,128)(2,1)} %collective-permute-done.2, bf16[512,2048]{1,0:T(8,128)(2,1)S(1)} %copy-done, bf16[128,2048]{1,0:T(8,128)(2,1)} %multiply_convert_fusion, ...), kind=kOutput, calls=%fused_computation.43 | convolution fusion | flops 538574848 | bytes 8126464 | tf_op jit(solution)/shard_map/dot_general | solution.py:161
  (86 shorter events, 9.5 us)
Async XLA Ops:
  0.0 222.3 %copy-start = (bf16[512,2048]{1,0:T(8,128)(2,1)S(1)}, bf16[512,2048]{1,0:T(8,128)(2,1)}, u32[]{:S(2)}) copy-start(bf16[512,2048]{1,0:T(8,128)(2,1)} %param.35) | copy-start | bytes 6291460
  5.6 17.0 %all-to-all-start = ((bf16[8,144,128]{2,1,0:T(8,128)(2,1)}), bf16[8,144,128]{2,1,0:T(8,128)(2,1)S(1)}, u32[]{:S(2)}, u32[]{:S(2)}) async-start(bf16[8,144,128]{2,1,0:T(8,128)(2,1)} %get-tuple-element.10), calls=%async_computation | async-start | bytes 589824 | tf_op jit(solution)/shard_map/all_to_all | solution.py:136
  15.0 27.8 %collective-permute-start = (f32[128,8]{0,1:T(8,128)S(1)}, f32[128,8]{0,1:T(8,128)S(1)}, u32[]{:S(2)}, u32[]{:S(2)}) collective-permute-start(f32[128,8]{0,1:T(8,128)S(1)} %pad_maximum_fusion), channel_id=1, source_target_pairs={{0,16},{4,20},{8,24},{12,28},{16,0},{20,4},{24,8},{28,12},{1,17},{... | collective-permute-start | bytes 12296 | tf_op jit(solution)/shard_map/ppermute | solution.py:244
  18.0 25.4 %copy-start.27 = (s32[512]{0:T(512)}, s32[512]{0:T(512)S(1)}, u32[]{:S(2)}) copy-start(s32[512]{0:T(512)S(1)} %get-tuple-element.30) | copy-start | bytes 6148
  28.2 9.4 %all-to-all-start.1 = ((bf16[4,128,256]{1,2,0:T(8,128)(2,1)}), bf16[4,128,256]{1,2,0:T(8,128)(2,1)S(1)}, u32[]{:S(2)}, u32[]{:S(2)}) async-start(bf16[4,128,256]{1,2,0:T(8,128)(2,1)} %copy.21), calls=%async_computation.1 | async-start | bytes 524288 | tf_op jit(solution)/shard_map/all_to_all | solution.py:263
  31.7 11.8 %copy-start.31 = (pred[512]{0:T(512)(128)(4,1)}, pred[512]{0:T(512)(128)(4,1)S(1)}, u32[]{:S(2)}) copy-start(pred[512]{0:T(512)(128)(4,1)S(1)} %get-tuple-element.34) | copy-start | bytes 1540
  31.7 11.8 %copy-start.29 = (s32[512]{0:T(512)}, s32[512]{0:T(512)S(1)}, u32[]{:S(2)}) copy-start(s32[512]{0:T(512)S(1)} %get-tuple-element.31) | copy-start | bytes 6148
  37.6 3.1 %copy-start.2 = (f32[2048]{0:T(1024)S(1)}, f32[2048]{0:T(1024)}, u32[]{:S(2)}) copy-start(f32[2048]{0:T(1024)} %param.27) | copy-start | bytes 24580
  41.7 25.8 %collective-permute-start.1 = (bf16[128,2048]{1,0:T(8,128)(2,1)}, bf16[128,2048]{1,0:T(8,128)(2,1)}, u32[]{:S(2)}, u32[]{:S(2)}) collective-permute-start(bf16[128,2048]{1,0:T(8,128)(2,1)} %multiply_convert_fusion), channel_id=1, source_target_pairs={{0,16},{4,20},{8,24},{12,28},{16,0},{20,4},{24,8},{28,12},{1,17},{... | collective-permute-start | bytes 1572872 | tf_op jit(solution)/shard_map/ppermute | solution.py:290
  43.4 27.3 %copy-start.7 = (f32[128]{0:T(128)}, f32[128]{0:T(128)S(1)}, u32[]{:S(2)}) copy-start(f32[128]{0:T(128)S(1)} %get-tuple-element.15) | copy-start | bytes 1540
  43.4 27.3 %copy-start.9 = (f32[128]{0:T(128)}, f32[128]{0:T(128)S(1)}, u32[]{:S(2)}) copy-start(f32[128]{0:T(128)S(1)} %get-tuple-element.16) | copy-start | bytes 1540
  43.4 27.3 %copy-start.11 = (f32[128]{0:T(128)}, f32[128]{0:T(128)S(1)}, u32[]{:S(2)}) copy-start(f32[128]{0:T(128)S(1)} %get-tuple-element.17) | copy-start | bytes 1540
  43.4 27.3 %copy-start.13 = (f32[128]{0:T(128)}, f32[128]{0:T(128)S(1)}, u32[]{:S(2)}) copy-start(f32[128]{0:T(128)S(1)} %get-tuple-element.18) | copy-start | bytes 1540
  70.7 5.1 %copy-start.28 = (s32[512]{0:T(512)S(1)}, s32[512]{0:T(512)}, u32[]{:S(2)}) copy-start(s32[512]{0:T(512)} %copy-done.27) | copy-start | bytes 6148
  70.7 5.1 %copy-start.30 = (s32[512]{0:T(512)S(1)}, s32[512]{0:T(512)}, u32[]{:S(2)}) copy-start(s32[512]{0:T(512)} %copy-done.29) | copy-start | bytes 6148
  70.7 5.1 %copy-start.32 = (pred[512]{0:T(512)(128)(4,1)S(1)}, pred[512]{0:T(512)(128)(4,1)}, u32[]{:S(2)}) copy-start(pred[512]{0:T(512)(128)(4,1)} %copy-done.31) | copy-start | bytes 1540
  70.7 33.5 %all-to-all-start.4 = ((bf16[16,32,2048]{2,1,0:T(8,128)(2,1)}), bf16[16,32,2048]{2,1,0:T(8,128)(2,1)}, u32[]{:S(2)}, u32[]{:S(2)}) async-start(bf16[16,32,2048]{2,1,0:T(8,128)(2,1)} %bitcast.137), calls=%async_computation.4 | async-start | bytes 4194304 | tf_op jit(solution)/shard_map/all_to_all | solution.py:273
  104.3 33.6 %all-to-all-start.2 = ((bf16[16,32,2048]{2,1,0:T(8,128)(2,1)}), bf16[16,32,2048]{2,1,0:T(8,128)(2,1)}, u32[]{:S(2)}, u32[]{:S(2)}) async-start(bf16[16,32,2048]{2,1,0:T(8,128)(2,1)} %bitcast.139), calls=%async_computation.2 | async-start | bytes 4194304 | tf_op jit(solution)/shard_map/all_to_all | solution.py:273
  137.9 34.1 %all-to-all-start.5 = ((bf16[16,32,2048]{2,1,0:T(8,128)(2,1)}), bf16[16,32,2048]{2,1,0:T(8,128)(2,1)}, u32[]{:S(2)}, u32[]{:S(2)}) async-start(bf16[16,32,2048]{2,1,0:T(8,128)(2,1)} %bitcast.138), calls=%async_computation.5 | async-start | bytes 4194304 | tf_op jit(solution)/shard_map/all_to_all | solution.py:273
  171.9 45.0 %all-to-all-start.3 = ((bf16[16,32,2048]{2,1,0:T(8,128)(2,1)}), bf16[16,32,2048]{2,1,0:T(8,128)(2,1)}, u32[]{:S(2)}, u32[]{:S(2)}) async-start(bf16[16,32,2048]{2,1,0:T(8,128)(2,1)} %bitcast.136), calls=%async_computation.3 | async-start | bytes 4194304 | tf_op jit(solution)/shard_map/all_to_all | solution.py:273
  176.9 2.9 %copy-start.3 = (f32[128]{0:T(128)S(1)}, f32[128]{0:T(128)}, u32[]{:S(2)}) copy-start(f32[128]{0:T(128)} %get-tuple-element.11) | copy-start | bytes 1540
  176.9 2.9 %copy-start.4 = (f32[128]{0:T(128)S(1)}, f32[128]{0:T(128)}, u32[]{:S(2)}) copy-start(f32[128]{0:T(128)} %get-tuple-element.12) | copy-start | bytes 1540
  176.9 2.9 %copy-start.5 = (f32[128]{0:T(128)S(1)}, f32[128]{0:T(128)}, u32[]{:S(2)}) copy-start(f32[128]{0:T(128)} %get-tuple-element.13) | copy-start | bytes 1540
  182.0 34.8 %copy-start.16 = (f32[128]{0:T(128)S(1)}, f32[128]{0:T(128)}, u32[]{:S(2)}) copy-start(f32[128]{0:T(128)} %copy-done.15) | copy-start | bytes 1540
  185.0 34.1 %copy-start.18 = (f32[128]{0:T(128)S(1)}, f32[128]{0:T(128)}, u32[]{:S(2)}) copy-start(f32[128]{0:T(128)} %copy-done.17) | copy-start | bytes 1540
  185.0 34.1 %copy-start.20 = (f32[128]{0:T(128)S(1)}, f32[128]{0:T(128)}, u32[]{:S(2)}) copy-start(f32[128]{0:T(128)} %copy-done.19) | copy-start | bytes 1540
  185.0 34.1 %copy-start.22 = (f32[128]{0:T(128)S(1)}, f32[128]{0:T(128)}, u32[]{:S(2)}) copy-start(f32[128]{0:T(128)} %copy-done.21) | copy-start | bytes 1540
  185.0 34.1 %copy-start.23 = (f32[128]{0:T(128)S(1)}, f32[128]{0:T(128)}, u32[]{:S(2)}) copy-start(f32[128]{0:T(128)} %get-tuple-element.19) | copy-start | bytes 1540
  185.0 34.1 %copy-start.24 = (f32[128]{0:T(128)S(1)}, f32[128]{0:T(128)}, u32[]{:S(2)}) copy-start(f32[128]{0:T(128)} %get-tuple-element.20) | copy-start | bytes 1540
  185.1 34.1 %copy-start.25 = (f32[128]{0:T(128)S(1)}, f32[128]{0:T(128)}, u32[]{:S(2)}) copy-start(f32[128]{0:T(128)} %get-tuple-element.21) | copy-start | bytes 1540
  185.1 34.1 %copy-start.26 = (f32[128]{0:T(128)S(1)}, f32[128]{0:T(128)}, u32[]{:S(2)}) copy-start(f32[128]{0:T(128)} %get-tuple-element.22) | copy-start | bytes 1540
  185.1 37.3 %collective-permute-start.2 = (bf16[128,2048]{1,0:T(8,128)(2,1)}, bf16[128,2048]{1,0:T(8,128)(2,1)}, u32[]{:S(2)}, u32[]{:S(2)}) collective-permute-start(bf16[128,2048]{1,0:T(8,128)(2,1)} %fusion.26), channel_id=1, source_target_pairs={{0,16},{4,20},{8,24},{12,28},{16,0},{20,4},{24,8},{28,12},{1,17},{... | collective-permute-start | bytes 1572872 | tf_op jit(solution)/shard_map/ppermute | solution.py:298
  (10 other events, 17.6 us)

commit v2 on v1

--- a/solution.py
+++ b/solution.py
@@ -1,3 +1,5 @@
+import functools
+
 import jax
 import jax.numpy as jnp
 from jax import lax
@@ -21,15 +23,20 @@
 
 def state_kernel(k_ref, v_ref, c_ref, o_ref, within_ref, starts_ref, msg_ref):
     rows, width = k_ref.shape
-    heads = o_ref.shape[1]
+    heads = o_ref.shape[0]
     vdim = v_ref.shape[1] // heads
     x = c_ref[...].astype(jnp.float32)
     decay = (jnp.minimum(x, 0.0) - jnp.log1p(jnp.exp(-jnp.abs(x)))) / decay_running
-    head_of = lane_head((rows, width))
-    spike = jnp.zeros((rows, width), jnp.float32)
-    for h in range(heads):
-        spike = jnp.where(head_of == h, o_ref[:, h : h + 1], spike)
-    decay = decay + spike
+    columns_of = (
+        lax.broadcasted_iota(jnp.int32, (heads, width), 0) == lane_head((heads, width))
+    ).astype(jnp.float32)
+    decay = decay + lax.dot_general(
+        o_ref[...],
+        columns_of,
+        (((0,), (0,)), ((), ())),
+        precision=lax.Precision.HIGHEST,
+        preferred_element_type=jnp.float32,
+    )
     lower = lax.broadcasted_iota(jnp.int32, (BLOCK, BLOCK), 0) >= lax.broadcasted_iota(
         jnp.int32, (BLOCK, BLOCK), 1
     )
@@ -132,7 +139,7 @@
             jax.ShapeDtypeStruct((seq, vdim + MSG_PAD, width), jnp.bfloat16),
         ),
         name="mixer_state",
-    )(keys, values, channel_decay_input, head_decay_offset)
+    )(keys, values, channel_decay_input, head_decay_offset.T)
     arrived = lax.all_to_all(message, "sp", split_axis=0, concat_axis=0, tiled=True)
     vmem = pl.BlockSpec(memory_space=pltpu.VMEM)
     return pl.pallas_call(
@@ -154,55 +161,151 @@
     )
 
 
-def shared_block(rows, gate_weight, up_weight, down_weight):
-    gate_pre = jnp.dot(rows, gate_weight, preferred_element_type=jnp.float32)
-    up_pre = jnp.dot(rows, up_weight, preferred_element_type=jnp.float32)
-    hidden = (jax.nn.silu(gate_pre) * up_pre).astype(jnp.bfloat16)
-    return jnp.dot(hidden, down_weight, preferred_element_type=jnp.float32)
-
-
-def apply_experts(arrived, routed_gate_weight, routed_up_weight, routed_down_weight):
-    gate_pre = jnp.einsum(
-        "sech,ehf->secf", arrived, routed_gate_weight, preferred_element_type=jnp.float32
-    )
-    up_pre = jnp.einsum(
-        "sech,ehf->secf", arrived, routed_up_weight, preferred_element_type=jnp.float32
-    )
-    hidden = (jax.nn.silu(gate_pre) * up_pre).astype(jnp.bfloat16)
-    return jnp.einsum(
-        "secf,efh->sech", hidden, routed_down_weight, preferred_element_type=jnp.float32
-    ).astype(jnp.bfloat16)
-
-
-def slot_tables(chosen, weights, first_expert, slots, cap):
-    tokens = chosen.shape[0]
+def ffn_kernel(x_ref, gate_ref, up_ref, down_ref, *rest):
+    add_ref, out_ref, acc_ref = rest if len(rest) == 3 else (None,) + rest
+    step = pl.program_id(1)
+    rows = x_ref.shape[0] * x_ref.shape[1]
+    x = x_ref[...].reshape(rows, x_ref.shape[2])
+    gate_pre = jnp.dot(x, gate_ref[0], preferred_element_type=jnp.float32)
+    up_pre = jnp.dot(x, up_ref[0], preferred_element_type=jnp.float32)
+    hidden = (gate_pre / (1.0 + jnp.exp(-gate_pre)) * up_pre).astype(jnp.bfloat16)
+    part = jnp.dot(hidden, down_ref[0], preferred_element_type=jnp.float32)
+
+    @pl.when(step == 0)
+    def _():
+        acc_ref[...] = part
+
+    @pl.when(step != 0)
+    def _():
+        acc_ref[...] += part
+
+    @pl.when(step == pl.num_programs(1) - 1)
+    def _():
+        whole = acc_ref[...]
+        if add_ref is not None:
+            whole = whole + add_ref[...].astype(jnp.float32)
+        out_ref[...] = whole.astype(out_ref.dtype).reshape(out_ref.shape)
+
+
+def ffn(rows, gate_weight, up_weight, down_weight, cap, add=None):
+    sources, _, width = rows.shape
+    count, _, hidden = gate_weight.shape
+    steps = 2 if hidden % 256 == 0 else 1
+    piece = hidden // steps
+    row_spec = pl.BlockSpec((sources, cap, width), lambda e, f: (0, e, 0))
+    in_specs = [
+        row_spec,
+        pl.BlockSpec((1, width, piece), lambda e, f: (e, 0, f)),
+        pl.BlockSpec((1, width, piece), lambda e, f: (e, 0, f)),
+        pl.BlockSpec((1, piece, width), lambda e, f: (e, f, 0)),
+    ]
+    args = [rows, gate_weight, up_weight, down_weight]
+    dtype = jnp.bfloat16
+    if add is not None:
+        in_specs.append(pl.BlockSpec((sources * cap, width), lambda e, f: (0, 0)))
+        args.append(add)
+        dtype = jnp.float32
+    return pl.pallas_call(
+        ffn_kernel,
+        grid=(count, steps),
+        in_specs=in_specs,
+        out_specs=row_spec,
+        out_shape=jax.ShapeDtypeStruct(rows.shape, dtype),
+        scratch_shapes=[pltpu.VMEM((sources * cap, width), jnp.float32)],
+        compiler_params=pltpu.CompilerParams(vmem_limit_bytes=48 << 20),
+        cost_estimate=pl.CostEstimate(
+            flops=6 * rows.shape[0] * rows.shape[1] * width * hidden,
+            transcendentals=rows.shape[0] * rows.shape[1] * hidden,
+            bytes_accessed=6 * count * width * hidden + 4 * rows.size,
+        ),
+    )(*args)
+
+
+def slot_tables(chosen, first_expert, held_ref, weight_ref, cap):
+    tokens, slots = held_ref.shape
     slot = lax.broadcasted_iota(jnp.int32, (tokens, slots), 1)
     expert = (first_expert + slot // cap).astype(jnp.float32)
+    total = chosen[:, TOP_K : TOP_K + 1]
+    for k in range(1, TOP_K):
+        total = total + chosen[:, TOP_K + k : TOP_K + k + 1]
     named = jnp.zeros((tokens, slots), jnp.float32)
     weight = jnp.zeros((tokens, slots), jnp.float32)
     for k in range(TOP_K):
         hit = chosen[:, k : k + 1] == expert
         named = jnp.where(hit, 1.0, named)
-        weight = jnp.where(hit, weights[:, k : k + 1], weight)
-    earlier = jnp.tril(jnp.ones((tokens, tokens), jnp.bfloat16), -1)
-    rank = jnp.dot(earlier, named.astype(jnp.bfloat16), preferred_element_type=jnp.float32)
+        weight = jnp.where(
+            hit, routed_scale * chosen[:, TOP_K + k : TOP_K + k + 1] / total, weight
+        )
+    earlier = lax.broadcasted_iota(jnp.int32, (tokens, tokens), 0) > lax.broadcasted_iota(
+        jnp.int32, (tokens, tokens), 1
+    )
+    rank = jnp.dot(
+        jnp.where(earlier, 1.0, 0.0).astype(jnp.bfloat16),
+        named.astype(jnp.bfloat16),
+        preferred_element_type=jnp.float32,
+    )
     held = (named > 0) & (rank == (slot % cap).astype(jnp.float32))
     weight = jnp.where(held, weight, 0.0)
     high = weight.astype(jnp.bfloat16)
-    low = (weight - high.astype(jnp.float32)).astype(jnp.bfloat16)
-    return held.astype(jnp.bfloat16), high, low
-
-
-def pack(held, rows):
+    held_ref[...] = jnp.where(held, 1.0, 0.0).astype(jnp.bfloat16)
+    weight_ref[0] = high
+    weight_ref[1] = (weight - high.astype(jnp.float32)).astype(jnp.bfloat16)
+
+
+def tables_kernel(cap, first_ref, near_ref, far_ref, held_near, near_w, held_far, far_w):
+    slot_tables(near_ref[...], first_ref[0], held_near, near_w, cap)
+    slot_tables(far_ref[...], first_ref[0], held_far, far_w, cap)
+
+
+def pick(held, rows):
     return lax.dot_general(
         held, rows, (((0,), (0,)), ((), ())), preferred_element_type=jnp.float32
     ).astype(jnp.bfloat16)
 
 
-def weigh(high, low, results):
-    return jnp.dot(high, results, preferred_element_type=jnp.float32) + jnp.dot(
-        low, results, preferred_element_type=jnp.float32
-    )
+def project_kernel(g_ref, w_ref, res_ref, gain_ref, held_ref, mid_ref, norm_ref, sent_ref):
+    count, _, cols = g_ref.shape
+    total = res_ref[...].astype(jnp.float32)
+    for t in range(count):
+        total = total + jnp.dot(
+            g_ref[t], w_ref[t * cols : (t + 1) * cols, :], preferred_element_type=jnp.float32
+        )
+    middle = total.astype(jnp.bfloat16)
+    mid_ref[...] = middle
+    wide = middle.astype(jnp.float32)
+    scale = lax.rsqrt(jnp.mean(wide * wide, axis=-1, keepdims=True) + eps_norm)
+    normed = (wide * scale * gain_ref[...]).astype(jnp.bfloat16)
+    norm_ref[...] = normed
+    sent_ref[...] = pick(held_ref[...], normed)
+
+
+def pack_kernel(held_ref, rows_ref, sent_ref):
+    sent_ref[...] = pick(held_ref[...], rows_ref[...])
+
+
+def weighed(weight_ref, results_ref):
+    results = results_ref[...]
+    return jnp.dot(weight_ref[0], results, preferred_element_type=jnp.float32) + jnp.dot(
+        weight_ref[1], results, preferred_element_type=jnp.float32
+    )
+
+
+def far_kernel(weight_ref, results_ref, out_ref):
+    out_ref[...] = weighed(weight_ref, results_ref).astype(jnp.bfloat16)
+
+
+def final_kernel(weight_ref, results_ref, base_ref, far_ref, out_ref):
+    out_ref[...] = (
+        base_ref[...] + weighed(weight_ref, results_ref) + far_ref[...].astype(jnp.float32)
+    ).astype(jnp.bfloat16)
+
+
+def call(kernel, out, *args, scalars=0):
+    vmem = pl.BlockSpec(memory_space=pltpu.VMEM)
+    in_specs = [pl.BlockSpec(memory_space=pltpu.SMEM)] * scalars + [vmem] * (len(args) - scalars)
+    return pl.pallas_call(
+        kernel, in_specs=in_specs, out_specs=jax.tree.map(lambda _: vmem, out), out_shape=out
+    )(*args)
 
 
 def on_device(
@@ -235,20 +338,44 @@
     exp_dev = routed_gate_weight.shape[0]
     cap = 2 * TOP_K * tok_count // (exp_dev * devices)
     slots = exp_dev * half * cap
-    first_expert = (lax.axis_index("sp") // (seq // 2)) * (exp_dev * half)
-
-    weights = (
-        routed_scale * chosen_router_scores / jnp.sum(chosen_router_scores, axis=-1, keepdims=True)
-    )
-    chosen = jnp.concatenate([routes.astype(jnp.float32), weights], axis=1)
+    first_expert = lax.div(lax.axis_index("sp"), jnp.int32(seq // 2)) * (exp_dev * half)
+
+    def like(shape, dtype=jnp.bfloat16):
+        return jax.ShapeDtypeStruct(shape, dtype)
+
+    def spread(rows):
+        return lax.all_to_all(
+            rows.reshape(half, exp_dev * cap, width),
+            axes,
+            split_axis=0,
+            concat_axis=0,
+            axis_index_groups=halves,
+            tiled=True,
+        ).reshape(slots, width)
+
+    def experts(rows):
+        weights = (routed_gate_weight, routed_up_weight, routed_down_weight)
+        if cap % 16 == 0:
+            rows = rows.reshape(half, exp_dev * cap, width)
+            return ffn(rows, *weights, cap).reshape(slots, width)
+        order = (half, exp_dev, cap, width)
+        rows = rows.reshape(order).transpose(1, 0, 2, 3).reshape(1, slots, width)
+        done = ffn(rows, *weights, half * cap)
+        return done.reshape(exp_dev, half, cap, width).transpose(1, 0, 2, 3).reshape(slots, width)
+
+    packed = like((slots, width))
+    chosen = jnp.concatenate([routes.astype(jnp.float32), chosen_router_scores], axis=1)
     chosen_far = lax.ppermute(chosen, "sp", swap)
-    held_near, high_near, low_near = slot_tables(
-        chosen[:, :TOP_K], chosen[:, TOP_K:], first_expert, slots, cap
-    )
-    held_far, high_far, low_far = slot_tables(
-        chosen_far[:, :TOP_K], chosen_far[:, TOP_K:], first_expert, slots, cap
-    )
-
+    held = like((tok_count, slots))
+    slot_weights = like((2, tok_count, slots))
+    held_near, weights_near, held_far, weights_far = call(
+        functools.partial(tables_kernel, cap),
+        (held, slot_weights, held, slot_weights),
+        first_expert.astype(jnp.int32).reshape(1),
+        chosen,
+        chosen_far,
+        scalars=1,
+    )
     gated = mixer(
         queries,
         key_matrix,
@@ -259,46 +386,36 @@
         head_norm_gain,
     )
     stacked = gated.reshape(heads_axis, tok_count, gated.shape[1])
-    projected = jnp.dot(
-        lax.all_to_all(stacked, "tp", split_axis=0, concat_axis=2, tiled=True)[0],
+    stacked = lax.all_to_all(stacked, "tp", split_axis=0, concat_axis=0, tiled=True)
+    rows = like((tok_count, width))
+    middle, normed, sent_near = call(
+        project_kernel,
+        (rows, rows, packed),
+        stacked,
         mixer_output_weight,
-        preferred_element_type=jnp.float32,
-    )
-    middle = (residual.astype(jnp.float32) + projected).astype(jnp.bfloat16)
-    middle_wide = middle.astype(jnp.float32)
-    norm_scale = lax.rsqrt(jnp.mean(middle_wide * middle_wide, axis=-1, keepdims=True) + eps_norm)
-    normed = (middle_wide * norm_scale * expert_norm_gain).astype(jnp.bfloat16)
-
-    def spread(rows):
-        return lax.all_to_all(
-            rows.reshape(half, exp_dev * cap, width),
-            axes,
-            split_axis=0,
-            concat_axis=0,
-            axis_index_groups=halves,
-            tiled=True,
-        )
-
-    def experts(arrived):
-        return apply_experts(
-            arrived.reshape(half, exp_dev, cap, width),
-            routed_gate_weight,
-            routed_up_weight,
-            routed_down_weight,
-        ).reshape(slots, width)
-
+        residual,
+        expert_norm_gain.reshape(1, width),
+        held_near,
+    )
+    arrived_near = spread(sent_near)
     normed_far = lax.ppermute(normed, "sp", swap)
-    arrived_near = spread(pack(held_near, normed))
-    arrived_far = spread(pack(held_far, normed_far))
-    shared = shared_block(normed, common_gate_weight, common_up_weight, common_down_weight)
+    base = ffn(
+        normed[None],
+        common_gate_weight[None],
+        common_up_weight[None],
+        common_down_weight[None],
+        tok_count,
+        add=middle,
+    )[0]
+    sent_far = call(pack_kernel, packed, held_far, normed_far)
+    arrived_far = spread(sent_far)
     done_near = experts(arrived_near)
     done_far = experts(arrived_far)
-    back_far = spread(done_far).reshape(slots, width)
-    far = weigh(high_far, low_far, back_far).astype(jnp.bfloat16)
+    back_far = spread(done_far)
+    back_near = spread(done_near)
+    far = call(far_kernel, rows, weights_far, back_far)
     from_far = lax.ppermute(far, "sp", swap)
-    back_near = spread(done_near).reshape(slots, width)
-    routed = weigh(high_near, low_near, back_near) + from_far.astype(jnp.float32)
-    return (middle_wide + routed + shared).astype(jnp.bfloat16)
+    return call(final_kernel, rows, weights_near, back_near, base, from_far)
 
 
 def solution(mesh):

time: 227 us -> 221 us (0.974)
  matrix products: 53.1 us -> 0 us
  Pallas kernels: 6.96 us -> 46.5 us
  blocking collectives: 0 us -> 31.8 us
  waiting for transfers between devices: 116 us -> 108 us
  starting transfers between devices: 34 us -> 26.6 us
  local copies, waits for them, and re-layouts: 12.4 us -> 6.98 us
  other arithmetic: 3.08 us -> 0.01 us
    dot_general x15 -> x0, matrix products: 53.1 us -> none  [the longest x2 16.3 us: apply_experts(): jnp.einsum('secf,efh->sech', hidden, routed_down_weight, preferred_elemen...]
    pallas_call x0 -> x8, Pallas kernels: none -> 39.2 us  [the longest x3 20.9 us: ffn(): pl.pallas_call(ffn_kernel, grid=(count, steps), in_specs=in_specs, out_sp...]
    all_to_all x0 -> x1, blocking collectives: none -> 31.8 us  [spread(): lax.all_to_all(rows.reshape(half, exp_dev * cap, width), axes, split_axis...]
    all_to_all x4 -> x3, waiting for transfers between devices: 81.8 us -> 68.4 us  [spread(): lax.all_to_all(rows.reshape(half, exp_dev * cap, width), axes, split_axis...]
    convert_element_type x2 -> x0, local copies, waits for them, and re-layouts: 6.38 us -> none  [apply_experts(): return jnp.einsum('secf,efh->sech', hidden, routed_down_weight, preferred...]
    all_to_all x1, waiting for transfers between devices: 5.93 us -> 0.01 us  [on_device(): lax.all_to_all(stacked, 'tp', split_axis=0, concat_axis=0, tiled=True)]
    ppermute x1, waiting for transfers between devices: 0.01 us -> 5.64 us  [on_device(): chosen_far = lax.ppermute(chosen, 'sp', swap)]
    all_to_all x4 -> x3, starting transfers between devices: 18.8 us -> 13.3 us  [spread(): lax.all_to_all(rows.reshape(half, exp_dev * cap, width), axes, split_axis...]
  transfers between devices with their start and end apart: 9 -> 8, of which waited for: 7 -> 6; matrix products, arithmetic and copies ran while one was open for 26% -> 0% of each run, Pallas kernels for 1% -> 12%
where the time goes in v2:
time: 221 us; the launch traced here: 220 us
  waiting for transfers between devices  108 us (49%)
  Pallas kernels  46.5 us (21%)
  blocking collectives  31.8 us (14%)
  starting transfers between devices  26.6 us (12%)
  local copies, waits for them, and re-layouts  6.98 us (3%)
    all_to_all x3, waiting for transfers between devices, spread(): lax.all_to_all(rows.reshape(half, exp_dev * cap, width), axes, split_axis...  68.4 us
    all_to_all x1, blocking collectives, spread(): lax.all_to_all(rows.reshape(half, exp_dev * cap, width), axes, split_axis...  31.8 us
    ppermute x1, waiting for transfers between devices, on_device(): normed_far = lax.ppermute(normed, 'sp', swap)  24.9 us
    pallas_call x3, Pallas kernels, ffn(): pl.pallas_call(ffn_kernel, grid=(count, steps), in_specs=in_specs, out_sp...  20.9 us
    pallas_call x5, Pallas kernels, call(): pl.pallas_call(kernel, in_specs=in_specs, out_specs=jax.tree.map(lambda _...  18.3 us
    all_to_all x3, starting transfers between devices, spread(): lax.all_to_all(rows.reshape(half, exp_dev * cap, width), axes, split_axis...  13.3 us
    all_to_all x1, waiting for transfers between devices, mixer(): lax.all_to_all(message, 'sp', split_axis=0, concat_axis=0, tiled=True)  9.61 us
    all_to_all x1, starting transfers between devices, mixer(): lax.all_to_all(message, 'sp', split_axis=0, concat_axis=0, tiled=True)  7.31 us
  transfers between devices with their start and end apart: 8, of which 6 were waited for; matrix products, arithmetic and copies ran while one was open for 0% of the time, Pallas kernels for 12%

profile of v2, /device:TPU:0, one launch (start us, length us, event | category | flops | bytes accessed | tf_op | source)
XLA Modules:
  0.0 220.5 jit_solution(12276734816435122202)
XLA Ops:
  0.0 4.3 %mixer_state.1 = (f32[512,128]{1,0:T(8,128)}, f32[8,128,128]{2,1,0:T(8,128)}, bf16[8,144,128]{2,1,0:T(8,128)(2,1)}) custom-call(bf16[512,128]{1,0:T(8,128)(2,1)} %k_ref.3, bf16[512,256]{1,0:T(8,128)(2,1)} %v_ref.3, bf16[512,128]{1,0:T(8,128)(2,1)} %c_ref.1, f32[2,512]{1,0:T(2,128)} %bitcast.24), custom_call_target="tpu_custom_call" | custom-call | tf_op jit(solution)/shard_map/mixer_state/pallas_call | solution.py:134
  4.3 7.3 %all-to-all-start = ((bf16[8,144,128]{2,1,0:T(8,128)(2,1)}), bf16[8,144,128]{2,1,0:T(8,128)(2,1)S(1)}, u32[]{:S(2)}, u32[]{:S(2)}) async-start(bf16[8,144,128]{2,1,0:T(8,128)(2,1)} %get-tuple-element.18), calls=%async_computation | async-start | bytes 589824 | tf_op jit(solution)/shard_map/all_to_all | solution.py:143
  11.6 9.6 %all-to-all-done.msg_ref = bf16[8,144,128]{2,1,0:T(8,128)(2,1)S(1)} async-done(((bf16[8,144,128]{2,1,0:T(8,128)(2,1)}), bf16[8,144,128]{2,1,0:T(8,128)(2,1)S(1)}, u32[]{:S(2)}, u32[]{:S(2)}) %all-to-all-start) | async-done | bytes 294944 | tf_op jit(solution)/shard_map/all_to_all | solution.py:143
  21.2 0.7 copy-done.6
  21.9 3.1 %mixer_output.1 = bf16[512,256]{1,0:T(8,128)(2,1)} custom-call(s32[1]{0:T(128)} %bitcast.1.place_ref, bf16[512,128]{1,0:T(8,128)(2,1)} %q_ref.1, bf16[512,128]{1,0:T(8,128)(2,1)} %k_ref.3, bf16[512,256]{1,0:T(8,128)(2,1)} %v_ref.3, f32[512,128]{1,0:T(8,128)} %get-tuple-element.16.within_ref, f32[8,128,128]{2,1,0:T(8,128)} %get-tuple-element.17.starts_ref, ...), custom_call_target="tpu_custom_call" | custom-call | tf_op jit(solution)/shard_map/mixer_output/pallas_call | solution.py:145
  25.0 3.4 %all-to-all-start.1 = ((bf16[4,128,256]{2,1,0:T(8,128)(2,1)}), bf16[4,128,256]{2,1,0:T(8,128)(2,1)S(1)}, u32[]{:S(2)}, u32[]{:S(2)}) async-start(bf16[4,128,256]{2,1,0:T(8,128)(2,1)} %bitcast.22), calls=%async_computation.1 | async-start | bytes 524288 | tf_op jit(solution)/shard_map/all_to_all | solution.py:389
  28.4 0.1 copy.22.near_ref
  28.5 1.2 collective-permute-start
  29.7 5.6 %collective-permute-done.far_ref = f32[128,8]{1,0:T(8,128)S(1)} collective-permute-done((f32[128,8]{1,0:T(8,128)S(1)}, f32[128,8]{1,0:T(8,128)S(1)}, u32[]{:S(2)}, u32[]{:S(2)}) %collective-permute-start) | collective-permute-done | bytes 4128 | tf_op jit(solution)/shard_map/ppermute | solution.py:368
  35.4 0.6 copy-done.10
  36.0 2.8 %shard_map.172 = (bf16[128,512]{1,0:T(8,128)(2,1)}, bf16[2,128,512]{2,1,0:T(8,128)(2,1)}, bf16[128,512]{1,0:T(8,128)(2,1)}, bf16[2,128,512]{2,1,0:T(8,128)(2,1)}) custom-call(s32[1]{0:T(128)} %bitcast.first_ref, f32[128,8]{1,0:T(8,128)} %copy-done.9, f32[128,8]{1,0:T(8,128)} %copy-done.10), custom_call_target="tpu_custom_call" | custom-call | tf_op jit(solution)/shard_map/pallas_call | solution.py:306
  38.8 0.7 copy-done.7
  39.5 5.3 %shard_map.173 = (bf16[128,2048]{1,0:T(8,128)(2,1)}, bf16[128,2048]{1,0:T(8,128)(2,1)}, bf16[512,2048]{1,0:T(8,128)(2,1)}) custom-call(bf16[4,128,256]{2,1,0:T(8,128)(2,1)} %copy-done.7, bf16[1024,2048]{1,0:T(8,128)(2,1)} %w_ref.1, bf16[128,2048]{1,0:T(8,128)(2,1)} %res_ref.1, f32[1,2048]{1,0:T(1,128)} %bitcast.23, bf16[128,512]{1,0:T(8,128)(2,1)} %get-tuple-element.19.held_ref), custom_call_target="tpu_custom_call" | custom-call | tf_op jit(solution)/shard_map/pallas_call | solution.py:306
  44.8 24.9 %collective-permute-done.1.rows_ref = bf16[128,2048]{1,0:T(8,128)(2,1)S(1)} collective-permute-done((bf16[128,2048]{1,0:T(8,128)(2,1)}, bf16[128,2048]{1,0:T(8,128)(2,1)S(1)}, u32[]{:S(2)}, u32[]{:S(2)}) %collective-permute-start.1) | collective-permute-done | bytes 524320 | tf_op jit(solution)/shard_map/ppermute | solution.py:401
  69.7 0.8 copy-done.8
  70.5 3.1 %shard_map.176 = bf16[512,2048]{1,0:T(8,128)(2,1)} custom-call(bf16[128,512]{1,0:T(8,128)(2,1)} %get-tuple-element.24.held_ref, bf16[128,2048]{1,0:T(8,128)(2,1)} %copy-done.8), custom_call_target="tpu_custom_call" | custom-call | tf_op jit(solution)/shard_map/pallas_call | solution.py:306
  73.7 31.8 %all_to_all.30.x_ref = bf16[16,32,2048]{2,1,0:T(8,128)(2,1)} all-to-all(bf16[16,32,2048]{2,1,0:T(8,128)(2,1)} %bitcast.18), channel_id=1, replica_groups={{0,1,2,3,4,5,6,7,8,9,10,11,12,13,14,15},{16,17,18,19,20,21,22,23,24,25,..., dimensions={0} | all-to-all | bytes 4194304 | tf_op jit(solution)/shard_map/all_to_all | solution.py:347
  105.5 3.7 %all-to-all-start.2 = ((bf16[16,32,2048]{2,1,0:T(8,128)(2,1)}), bf16[16,32,2048]{2,1,0:T(8,128)(2,1)S(1)}, u32[]{:S(2)}, u32[]{:S(2)}) async-start(bf16[16,32,2048]{2,1,0:T(8,128)(2,1)} %bitcast.19), calls=%async_computation.2 | async-start | bytes 4194304 | tf_op jit(solution)/shard_map/all_to_all | solution.py:347
  109.2 1.6 copy-done.1
  110.8 8.2 %shard_map.177 = bf16[16,32,2048]{2,1,0:T(8,128)(2,1)S(1)} custom-call(bf16[16,32,2048]{2,1,0:T(8,128)(2,1)S(1)} %copy-done.1, bf16[2,2048,512]{2,1,0:T(8,128)(2,1)} %gate_ref.5, bf16[2,2048,512]{2,1,0:T(8,128)(2,1)} %up_ref.3, bf16[2,512,2048]{2,1,0:T(8,128)(2,1)} %down_ref.3), custom_call_target="tpu_custom_call" | custom-call | flops 3221225472 | bytes 16777216 | tf_op jit(solution)/shard_map/pallas_call | solution.py:208
  119.0 1.4 copy-done
  120.4 17.9 %all-to-all-done.2.x_ref = bf16[16,32,2048]{2,1,0:T(8,128)(2,1)S(1)} async-done(((bf16[16,32,2048]{2,1,0:T(8,128)(2,1)}), bf16[16,32,2048]{2,1,0:T(8,128)(2,1)S(1)}, u32[]{:S(2)}, u32[]{:S(2)}) %all-to-all-start.2) | async-done | bytes 2097184 | tf_op jit(solution)/shard_map/all_to_all | solution.py:347
  138.2 4.5 %all-to-all-start.5 = ((bf16[16,32,2048]{2,1,0:T(8,128)(2,1)}), bf16[16,32,2048]{2,1,0:T(8,128)(2,1)}, u32[]{:S(2)}, u32[]{:S(2)}) async-start(bf16[16,32,2048]{2,1,0:T(8,128)(2,1)} %copy-done), calls=%async_computation.5 | async-start | bytes 4194304 | tf_op jit(solution)/shard_map/all_to_all | solution.py:347
  142.7 9.4 %shard_map.174 = bf16[16,32,2048]{2,1,0:T(8,128)(2,1)} custom-call(bf16[16,32,2048]{2,1,0:T(8,128)(2,1)S(1)} %all-to-all-done.2.x_ref, bf16[2,2048,512]{2,1,0:T(8,128)(2,1)} %gate_ref.5, bf16[2,2048,512]{2,1,0:T(8,128)(2,1)} %up_ref.3, bf16[2,512,2048]{2,1,0:T(8,128)(2,1)} %down_ref.3), custom_call_target="tpu_custom_call" | custom-call | flops 3221225472 | bytes 16777216 | tf_op jit(solution)/shard_map/pallas_call | solution.py:208
  152.1 19.7 %all-to-all-done.5 = bf16[16,32,2048]{2,1,0:T(8,128)(2,1)} async-done(((bf16[16,32,2048]{2,1,0:T(8,128)(2,1)}), bf16[16,32,2048]{2,1,0:T(8,128)(2,1)}, u32[]{:S(2)}, u32[]{:S(2)}) %all-to-all-start.5) | async-done | bytes 2097184 | tf_op jit(solution)/shard_map/all_to_all | solution.py:347
  171.8 5.1 %all-to-all-start.3 = ((bf16[16,32,2048]{2,1,0:T(8,128)(2,1)}), bf16[16,32,2048]{2,1,0:T(8,128)(2,1)}, u32[]{:S(2)}, u32[]{:S(2)}) async-start(bf16[16,32,2048]{2,1,0:T(8,128)(2,1)} %shard_map.174), calls=%async_computation.3 | async-start | bytes 4194304 | tf_op jit(solution)/shard_map/all_to_all | solution.py:347
  176.9 3.4 %shard_map.178 = bf16[128,2048]{1,0:T(8,128)(2,1)} custom-call(bf16[2,128,512]{2,1,0:T(8,128)(2,1)} %get-tuple-element.23.weight_ref, bf16[512,2048]{1,0:T(8,128)(2,1)} %bitcast.14.results_ref), custom_call_target="tpu_custom_call" | custom-call | tf_op jit(solution)/shard_map/pallas_call | solution.py:306
  180.3 1.4 collective-permute-start.2
  181.7 3.3 %shard_map.175 = f32[1,128,2048]{2,1,0:T(8,128)S(1)} custom-call(bf16[1,128,2048]{2,1,0:T(8,128)(2,1)S(1)} %bitcast.17, bf16[1,2048,512]{2,1,0:T(8,128)(2,1)S(1)} %bitcast.16, bf16[1,2048,512]{2,1,0:T(8,128)(2,1)} %bitcast.20, bf16[1,512,2048]{2,1,0:T(8,128)(2,1)} %bitcast.21, bf16[128,2048]{1,0:T(8,128)(2,1)S(1)} %copy-done.4), custom_call_target="tpu_custom_call" | custom-call | flops 805306368 | bytes 7340032 | tf_op jit(solution)/shard_map/pallas_call | solution.py:208
  185.0 1.0 copy-done.2
  186.0 30.9 %all-to-all-done.3 = bf16[16,32,2048]{2,1,0:T(8,128)(2,1)} async-done(((bf16[16,32,2048]{2,1,0:T(8,128)(2,1)}), bf16[16,32,2048]{2,1,0:T(8,128)(2,1)}, u32[]{:S(2)}, u32[]{:S(2)}) %all-to-all-start.3) | async-done | bytes 2097184 | tf_op jit(solution)/shard_map/all_to_all | solution.py:347
  216.9 3.6 %shard_map.179 = bf16[128,2048]{1,0:T(8,128)(2,1)} custom-call(bf16[2,128,512]{2,1,0:T(8,128)(2,1)} %get-tuple-element.15.weight_ref, bf16[512,2048]{1,0:T(8,128)(2,1)} %bitcast.7.results_ref, f32[128,2048]{1,0:T(8,128)} %bitcast.15, bf16[128,2048]{1,0:T(8,128)(2,1)} %collective-permute-done.2.far_ref), custom_call_target="tpu_custom_call" | custom-call | tf_op jit(solution)/shard_map/pallas_call | solution.py:306
  (24 shorter events, 0.1 us)
Async XLA Ops:
  0.0 28.4 %copy-start.11 = (s32[128,4]{0,1:T(4,128)S(1)}, s32[128,4]{0,1:T(4,128)}, u32[]{:S(2)}) copy-start(s32[128,4]{0,1:T(4,128)} %param.28) | copy-start | bytes 6148
  0.0 28.4 %copy-start.12 = (f32[128,4]{0,1:T(4,128)S(1)}, f32[128,4]{0,1:T(4,128)}, u32[]{:S(2)}) copy-start(f32[128,4]{0,1:T(4,128)} %param.29) | copy-start | bytes 6148
  4.3 16.9 %all-to-all-start = ((bf16[8,144,128]{2,1,0:T(8,128)(2,1)}), bf16[8,144,128]{2,1,0:T(8,128)(2,1)S(1)}, u32[]{:S(2)}, u32[]{:S(2)}) async-start(bf16[8,144,128]{2,1,0:T(8,128)(2,1)} %get-tuple-element.18), calls=%async_computation | async-start | bytes 589824 | tf_op jit(solution)/shard_map/all_to_all | solution.py:143
  21.2 0.7 copy-start.6
  25.0 13.8 %all-to-all-start.1 = ((bf16[4,128,256]{2,1,0:T(8,128)(2,1)}), bf16[4,128,256]{2,1,0:T(8,128)(2,1)S(1)}, u32[]{:S(2)}, u32[]{:S(2)}) async-start(bf16[4,128,256]{2,1,0:T(8,128)(2,1)} %bitcast.22), calls=%async_computation.1 | async-start | bytes 524288 | tf_op jit(solution)/shard_map/all_to_all | solution.py:389
  28.5 6.8 %copy-start.9 = (f32[128,8]{1,0:T(8,128)}, f32[128,8]{1,0:T(8,128)S(1)}, u32[]{:S(2)}) copy-start(f32[128,8]{1,0:T(8,128)S(1)} %copy.22.near_ref) | copy-start | bytes 12292
  28.5 6.8 %collective-permute-start = (f32[128,8]{1,0:T(8,128)S(1)}, f32[128,8]{1,0:T(8,128)S(1)}, u32[]{:S(2)}, u32[]{:S(2)}) collective-permute-start(f32[128,8]{1,0:T(8,128)S(1)} %copy.22.near_ref), channel_id=1, source_target_pairs={{0,16},{4,20},{8,24},{12,28},{16,0},{20,4},{24,8},{28,12},{1,17},{... | collective-permute-start | bytes 12296 | tf_op jit(solution)/shard_map/ppermute | solution.py:368
  35.3 0.6 copy-start.10
  38.8 0.7 copy-start.7
  44.8 24.9 %collective-permute-start.1 = (bf16[128,2048]{1,0:T(8,128)(2,1)}, bf16[128,2048]{1,0:T(8,128)(2,1)S(1)}, u32[]{:S(2)}, u32[]{:S(2)}) collective-permute-start(bf16[128,2048]{1,0:T(8,128)(2,1)} %get-tuple-element.21), channel_id=1, source_target_pairs={{0,16},{4,20},{8,24},{12,28},{16,0},{20,4},{24,8},{28,12},{1,17},{... | collective-permute-start | bytes 1572872 | tf_op jit(solution)/shard_map/ppermute | solution.py:401
  69.7 0.8 copy-start.8
  105.5 32.8 %all-to-all-start.2 = ((bf16[16,32,2048]{2,1,0:T(8,128)(2,1)}), bf16[16,32,2048]{2,1,0:T(8,128)(2,1)S(1)}, u32[]{:S(2)}, u32[]{:S(2)}) async-start(bf16[16,32,2048]{2,1,0:T(8,128)(2,1)} %bitcast.19), calls=%async_computation.2 | async-start | bytes 4194304 | tf_op jit(solution)/shard_map/all_to_all | solution.py:347
  109.2 1.6 copy-start.1
  119.0 1.4 copy-start
  138.2 33.5 %all-to-all-start.5 = ((bf16[16,32,2048]{2,1,0:T(8,128)(2,1)}), bf16[16,32,2048]{2,1,0:T(8,128)(2,1)}, u32[]{:S(2)}, u32[]{:S(2)}) async-start(bf16[16,32,2048]{2,1,0:T(8,128)(2,1)} %copy-done), calls=%async_computation.5 | async-start | bytes 4194304 | tf_op jit(solution)/shard_map/all_to_all | solution.py:347
  171.8 9.9 %copy-start.5 = (bf16[128,2048]{1,0:T(8,128)(2,1)S(1)}, bf16[128,2048]{1,0:T(8,128)(2,1)}, u32[]{:S(2)}) copy-start(bf16[128,2048]{1,0:T(8,128)(2,1)} %get-tuple-element.21) | copy-start | bytes 1572868
  171.8 45.1 %all-to-all-start.3 = ((bf16[16,32,2048]{2,1,0:T(8,128)(2,1)}), bf16[16,32,2048]{2,1,0:T(8,128)(2,1)}, u32[]{:S(2)}, u32[]{:S(2)}) async-start(bf16[16,32,2048]{2,1,0:T(8,128)(2,1)} %shard_map.174), calls=%async_computation.3 | async-start | bytes 4194304 | tf_op jit(solution)/shard_map/all_to_all | solution.py:347
  176.9 4.8 %copy-start.3 = (bf16[2048,512]{1,0:T(8,128)(2,1)S(1)}, bf16[2048,512]{1,0:T(8,128)(2,1)}, u32[]{:S(2)}) copy-start(bf16[2048,512]{1,0:T(8,128)(2,1)} %param.33) | copy-start | bytes 6291460
  176.9 4.8 %copy-start.4 = (bf16[128,2048]{1,0:T(8,128)(2,1)S(1)}, bf16[128,2048]{1,0:T(8,128)(2,1)}, u32[]{:S(2)}) copy-start(bf16[128,2048]{1,0:T(8,128)(2,1)} %get-tuple-element.22.rest_0_) | copy-start | bytes 1572868
  180.3 36.6 %collective-permute-start.2 = (bf16[128,2048]{1,0:T(8,128)(2,1)}, bf16[128,2048]{1,0:T(8,128)(2,1)}, u32[]{:S(2)}, u32[]{:S(2)}) collective-permute-start(bf16[128,2048]{1,0:T(8,128)(2,1)} %shard_map.178), channel_id=1, source_target_pairs={{0,16},{4,20},{8,24},{12,28},{16,0},{20,4},{24,8},{28,12},{1,17},{... | collective-permute-start | bytes 1572872 | tf_op jit(solution)/shard_map/ppermute | solution.py:417
  185.0 1.0 copy-start.2

commit v3 on v2

--- a/solution.py
+++ b/solution.py
@@ -21,7 +21,14 @@
     return lax.broadcasted_iota(jnp.int32, shape, 1) // KEY_CHANNELS
 
 
-def state_kernel(k_ref, v_ref, c_ref, o_ref, within_ref, starts_ref, msg_ref):
+def two_pieces(value):
+    high = value.astype(jnp.bfloat16).astype(jnp.float32)
+    return high, value - high
+
+
+def state_kernel(
+    k_ref, v_ref, c_ref, o_ref, routes_ref, scores_ref, within_ref, starts_ref, msg_ref
+):
     rows, width = k_ref.shape
     heads = o_ref.shape[0]
     vdim = v_ref.shape[1] // heads
@@ -68,10 +75,15 @@
         state = state * jnp.exp(last) + added
         total = total + last
     factor = jnp.exp(total)
-    high = factor.astype(jnp.bfloat16).astype(jnp.float32)
-    low = factor - high
+    tail_rows = jnp.zeros((MSG_PAD, width), jnp.float32)
     row = lax.broadcasted_iota(jnp.int32, (MSG_PAD, width), 0)
-    tail_rows = jnp.where(row == 0, high, jnp.where(row == 1, low, 0.0)).astype(jnp.bfloat16)
+    scores = scores_ref[...]
+    place = 0
+    for value in two_pieces(factor) + (routes_ref[...].astype(jnp.float32),) + two_pieces(scores):
+        for r in range(value.shape[0]):
+            tail_rows = jnp.where(row == place, value[r : r + 1], tail_rows)
+            place += 1
+    tail_rows = tail_rows.astype(jnp.bfloat16)
     state = state.astype(jnp.bfloat16)
     for j in range(msg_ref.shape[0]):
         msg_ref[j, :vdim, :] = state
@@ -127,38 +139,21 @@
         before = before + within[BLOCK - 1 : BLOCK]
 
 
-def mixer(queries, keys, values, channel_decay_input, head_decay_offset, gates, gain):
-    rows, width = keys.shape
-    vdim = gain.shape[0]
-    seq = lax.axis_size("sp")
-    within, starts, message = pl.pallas_call(
-        state_kernel,
-        out_shape=(
-            jax.ShapeDtypeStruct((rows, width), jnp.float32),
-            jax.ShapeDtypeStruct((rows // BLOCK, vdim, width), jnp.float32),
-            jax.ShapeDtypeStruct((seq, vdim + MSG_PAD, width), jnp.bfloat16),
-        ),
-        name="mixer_state",
-    )(keys, values, channel_decay_input, head_decay_offset.T)
-    arrived = lax.all_to_all(message, "sp", split_axis=0, concat_axis=0, tiled=True)
-    vmem = pl.BlockSpec(memory_space=pltpu.VMEM)
+def call(kernel, out, *args, scalars=0):
+    def whole(x):
+        return pl.BlockSpec(x.shape, lambda i, rank=len(x.shape): (0,) * rank)
+
+    in_specs = [pl.BlockSpec(memory_space=pltpu.SMEM)] * scalars + [
+        whole(x) for x in args[scalars:]
+    ]
     return pl.pallas_call(
-        mixer_kernel,
-        in_specs=[pl.BlockSpec(memory_space=pltpu.SMEM)] + [vmem] * 8,
-        out_specs=vmem,
-        out_shape=jax.ShapeDtypeStruct(values.shape, jnp.bfloat16),
-        name="mixer_output",
-    )(
-        lax.axis_index("sp").astype(jnp.int32).reshape(1),
-        queries,
-        keys,
-        values,
-        within,
-        starts,
-        arrived,
-        gates,
-        gain.reshape(1, vdim),
-    )
+        kernel,
+        grid=(1,),
+        in_specs=in_specs,
+        out_specs=jax.tree.map(whole, out),
+        out_shape=out,
+        compiler_params=pltpu.CompilerParams(vmem_limit_bytes=48 << 20),
+    )(*args)
 
 
 def ffn_kernel(x_ref, gate_ref, up_ref, down_ref, *rest):
@@ -221,72 +216,132 @@
     )(*args)
 
 
-def slot_tables(chosen, first_expert, held_ref, weight_ref, cap):
-    tokens, slots = held_ref.shape
-    slot = lax.broadcasted_iota(jnp.int32, (tokens, slots), 1)
-    expert = (first_expert + slot // cap).astype(jnp.float32)
-    total = chosen[:, TOP_K : TOP_K + 1]
-    for k in range(1, TOP_K):
-        total = total + chosen[:, TOP_K + k : TOP_K + k + 1]
-    named = jnp.zeros((tokens, slots), jnp.float32)
-    weight = jnp.zeros((tokens, slots), jnp.float32)
+def slot_tables(routes, scores, first_expert, held_ref, weight_ref, cap):
+    slots, tokens = held_ref.shape
+    slot = lax.broadcasted_iota(jnp.int32, (slots, tokens), 0)
+    expert = (first_expert + lax.div(slot, jnp.int32(cap))).astype(jnp.float32)
+    weights = routed_scale * scores / jnp.sum(scores, axis=0, keepdims=True)
+    named = jnp.zeros((slots, tokens), jnp.float32)
+    weight = jnp.zeros((slots, tokens), jnp.float32)
     for k in range(TOP_K):
-        hit = chosen[:, k : k + 1] == expert
+        hit = routes[k : k + 1] == expert
         named = jnp.where(hit, 1.0, named)
-        weight = jnp.where(
-            hit, routed_scale * chosen[:, TOP_K + k : TOP_K + k + 1] / total, weight
-        )
-    earlier = lax.broadcasted_iota(jnp.int32, (tokens, tokens), 0) > lax.broadcasted_iota(
+        weight = jnp.where(hit, weights[k : k + 1], weight)
+    earlier = lax.broadcasted_iota(jnp.int32, (tokens, tokens), 0) < lax.broadcasted_iota(
         jnp.int32, (tokens, tokens), 1
     )
     rank = jnp.dot(
+        named.astype(jnp.bfloat16),
         jnp.where(earlier, 1.0, 0.0).astype(jnp.bfloat16),
-        named.astype(jnp.bfloat16),
         preferred_element_type=jnp.float32,
     )
-    held = (named > 0) & (rank == (slot % cap).astype(jnp.float32))
-    weight = jnp.where(held, weight, 0.0)
-    high = weight.astype(jnp.bfloat16)
+    held = (named > 0) & (rank == lax.rem(slot, jnp.int32(cap)).astype(jnp.float32))
     held_ref[...] = jnp.where(held, 1.0, 0.0).astype(jnp.bfloat16)
-    weight_ref[0] = high
-    weight_ref[1] = (weight - high.astype(jnp.float32)).astype(jnp.bfloat16)
-
-
-def tables_kernel(cap, first_ref, near_ref, far_ref, held_near, near_w, held_far, far_w):
-    slot_tables(near_ref[...], first_ref[0], held_near, near_w, cap)
-    slot_tables(far_ref[...], first_ref[0], held_far, far_w, cap)
+    high, low = two_pieces(jnp.where(held, weight, 0.0).T)
+    weight_ref[0] = high.astype(jnp.bfloat16)
+    weight_ref[1] = low.astype(jnp.bfloat16)
+
+
+def tables_kernel(
+    cap, place_ref, routes_ref, scores_ref, far_ref, held_near, near_w, held_far, far_w
+):
+    slot_tables(
+        routes_ref[...].astype(jnp.float32), scores_ref[...], place_ref[0], held_near, near_w, cap
+    )
+    far = far_ref[0].astype(jnp.float32)
+    at = [far[2 + k * TOP_K : 2 + (k + 1) * TOP_K] for k in range(3)]
+    slot_tables(at[0], at[1] + at[2], place_ref[0], held_far, far_w, cap)
+
+
+def tables(places, routes, scores, arrived, slots, cap):
+    tokens = routes.shape[1]
+    vdim = arrived.shape[1] - MSG_PAD
+    held = jax.ShapeDtypeStruct((slots, tokens), jnp.bfloat16)
+    weights = jax.ShapeDtypeStruct((2, tokens, slots), jnp.bfloat16)
+
+    def whole(x):
+        return pl.BlockSpec(x.shape, lambda i, p, rank=len(x.shape): (0,) * rank)
+
+    out = (held, weights, held, weights)
+    return pl.pallas_call(
+        functools.partial(tables_kernel, cap),
+        grid_spec=pltpu.PrefetchScalarGridSpec(
+            num_scalar_prefetch=1,
+            grid=(1,),
+            in_specs=[
+                whole(routes),
+                whole(scores),
+                pl.BlockSpec(
+                    (1, MSG_PAD, arrived.shape[2]), lambda i, p: (p[1], vdim // MSG_PAD, 0)
+                ),
+            ],
+            out_specs=jax.tree.map(whole, out),
+        ),
+        out_shape=out,
+        name="tables",
+    )(places, routes, scores, arrived)
 
 
 def pick(held, rows):
-    return lax.dot_general(
-        held, rows, (((0,), (0,)), ((), ())), preferred_element_type=jnp.float32
-    ).astype(jnp.bfloat16)
-
-
-def project_kernel(g_ref, w_ref, res_ref, gain_ref, held_ref, mid_ref, norm_ref, sent_ref):
-    count, _, cols = g_ref.shape
-    total = res_ref[...].astype(jnp.float32)
-    for t in range(count):
-        total = total + jnp.dot(
-            g_ref[t], w_ref[t * cols : (t + 1) * cols, :], preferred_element_type=jnp.float32
-        )
-    middle = total.astype(jnp.bfloat16)
-    mid_ref[...] = middle
-    wide = middle.astype(jnp.float32)
-    scale = lax.rsqrt(jnp.mean(wide * wide, axis=-1, keepdims=True) + eps_norm)
-    normed = (wide * scale * gain_ref[...]).astype(jnp.bfloat16)
-    norm_ref[...] = normed
-    sent_ref[...] = pick(held_ref[...], normed)
-
-
-def pack_kernel(held_ref, rows_ref, sent_ref):
-    sent_ref[...] = pick(held_ref[...], rows_ref[...])
+    return jnp.dot(held, rows, preferred_element_type=jnp.float32).astype(jnp.bfloat16)
+
+
+def project_kernel(g_ref, w_ref, res_ref, gain_ref, held_ref, sent_ref, *rest):
+    acc_ref = rest[-1]
+    step = pl.program_id(0)
+    part = jnp.dot(g_ref[0], w_ref[...], preferred_element_type=jnp.float32)
+
+    @pl.when(step == 0)
+    def _():
+        acc_ref[...] = res_ref[...].astype(jnp.float32) + part
+
+    @pl.when(step != 0)
+    def _():
+        acc_ref[...] += part
+
+    @pl.when(step == pl.num_programs(0) - 1)
+    def _():
+        middle = acc_ref[...].astype(jnp.bfloat16)
+        wide = middle.astype(jnp.float32)
+        scale = lax.rsqrt(jnp.mean(wide * wide, axis=-1, keepdims=True) + eps_norm)
+        normed = (wide * scale * gain_ref[...]).astype(jnp.bfloat16)
+        sent_ref[...] = pick(held_ref[...], normed)
+        if len(rest) == 3:
+            rest[0][...] = middle
+            rest[1][...] = normed
+
+
+def project(stacked, weight, residual, gain, held, keep_rows):
+    count, tokens, cols = stacked.shape
+    width = residual.shape[1]
+    slots = held.shape[0]
+    out = [jax.ShapeDtypeStruct((slots, width), jnp.bfloat16)]
+    if keep_rows:
+        out += [jax.ShapeDtypeStruct((tokens, width), jnp.bfloat16)] * 2
+
+    def whole(x):
+        return pl.BlockSpec(x.shape, lambda t, rank=len(x.shape): (0,) * rank)
+
+    return pl.pallas_call(
+        project_kernel,
+        grid=(count,),
+        in_specs=[
+            pl.BlockSpec((1, tokens, cols), lambda t: (t, 0, 0)),
+            pl.BlockSpec((cols, width), lambda t: (t, 0)),
+            whole(residual),
+            whole(gain),
+            whole(held),
+        ],
+        out_specs=[whole(x) for x in out],
+        out_shape=out,
+        scratch_shapes=[pltpu.VMEM((tokens, width), jnp.float32)],
+        compiler_params=pltpu.CompilerParams(vmem_limit_bytes=48 << 20),
+    )(stacked, weight, residual, gain, held)
 
 
 def weighed(weight_ref, results_ref):
-    results = results_ref[...]
-    return jnp.dot(weight_ref[0], results, preferred_element_type=jnp.float32) + jnp.dot(
-        weight_ref[1], results, preferred_element_type=jnp.float32
+    return jnp.dot(weight_ref[0], results_ref[...], preferred_element_type=jnp.float32) + jnp.dot(
+        weight_ref[1], results_ref[...], preferred_element_type=jnp.float32
     )
 
 
@@ -300,12 +355,20 @@
     ).astype(jnp.bfloat16)
 
 
-def call(kernel, out, *args, scalars=0):
-    vmem = pl.BlockSpec(memory_space=pltpu.VMEM)
-    in_specs = [pl.BlockSpec(memory_space=pltpu.SMEM)] * scalars + [vmem] * (len(args) - scalars)
+def by_columns(kernel, out, weights, *args):
+    steps = 4 if out.shape[1] % 512 == 0 else 1
+    piece = out.shape[1] // steps
+
+    def part(x):
+        return pl.BlockSpec((x.shape[0], piece), lambda c: (0, c))
+
     return pl.pallas_call(
-        kernel, in_specs=in_specs, out_specs=jax.tree.map(lambda _: vmem, out), out_shape=out
-    )(*args)
+        kernel,
+        grid=(steps,),
+        in_specs=[pl.BlockSpec(weights.shape, lambda c: (0, 0, 0))] + [part(x) for x in args],
+        out_specs=part(out),
+        out_shape=out,
+    )(weights, *args)
 
 
 def on_device(
@@ -338,7 +401,9 @@
     exp_dev = routed_gate_weight.shape[0]
     cap = 2 * TOP_K * tok_count // (exp_dev * devices)
     slots = exp_dev * half * cap
-    first_expert = lax.div(lax.axis_index("sp"), jnp.int32(seq // 2)) * (exp_dev * half)
+    place = lax.axis_index("sp").astype(jnp.int32)
+    first_expert = lax.div(place, jnp.int32(seq // 2)) * (exp_dev * half)
+    far_place = lax.rem(place + seq // 2, jnp.int32(seq))
 
     def like(shape, dtype=jnp.bfloat16):
         return jax.ShapeDtypeStruct(shape, dtype)
@@ -363,42 +428,50 @@
         done = ffn(rows, *weights, half * cap)
         return done.reshape(exp_dev, half, cap, width).transpose(1, 0, 2, 3).reshape(slots, width)
 
-    packed = like((slots, width))
-    chosen = jnp.concatenate([routes.astype(jnp.float32), chosen_router_scores], axis=1)
-    chosen_far = lax.ppermute(chosen, "sp", swap)
-    held = like((tok_count, slots))
-    slot_weights = like((2, tok_count, slots))
-    held_near, weights_near, held_far, weights_far = call(
-        functools.partial(tables_kernel, cap),
-        (held, slot_weights, held, slot_weights),
-        first_expert.astype(jnp.int32).reshape(1),
-        chosen,
-        chosen_far,
-        scalars=1,
-    )
-    gated = mixer(
+    key_rows, key_cols = key_matrix.shape
+    vdim = head_norm_gain.shape[0]
+    routes_t, scores_t = routes.T, chosen_router_scores.T
+    within, starts, message = call(
+        state_kernel,
+        (
+            like((key_rows, key_cols), jnp.float32),
+            like((key_rows // BLOCK, vdim, key_cols), jnp.float32),
+            like((seq, vdim + MSG_PAD, key_cols)),
+        ),
+        key_matrix,
+        value_matrix,
+        channel_decay_input,
+        head_decay_offset.T,
+        routes_t,
+        scores_t,
+    )
+    arrived = lax.all_to_all(message, "sp", split_axis=0, concat_axis=0, tiled=True)
+    residual_far = lax.ppermute(residual, "sp", swap)
+    gated = call(
+        mixer_kernel,
+        like(value_matrix.shape),
+        place.reshape(1),
         queries,
         key_matrix,
         value_matrix,
-        channel_decay_input,
-        head_decay_offset,
+        within,
+        starts,
+        arrived,
         output_gate_input,
-        head_norm_gain,
+        head_norm_gain.reshape(1, vdim),
+        scalars=1,
     )
     stacked = gated.reshape(heads_axis, tok_count, gated.shape[1])
     stacked = lax.all_to_all(stacked, "tp", split_axis=0, concat_axis=0, tiled=True)
-    rows = like((tok_count, width))
-    middle, normed, sent_near = call(
-        project_kernel,
-        (rows, rows, packed),
-        stacked,
-        mixer_output_weight,
-        residual,
-        expert_norm_gain.reshape(1, width),
-        held_near,
+    held_near, weights_near, held_far, weights_far = tables(
+        jnp.stack([first_expert, far_place]), routes_t, scores_t, arrived, slots, cap
+    )
+    stacked_far = lax.ppermute(stacked, "sp", swap)
+    gain = expert_norm_gain.reshape(1, width)
+    sent_near, middle, normed = project(
+        stacked, mixer_output_weight, residual, gain, held_near, True
     )
     arrived_near = spread(sent_near)
-    normed_far = lax.ppermute(normed, "sp", swap)
     base = ffn(
         normed[None],
         common_gate_weight[None],
@@ -407,15 +480,16 @@
         tok_count,
         add=middle,
     )[0]
-    sent_far = call(pack_kernel, packed, held_far, normed_far)
+    (sent_far,) = project(stacked_far, mixer_output_weight, residual_far, gain, held_far, False)
     arrived_far = spread(sent_far)
     done_near = experts(arrived_near)
     done_far = experts(arrived_far)
     back_far = spread(done_far)
     back_near = spread(done_near)
-    far = call(far_kernel, rows, weights_far, back_far)
+    rows = like((tok_count, width))
+    far = by_columns(far_kernel, rows, weights_far, back_far)
     from_far = lax.ppermute(far, "sp", swap)
-    return call(final_kernel, rows, weights_near, back_near, base, from_far)
+    return by_columns(final_kernel, rows, weights_near, back_near, base, from_far)
 
 
 def solution(mesh):

time: 221 us -> 225 us (1.018)
  blocking collectives: 31.8 us -> 8.56 us
  waiting for transfers between devices: 108 us -> 121 us
  local copies, waits for them, and re-layouts: 6.98 us -> 16.1 us
  starting transfers between devices: 26.6 us -> 29.1 us
    all_to_all x1, blocking collectives: 31.8 us -> 8.56 us  [on_device(): lax.all_to_all(stacked, 'tp', split_axis=0, concat_axis=0, tiled=True)]
    all_to_all x3 -> x4, waiting for transfers between devices: 68.4 us -> 91.5 us  [spread(): lax.all_to_all(rows.reshape(half, exp_dev * cap, width), axes, split_axis...]
    ppermute x2, waiting for transfers between devices: 30.5 us -> 10.5 us  [the longest x1 10.5 us: on_device(): stacked_far = lax.ppermute(stacked, 'sp', swap)]
    all_to_all x2 -> x1, waiting for transfers between devices: 9.61 us -> 19.3 us  [on_device(): lax.all_to_all(message, 'sp', split_axis=0, concat_axis=0, tiled=True)]
    unnamed x26 -> x46, local copies, waits for them, and re-layouts: 6.87 us -> 16.1 us
    all_to_all x3 -> x4, starting transfers between devices: 13.3 us -> 18.1 us  [spread(): lax.all_to_all(rows.reshape(half, exp_dev * cap, width), axes, split_axis...]
    all_to_all x2 -> x1, starting transfers between devices: 10.7 us -> 7.31 us  [on_device(): lax.all_to_all(message, 'sp', split_axis=0, concat_axis=0, tiled=True)]
  transfers between devices with their start and end apart: 8 -> 8, of which waited for: 6 -> 6; matrix products, arithmetic and copies ran while one was open for 0% -> 0% of each run, Pallas kernels for 12% -> 15%
where the time goes in v3:
time: 225 us; the launch traced here: 223 us
  waiting for transfers between devices  121 us (54%)
  Pallas kernels  47.5 us (21%)
  starting transfers between devices  29.1 us (13%)
  local copies, waits for them, and re-layouts  16.1 us (7%)
  blocking collectives  8.56 us (4%)
    all_to_all x4, waiting for transfers between devices, spread(): lax.all_to_all(rows.reshape(half, exp_dev * cap, width), axes, split_axis...  91.5 us
    pallas_call x3, Pallas kernels, ffn(): pl.pallas_call(ffn_kernel, grid=(count, steps), in_specs=in_specs, out_sp...  21.3 us
    all_to_all x1, waiting for transfers between devices, on_device(): lax.all_to_all(message, 'sp', split_axis=0, concat_axis=0, tiled=True)  19.3 us
    all_to_all x4, starting transfers between devices, spread(): lax.all_to_all(rows.reshape(half, exp_dev * cap, width), axes, split_axis...  18.1 us
    unnamed x46, local copies, waits for them, and re-layouts  16.1 us
    pallas_call x2, Pallas kernels, project(): pl.pallas_call(project_kernel, grid=(count,), in_specs=[pl.BlockSpec((1,...  10.7 us
    ppermute x1, waiting for transfers between devices, on_device(): stacked_far = lax.ppermute(stacked, 'sp', swap)  10.5 us
    pallas_call x2, Pallas kernels, by_columns(): pl.pallas_call(kernel, grid=(steps,), in_specs=[pl.BlockSpec(weights.shap...  8.78 us
  transfers between devices with their start and end apart: 8, of which 6 were waited for; matrix products, arithmetic and copies ran while one was open for 0% of the time, Pallas kernels for 15%

profile of v3, /device:TPU:0, one launch (start us, length us, event | category | flops | bytes accessed | tf_op | source)
XLA Modules:
  0.0 223.5 jit_solution(13750025346626547603)
XLA Ops:
  0.0 0.9 copy-done.5
  1.0 0.9 copy-done.10
  1.9 0.9 copy-done.15
  4.8 3.1 %shard_map.172 = (f32[512,128]{1,0:T(8,128)S(1)}, f32[8,128,128]{2,1,0:T(8,128)S(1)}, bf16[8,144,128]{2,1,0:T(8,128)(2,1)}) custom-call(bf16[512,128]{1,0:T(8,128)(2,1)S(1)} %copy-done.10, bf16[512,256]{1,0:T(8,128)(2,1)S(1)} %copy-done.5, bf16[512,128]{1,0:T(8,128)(2,1)S(1)} %copy-done.15, f32[2,512]{1,0:T(2,128)S(1)} %bitcast.29, s32[4,128]{1,0:T(4,128)S(1)} %bitcast.26, ...), custom_call_target="tpu_custom_call" | custom-call | tf_op jit(solution)/shard_map/pallas_call | solution.py:149
  8.0 7.3 %all-to-all-start = ((bf16[8,144,128]{2,1,0:T(8,128)(2,1)}), bf16[8,144,128]{2,1,0:T(8,128)(2,1)S(1)}, u32[]{:S(2)}, u32[]{:S(2)}) async-start(bf16[8,144,128]{2,1,0:T(8,128)(2,1)} %get-tuple-element.15), calls=%async_computation | async-start | bytes 589824 | tf_op jit(solution)/shard_map/all_to_all | solution.py:448
  15.3 2.9 %collective-permute-start.1 = (bf16[128,2048]{1,0:T(8,128)(2,1)}, bf16[128,2048]{1,0:T(8,128)(2,1)S(1)}, u32[]{:S(2)}, u32[]{:S(2)}) collective-permute-start(bf16[128,2048]{1,0:T(8,128)(2,1)} %res_ref.1), channel_id=1, source_target_pairs={{0,16},{4,20},{8,24},{12,28},{16,0},{20,4},{24,8},{28,12},{1,17},{... | collective-permute-start | bytes 1572872 | tf_op jit(solution)/shard_map/ppermute | solution.py:449
  18.2 19.3 %all-to-all-done.far_ref.msg_ref = bf16[8,144,128]{2,1,0:T(8,128)(2,1)S(1)} async-done(((bf16[8,144,128]{2,1,0:T(8,128)(2,1)}), bf16[8,144,128]{2,1,0:T(8,128)(2,1)S(1)}, u32[]{:S(2)}, u32[]{:S(2)}) %all-to-all-start) | async-done | bytes 294944 | tf_op jit(solution)/shard_map/all_to_all | solution.py:448
  37.5 1.1 copy-done.6
  39.5 0.9 copy-done.12
  42.9 8.6 %all_to_all.30.g_ref = bf16[4,128,256]{2,1,0:T(8,128)(2,1)S(1)} all-to-all(bf16[4,128,256]{2,1,0:T(8,128)(2,1)S(1)} %bitcast.21), channel_id=1, replica_groups=mesh['sp'=8,'tp'=4] {'tp'}, dimensions={0} | all-to-all | bytes 524288 | tf_op jit(solution)/shard_map/all_to_all | solution.py:465
  52.1 2.7 %tables.1 = (bf16[512,128]{1,0:T(8,128)(2,1)}, bf16[2,128,512]{2,1,0:T(8,128)(2,1)}, bf16[512,128]{1,0:T(8,128)(2,1)}, bf16[2,128,512]{2,1,0:T(8,128)(2,1)}) custom-call(s32[2]{0:T(128)} %pad_add_fusion.place_ref, s32[4,128]{1,0:T(4,128)} %bitcast.25, f32[4,128]{1,0:T(4,128)} %bitcast.27, bf16[8,144,128]{2,1,0:T(8,128)(2,1)} %copy-done.2), custom_call_target="tpu_custom_call" | custom-call | tf_op jit(solution)/shard_map/tables/pallas_call | solution.py:266
  54.8 10.5 %collective-permute-done.g_ref = bf16[4,128,256]{2,1,0:T(8,128)(2,1)S(1)} collective-permute-done((bf16[4,128,256]{2,1,0:T(8,128)(2,1)S(1)}, bf16[4,128,256]{2,1,0:T(8,128)(2,1)S(1)}, u32[]{:S(2)}, u32[]{:S(2)}) %collective-permute-start) | collective-permute-done | bytes 262176 | tf_op jit(solution)/shard_map/ppermute | solution.py:469
  65.4 0.9 copy-done.13
  66.3 6.0 %shard_map.177 = bf16[512,2048]{1,0:T(8,128)(2,1)} custom-call(bf16[4,128,256]{2,1,0:T(8,128)(2,1)S(1)} %collective-permute-done.g_ref, bf16[1024,2048]{1,0:T(8,128)(2,1)} %w_ref.3, bf16[128,2048]{1,0:T(8,128)(2,1)S(1)} %collective-permute-done.1.res_ref, f32[1,2048]{1,0:T(1,128)S(1)} %bitcast.23, bf16[512,128]{1,0:T(8,128)(2,1)S(1)} %copy-done.13), custom_call_target="tpu_custom_call" | custom-call | tf_op jit(solution)/shard_map/pallas_call | solution.py:325
  72.2 3.8 %all-to-all-start.4 = ((bf16[16,32,2048]{2,1,0:T(8,128)(2,1)}), bf16[16,32,2048]{2,1,0:T(8,128)(2,1)S(1)}, u32[]{:S(2)}, u32[]{:S(2)}) async-start(bf16[16,32,2048]{2,1,0:T(8,128)(2,1)} %bitcast.16), calls=%async_computation.4 | async-start | bytes 4194304 | tf_op jit(solution)/shard_map/all_to_all | solution.py:412
  76.1 4.7 %shard_map.174 = (bf16[512,2048]{1,0:T(8,128)(2,1)S(1)}, bf16[128,2048]{1,0:T(8,128)(2,1)S(1)}, bf16[128,2048]{1,0:T(8,128)(2,1)S(1)}) custom-call(bf16[4,128,256]{2,1,0:T(8,128)(2,1)S(1)} %all_to_all.30.g_ref, bf16[1024,2048]{1,0:T(8,128)(2,1)} %w_ref.3, bf16[128,2048]{1,0:T(8,128)(2,1)S(1)} %copy-done.7, f32[1,2048]{1,0:T(1,128)S(1)} %bitcast.24, ...), custom_call_target="tpu_custom_call" | custom-call | tf_op jit(solution)/shard_map/pallas_call | solution.py:325
  80.9 1.4 copy-done.3
  83.0 22.1 %all-to-all-done.4.x_ref = bf16[16,32,2048]{2,1,0:T(8,128)(2,1)S(1)} async-done(((bf16[16,32,2048]{2,1,0:T(8,128)(2,1)}), bf16[16,32,2048]{2,1,0:T(8,128)(2,1)S(1)}, u32[]{:S(2)}, u32[]{:S(2)}) %all-to-all-start.4) | async-done | bytes 2097184 | tf_op jit(solution)/shard_map/all_to_all | solution.py:412
  105.1 4.5 %all-to-all-start.2 = ((bf16[16,32,2048]{2,1,0:T(8,128)(2,1)}), bf16[16,32,2048]{2,1,0:T(8,128)(2,1)}, u32[]{:S(2)}, u32[]{:S(2)}) async-start(bf16[16,32,2048]{2,1,0:T(8,128)(2,1)} %bitcast.19), calls=%async_computation.2 | async-start | bytes 4194304 | tf_op jit(solution)/shard_map/all_to_all | solution.py:412
  109.6 8.2 %shard_map.178 = bf16[16,32,2048]{2,1,0:T(8,128)(2,1)S(1)} custom-call(bf16[16,32,2048]{2,1,0:T(8,128)(2,1)S(1)} %all-to-all-done.4.x_ref, bf16[2,2048,512]{2,1,0:T(8,128)(2,1)} %gate_ref.5, bf16[2,2048,512]{2,1,0:T(8,128)(2,1)} %up_ref.3, bf16[2,512,2048]{2,1,0:T(8,128)(2,1)} %down_ref.3), custom_call_target="tpu_custom_call" | custom-call | flops 3221225472 | bytes 16777216 | tf_op jit(solution)/shard_map/pallas_call | solution.py:203
  117.8 1.4 copy-done
  119.2 19.5 %all-to-all-done.2.x_ref = bf16[16,32,2048]{2,1,0:T(8,128)(2,1)} async-done(((bf16[16,32,2048]{2,1,0:T(8,128)(2,1)}), bf16[16,32,2048]{2,1,0:T(8,128)(2,1)}, u32[]{:S(2)}, u32[]{:S(2)}) %all-to-all-start.2) | async-done | bytes 2097184 | tf_op jit(solution)/shard_map/all_to_all | solution.py:412
  138.7 4.9 %all-to-all-start.5 = ((bf16[16,32,2048]{2,1,0:T(8,128)(2,1)}), bf16[16,32,2048]{2,1,0:T(8,128)(2,1)S(1)}, u32[]{:S(2)}, u32[]{:S(2)}) async-start(bf16[16,32,2048]{2,1,0:T(8,128)(2,1)} %copy-done), calls=%async_computation.5 | async-start | bytes 4194304 | tf_op jit(solution)/shard_map/all_to_all | solution.py:412
  143.6 9.8 %shard_map.175 = bf16[16,32,2048]{2,1,0:T(8,128)(2,1)} custom-call(bf16[16,32,2048]{2,1,0:T(8,128)(2,1)} %all-to-all-done.2.x_ref, bf16[2,2048,512]{2,1,0:T(8,128)(2,1)} %gate_ref.5, bf16[2,2048,512]{2,1,0:T(8,128)(2,1)} %up_ref.3, bf16[2,512,2048]{2,1,0:T(8,128)(2,1)} %down_ref.3), custom_call_target="tpu_custom_call" | custom-call | flops 3221225472 | bytes 16777216 | tf_op jit(solution)/shard_map/pallas_call | solution.py:203
  153.4 19.3 %all-to-all-done.5 = bf16[16,32,2048]{2,1,0:T(8,128)(2,1)S(1)} async-done(((bf16[16,32,2048]{2,1,0:T(8,128)(2,1)}), bf16[16,32,2048]{2,1,0:T(8,128)(2,1)S(1)}, u32[]{:S(2)}, u32[]{:S(2)}) %all-to-all-start.5) | async-done | bytes 2097184 | tf_op jit(solution)/shard_map/all_to_all | solution.py:412
  172.7 1.4 copy-done.22
  174.0 5.0 %all-to-all-start.3 = ((bf16[16,32,2048]{2,1,0:T(8,128)(2,1)}), bf16[16,32,2048]{2,1,0:T(8,128)(2,1)}, u32[]{:S(2)}, u32[]{:S(2)}) async-start(bf16[16,32,2048]{2,1,0:T(8,128)(2,1)} %shard_map.175), calls=%async_computation.3 | async-start | bytes 4194304 | tf_op jit(solution)/shard_map/all_to_all | solution.py:412
  179.0 4.3 %shard_map.179 = bf16[128,2048]{1,0:T(8,128)(2,1)} custom-call(bf16[2,128,512]{2,1,0:T(8,128)(2,1)} %get-tuple-element.23.weight_ref, bf16[512,2048]{1,0:T(8,128)(2,1)} %bitcast.31), custom_call_target="tpu_custom_call" | custom-call | tf_op jit(solution)/shard_map/pallas_call | solution.py:365
  184.1 3.3 %shard_map.176 = f32[1,128,2048]{2,1,0:T(8,128)S(1)} custom-call(bf16[1,128,2048]{2,1,0:T(8,128)(2,1)S(1)} %bitcast.22, bf16[1,2048,512]{2,1,0:T(8,128)(2,1)S(1)} %bitcast.20, bf16[1,2048,512]{2,1,0:T(8,128)(2,1)} %bitcast.32, bf16[1,512,2048]{2,1,0:T(8,128)(2,1)} %bitcast.33, bf16[128,2048]{1,0:T(8,128)(2,1)S(1)} %get-tuple-element.22.rest_0_), custom_call_target="tpu_custom_call" | custom-call | flops 805306368 | bytes 7340032 | tf_op jit(solution)/shard_map/pallas_call | solution.py:203
  187.4 1.0 copy-done.1
  188.5 30.5 %all-to-all-done.3 = bf16[16,32,2048]{2,1,0:T(8,128)(2,1)} async-done(((bf16[16,32,2048]{2,1,0:T(8,128)(2,1)}), bf16[16,32,2048]{2,1,0:T(8,128)(2,1)}, u32[]{:S(2)}, u32[]{:S(2)}) %all-to-all-start.3) | async-done | bytes 2097184 | tf_op jit(solution)/shard_map/all_to_all | solution.py:412
  219.0 4.5 %shard_map.180 = bf16[128,2048]{1,0:T(8,128)(2,1)} custom-call(bf16[2,128,512]{2,1,0:T(8,128)(2,1)} %get-tuple-element.16.weight_ref, bf16[512,2048]{1,0:T(8,128)(2,1)} %bitcast.10.results_ref, f32[128,2048]{1,0:T(8,128)} %bitcast.18, bf16[128,2048]{1,0:T(8,128)(2,1)} %collective-permute-done.2.far_ref), custom_call_target="tpu_custom_call" | custom-call | tf_op jit(solution)/shard_map/pallas_call | solution.py:365
  (42 shorter events, 7.6 us)
Async XLA Ops:
  0.0 0.9 copy-start.5
  1.0 0.9 copy-start.10
  1.9 0.9 copy-start.15
  2.8 0.7 copy-start.18
  3.4 0.7 copy-start.19
  4.1 0.7 copy-start.20
  4.8 60.5 %copy-start.17 = (f32[2048]{0:T(1024)S(1)}, f32[2048]{0:T(1024)}, u32[]{:S(2)}) copy-start(f32[2048]{0:T(1024)} %param.27) | copy-start | bytes 24580
  8.0 29.6 %all-to-all-start = ((bf16[8,144,128]{2,1,0:T(8,128)(2,1)}), bf16[8,144,128]{2,1,0:T(8,128)(2,1)S(1)}, u32[]{:S(2)}, u32[]{:S(2)}) async-start(bf16[8,144,128]{2,1,0:T(8,128)(2,1)} %get-tuple-element.15), calls=%async_computation | async-start | bytes 589824 | tf_op jit(solution)/shard_map/all_to_all | solution.py:448
  15.3 39.6 %collective-permute-start.1 = (bf16[128,2048]{1,0:T(8,128)(2,1)}, bf16[128,2048]{1,0:T(8,128)(2,1)S(1)}, u32[]{:S(2)}, u32[]{:S(2)}) collective-permute-start(bf16[128,2048]{1,0:T(8,128)(2,1)} %res_ref.1), channel_id=1, source_target_pairs={{0,16},{4,20},{8,24},{12,28},{16,0},{20,4},{24,8},{28,12},{1,17},{... | collective-permute-start | bytes 1572872 | tf_op jit(solution)/shard_map/ppermute | solution.py:449
  37.5 14.6 %copy-start.2 = (bf16[8,144,128]{2,1,0:T(8,128)(2,1)}, bf16[8,144,128]{2,1,0:T(8,128)(2,1)S(1)}, u32[]{:S(2)}) copy-start(bf16[8,144,128]{2,1,0:T(8,128)(2,1)S(1)} %all-to-all-done.far_ref.msg_ref) | copy-start | bytes 884740
  37.5 1.1 copy-start.6
  38.6 0.9 copy-start.11
  39.5 0.9 copy-start.12
  40.4 0.9 copy-start.16
  41.3 0.7 copy-start.21
  51.4 13.9 %collective-permute-start = (bf16[4,128,256]{2,1,0:T(8,128)(2,1)S(1)}, bf16[4,128,256]{2,1,0:T(8,128)(2,1)S(1)}, u32[]{:S(2)}, u32[]{:S(2)}) collective-permute-start(bf16[4,128,256]{2,1,0:T(8,128)(2,1)S(1)} %all_to_all.30.g_ref), channel_id=1, source_target_pairs={{0,16},{4,20},{8,24},{12,28},{16,0},{20,4},{24,8},{28,12},{1,17},{... | collective-permute-start | bytes 786440 | tf_op jit(solution)/shard_map/ppermute | solution.py:469
  65.4 0.9 copy-start.13
  72.2 3.9 %copy-start.7 = (bf16[128,2048]{1,0:T(8,128)(2,1)S(1)}, bf16[128,2048]{1,0:T(8,128)(2,1)}, u32[]{:S(2)}) copy-start(bf16[128,2048]{1,0:T(8,128)(2,1)} %res_ref.1) | copy-start | bytes 1572868
  72.2 3.9 %copy-start.14 = (bf16[512,128]{1,0:T(8,128)(2,1)S(1)}, bf16[512,128]{1,0:T(8,128)(2,1)}, u32[]{:S(2)}) copy-start(bf16[512,128]{1,0:T(8,128)(2,1)} %get-tuple-element.19.held_ref) | copy-start | bytes 393220
  72.2 32.9 %all-to-all-start.4 = ((bf16[16,32,2048]{2,1,0:T(8,128)(2,1)}), bf16[16,32,2048]{2,1,0:T(8,128)(2,1)S(1)}, u32[]{:S(2)}, u32[]{:S(2)}) async-start(bf16[16,32,2048]{2,1,0:T(8,128)(2,1)} %bitcast.16), calls=%async_computation.4 | async-start | bytes 4194304 | tf_op jit(solution)/shard_map/all_to_all | solution.py:412
  80.8 1.4 copy-start.3
  82.2 0.8 copy-start.8
  105.1 33.6 %all-to-all-start.2 = ((bf16[16,32,2048]{2,1,0:T(8,128)(2,1)}), bf16[16,32,2048]{2,1,0:T(8,128)(2,1)}, u32[]{:S(2)}, u32[]{:S(2)}) async-start(bf16[16,32,2048]{2,1,0:T(8,128)(2,1)} %bitcast.19), calls=%async_computation.2 | async-start | bytes 4194304 | tf_op jit(solution)/shard_map/all_to_all | solution.py:412
  117.8 1.4 copy-start
  138.7 33.9 %all-to-all-start.5 = ((bf16[16,32,2048]{2,1,0:T(8,128)(2,1)}), bf16[16,32,2048]{2,1,0:T(8,128)(2,1)S(1)}, u32[]{:S(2)}, u32[]{:S(2)}) async-start(bf16[16,32,2048]{2,1,0:T(8,128)(2,1)} %copy-done), calls=%async_computation.5 | async-start | bytes 4194304 | tf_op jit(solution)/shard_map/all_to_all | solution.py:412
  172.7 1.4 copy-start.22
  174.0 44.9 %all-to-all-start.3 = ((bf16[16,32,2048]{2,1,0:T(8,128)(2,1)}), bf16[16,32,2048]{2,1,0:T(8,128)(2,1)}, u32[]{:S(2)}, u32[]{:S(2)}) async-start(bf16[16,32,2048]{2,1,0:T(8,128)(2,1)} %shard_map.175), calls=%async_computation.3 | async-start | bytes 4194304 | tf_op jit(solution)/shard_map/all_to_all | solution.py:412
  179.0 5.1 %copy-start.4 = (bf16[2048,512]{1,0:T(8,128)(2,1)S(1)}, bf16[2048,512]{1,0:T(8,128)(2,1)}, u32[]{:S(2)}) copy-start(bf16[2048,512]{1,0:T(8,128)(2,1)} %param.33) | copy-start | bytes 6291460
  179.0 5.1 %copy-start.9 = (bf16[128,2048]{1,0:T(8,128)(2,1)S(1)}, bf16[128,2048]{1,0:T(8,128)(2,1)}, u32[]{:S(2)}) copy-start(bf16[128,2048]{1,0:T(8,128)(2,1)} %copy-done.8) | copy-start | bytes 1572868
  183.3 35.7 %collective-permute-start.2 = (bf16[128,2048]{1,0:T(8,128)(2,1)}, bf16[128,2048]{1,0:T(8,128)(2,1)}, u32[]{:S(2)}, u32[]{:S(2)}) collective-permute-start(bf16[128,2048]{1,0:T(8,128)(2,1)} %shard_map.179), channel_id=1, source_target_pairs={{0,16},{4,20},{8,24},{12,28},{16,0},{20,4},{24,8},{28,12},{1,17},{... | collective-permute-start | bytes 1572872 | tf_op jit(solution)/shard_map/ppermute | solution.py:491
  187.4 1.0 copy-start.1

commit v4 on v3

--- a/solution.py
+++ b/solution.py
@@ -11,6 +11,7 @@
 BLOCK = 64
 TOP_K = 4
 MSG_PAD = 16
+ROOM = 40 << 20
 
 eps_norm = 1e-06
 decay_running = 16.0
@@ -139,20 +140,20 @@
         before = before + within[BLOCK - 1 : BLOCK]
 
 
-def call(kernel, out, *args, scalars=0):
-    def whole(x):
-        return pl.BlockSpec(x.shape, lambda i, rank=len(x.shape): (0,) * rank)
-
+def whole(x, loose=False):
+    return pl.BlockSpec(
+        x.shape,
+        lambda *_, rank=len(x.shape): (0,) * rank,
+        memory_space=None if loose else pltpu.VMEM,
+    )
+
+
+def call(kernel, out, *args, scalars=0, loose=()):
     in_specs = [pl.BlockSpec(memory_space=pltpu.SMEM)] * scalars + [
-        whole(x) for x in args[scalars:]
+        whole(x, i in loose) for i, x in enumerate(args[scalars:])
     ]
     return pl.pallas_call(
-        kernel,
-        grid=(1,),
-        in_specs=in_specs,
-        out_specs=jax.tree.map(whole, out),
-        out_shape=out,
-        compiler_params=pltpu.CompilerParams(vmem_limit_bytes=48 << 20),
+        kernel, grid=(1,), in_specs=in_specs, out_specs=jax.tree.map(whole, out), out_shape=out
     )(*args)
 
 
@@ -187,17 +188,19 @@
     count, _, hidden = gate_weight.shape
     steps = 2 if hidden % 256 == 0 else 1
     piece = hidden // steps
-    row_spec = pl.BlockSpec((sources, cap, width), lambda e, f: (0, e, 0))
+    row_spec = pl.BlockSpec(
+        (sources, cap, width), lambda e, f: (0, e, 0), memory_space=pltpu.VMEM
+    )
     in_specs = [
-        row_spec,
-        pl.BlockSpec((1, width, piece), lambda e, f: (e, 0, f)),
-        pl.BlockSpec((1, width, piece), lambda e, f: (e, 0, f)),
-        pl.BlockSpec((1, piece, width), lambda e, f: (e, f, 0)),
+        pl.BlockSpec((sources, cap, width), lambda e, f: (0, e, 0)),
+        pl.BlockSpec((1, width, piece), lambda e, f: (e, 0, f), memory_space=pltpu.VMEM),
+        pl.BlockSpec((1, width, piece), lambda e, f: (e, 0, f), memory_space=pltpu.VMEM),
+        pl.BlockSpec((1, piece, width), lambda e, f: (e, f, 0), memory_space=pltpu.VMEM),
     ]
     args = [rows, gate_weight, up_weight, down_weight]
     dtype = jnp.bfloat16
     if add is not None:
-        in_specs.append(pl.BlockSpec((sources * cap, width), lambda e, f: (0, 0)))
+        in_specs.append(whole(add))
         args.append(add)
         dtype = jnp.float32
     return pl.pallas_call(
@@ -207,7 +210,7 @@
         out_specs=row_spec,
         out_shape=jax.ShapeDtypeStruct(rows.shape, dtype),
         scratch_shapes=[pltpu.VMEM((sources * cap, width), jnp.float32)],
-        compiler_params=pltpu.CompilerParams(vmem_limit_bytes=48 << 20),
+        compiler_params=pltpu.CompilerParams(vmem_limit_bytes=None if add is not None else ROOM),
         cost_estimate=pl.CostEstimate(
             flops=6 * rows.shape[0] * rows.shape[1] * width * hidden,
             transcendentals=rows.shape[0] * rows.shape[1] * hidden,
@@ -238,8 +241,8 @@
     held = (named > 0) & (rank == lax.rem(slot, jnp.int32(cap)).astype(jnp.float32))
     held_ref[...] = jnp.where(held, 1.0, 0.0).astype(jnp.bfloat16)
     high, low = two_pieces(jnp.where(held, weight, 0.0).T)
-    weight_ref[0] = high.astype(jnp.bfloat16)
-    weight_ref[1] = low.astype(jnp.bfloat16)
+    weight_ref[:tokens] = high.astype(jnp.bfloat16)
+    weight_ref[tokens:] = low.astype(jnp.bfloat16)
 
 
 def tables_kernel(
@@ -257,10 +260,7 @@
     tokens = routes.shape[1]
     vdim = arrived.shape[1] - MSG_PAD
     held = jax.ShapeDtypeStruct((slots, tokens), jnp.bfloat16)
-    weights = jax.ShapeDtypeStruct((2, tokens, slots), jnp.bfloat16)
-
-    def whole(x):
-        return pl.BlockSpec(x.shape, lambda i, p, rank=len(x.shape): (0,) * rank)
+    weights = jax.ShapeDtypeStruct((2 * tokens, slots), jnp.bfloat16)
 
     out = (held, weights, held, weights)
     return pl.pallas_call(
@@ -319,56 +319,59 @@
     if keep_rows:
         out += [jax.ShapeDtypeStruct((tokens, width), jnp.bfloat16)] * 2
 
-    def whole(x):
-        return pl.BlockSpec(x.shape, lambda t, rank=len(x.shape): (0,) * rank)
-
     return pl.pallas_call(
         project_kernel,
         grid=(count,),
         in_specs=[
             pl.BlockSpec((1, tokens, cols), lambda t: (t, 0, 0)),
-            pl.BlockSpec((cols, width), lambda t: (t, 0)),
-            whole(residual),
+            pl.BlockSpec((cols, width), lambda t: (t, 0), memory_space=pltpu.VMEM),
+            whole(residual, not keep_rows),
             whole(gain),
             whole(held),
         ],
         out_specs=[whole(x) for x in out],
         out_shape=out,
         scratch_shapes=[pltpu.VMEM((tokens, width), jnp.float32)],
-        compiler_params=pltpu.CompilerParams(vmem_limit_bytes=48 << 20),
     )(stacked, weight, residual, gain, held)
 
 
-def weighed(weight_ref, results_ref):
-    return jnp.dot(weight_ref[0], results_ref[...], preferred_element_type=jnp.float32) + jnp.dot(
-        weight_ref[1], results_ref[...], preferred_element_type=jnp.float32
-    )
-
-
-def far_kernel(weight_ref, results_ref, out_ref):
-    out_ref[...] = weighed(weight_ref, results_ref).astype(jnp.bfloat16)
-
-
-def final_kernel(weight_ref, results_ref, base_ref, far_ref, out_ref):
-    out_ref[...] = (
-        base_ref[...] + weighed(weight_ref, results_ref) + far_ref[...].astype(jnp.float32)
-    ).astype(jnp.bfloat16)
-
-
-def by_columns(kernel, out, weights, *args):
-    steps = 4 if out.shape[1] % 512 == 0 else 1
-    piece = out.shape[1] // steps
-
-    def part(x):
-        return pl.BlockSpec((x.shape[0], piece), lambda c: (0, c))
-
+def weigh_kernel(weight_ref, results_ref, *rest):
+    out_ref, acc_ref = rest[-2:]
+    step = pl.program_id(0)
+    tokens = out_ref.shape[0]
+    both = jnp.dot(weight_ref[...], results_ref[...], preferred_element_type=jnp.float32)
+    part = both[:tokens] + both[tokens:]
+
+    @pl.when(step == 0)
+    def _():
+        acc_ref[...] = part
+
+    @pl.when(step == pl.num_programs(0) - 1)
+    def _():
+        total = acc_ref[...] + part
+        if len(rest) == 4:
+            total = total + rest[0][...] + rest[1][...].astype(jnp.float32)
+        out_ref[...] = total.astype(jnp.bfloat16)
+
+
+def weigh(out, weights, results, *more):
+    slots, width = results.shape
+    piece = slots // 2
+    in_specs = [
+        pl.BlockSpec((weights.shape[0], piece), lambda k: (0, k), memory_space=pltpu.VMEM),
+        pl.BlockSpec((piece, width), lambda k: (k, 0)),
+    ]
+    if more:
+        in_specs += [whole(more[0]), whole(more[1], True)]
     return pl.pallas_call(
-        kernel,
-        grid=(steps,),
-        in_specs=[pl.BlockSpec(weights.shape, lambda c: (0, 0, 0))] + [part(x) for x in args],
-        out_specs=part(out),
+        weigh_kernel,
+        grid=(2,),
+        in_specs=in_specs,
+        out_specs=whole(out),
         out_shape=out,
-    )(weights, *args)
+        scratch_shapes=[pltpu.VMEM(out.shape, jnp.float32)],
+        compiler_params=pltpu.CompilerParams(vmem_limit_bytes=ROOM if more else None),
+    )(weights, results, *more)
 
 
 def on_device(
@@ -460,6 +463,7 @@
         output_gate_input,
         head_norm_gain.reshape(1, vdim),
         scalars=1,
+        loose=(5,),
     )
     stacked = gated.reshape(heads_axis, tok_count, gated.shape[1])
     stacked = lax.all_to_all(stacked, "tp", split_axis=0, concat_axis=0, tiled=True)
@@ -487,9 +491,9 @@
     back_far = spread(done_far)
     back_near = spread(done_near)
     rows = like((tok_count, width))
-    far = by_columns(far_kernel, rows, weights_far, back_far)
+    far = weigh(rows, weights_far, back_far)
     from_far = lax.ppermute(far, "sp", swap)
-    return by_columns(final_kernel, rows, weights_near, back_near, base, from_far)
+    return weigh(rows, weights_near, back_near, base, from_far)
 
 
 def solution(mesh):

time: 225 us -> 219 us (0.973)
  waiting for transfers between devices: 121 us -> 115 us
    all_to_all x4, waiting for transfers between devices: 91.5 us -> 85.4 us  [spread(): lax.all_to_all(rows.reshape(half, exp_dev * cap, width), axes, split_axis...]
    pallas_call x2, Pallas kernels: 8.78 us -> 5.09 us  [weigh(): pl.pallas_call(weigh_kernel, grid=(2,), in_specs=in_specs, out_specs=whol...]
    pallas_call x2, Pallas kernels: 4.01 us -> 7.32 us  [call(): pl.pallas_call(kernel, grid=(1,), in_specs=in_specs, out_specs=jax.tree.m...]
    unnamed x46 -> x26, local copies, waits for them, and re-layouts: 16.1 us -> 15.4 us
  transfers between devices with their start and end apart: 8 -> 8, of which waited for: 6 -> 6; matrix products, arithmetic and copies ran while one was open for 0% -> 0% of each run, Pallas kernels for 15% -> 16%
where the time goes in v4:
time: 219 us; the launch traced here: 217 us
  waiting for transfers between devices  115 us (53%)
  Pallas kernels  47.8 us (22%)
  starting transfers between devices  29 us (13%)
  local copies, waits for them, and re-layouts  15.4 us (7%)
  blocking collectives  9.38 us (4%)
    all_to_all x4, waiting for transfers between devices, spread(): lax.all_to_all(rows.reshape(half, exp_dev * cap, width), axes, split_axis...  85.4 us
    pallas_call x3, Pallas kernels, ffn(): pl.pallas_call(ffn_kernel, grid=(count, steps), in_specs=in_specs, out_sp...  19.7 us
    all_to_all x1, waiting for transfers between devices, on_device(): lax.all_to_all(message, 'sp', split_axis=0, concat_axis=0, tiled=True)  19.3 us
    all_to_all x4, starting transfers between devices, spread(): lax.all_to_all(rows.reshape(half, exp_dev * cap, width), axes, split_axis...  18 us
    unnamed x26, local copies, waits for them, and re-layouts  15.4 us
    pallas_call x2, Pallas kernels, project(): pl.pallas_call(project_kernel, grid=(count,), in_specs=[pl.BlockSpec((1,...  12.9 us
    ppermute x1, waiting for transfers between devices, on_device(): stacked_far = lax.ppermute(stacked, 'sp', swap)  10.6 us
    all_to_all x1, blocking collectives, on_device(): lax.all_to_all(stacked, 'tp', split_axis=0, concat_axis=0, tiled=True)  9.38 us
  transfers between devices with their start and end apart: 8, of which 6 were waited for; matrix products, arithmetic and copies ran while one was open for 0% of the time, Pallas kernels for 16%

profile of v4, /device:TPU:0, one launch (start us, length us, event | category | flops | bytes accessed | tf_op | source)
XLA Modules:
  0.0 217.5 jit_solution(15327249788059890433)
XLA Ops:
  0.0 4.3 %shard_map.172 = (f32[512,128]{1,0:T(8,128)}, f32[8,128,128]{2,1,0:T(8,128)}, bf16[8,144,128]{2,1,0:T(8,128)(2,1)}) custom-call(bf16[512,128]{1,0:T(8,128)(2,1)} %k_ref.3, bf16[512,256]{1,0:T(8,128)(2,1)} %v_ref.3, bf16[512,128]{1,0:T(8,128)(2,1)} %c_ref.1, f32[2,512]{1,0:T(2,128)} %bitcast.34, s32[4,128]{1,0:T(4,128)} %bitcast.30, f32[4,128]{1,0:T(4,128)} %bitcast.32), custom_call_target="tpu_custom_call" | custom-call | tf_op jit(solution)/shard_map/pallas_call | solution.py:155
  4.3 7.3 %all-to-all-start = ((bf16[8,144,128]{2,1,0:T(8,128)(2,1)}), bf16[8,144,128]{2,1,0:T(8,128)(2,1)S(1)}, u32[]{:S(2)}, u32[]{:S(2)}) async-start(bf16[8,144,128]{2,1,0:T(8,128)(2,1)} %get-tuple-element.15), calls=%async_computation | async-start | bytes 589824 | tf_op jit(solution)/shard_map/all_to_all | solution.py:451
  11.6 2.9 %collective-permute-start.1 = (bf16[128,2048]{1,0:T(8,128)(2,1)}, bf16[128,2048]{1,0:T(8,128)(2,1)S(1)}, u32[]{:S(2)}, u32[]{:S(2)}) collective-permute-start(bf16[128,2048]{1,0:T(8,128)(2,1)} %res_ref.1), channel_id=1, source_target_pairs={{0,16},{4,20},{8,24},{12,28},{16,0},{20,4},{24,8},{28,12},{1,17},{... | collective-permute-start | bytes 1572872 | tf_op jit(solution)/shard_map/ppermute | solution.py:452
  14.5 19.3 %all-to-all-done.far_ref.msg_ref = bf16[8,144,128]{2,1,0:T(8,128)(2,1)S(1)} async-done(((bf16[8,144,128]{2,1,0:T(8,128)(2,1)}), bf16[8,144,128]{2,1,0:T(8,128)(2,1)S(1)}, u32[]{:S(2)}, u32[]{:S(2)}) %all-to-all-start) | async-done | bytes 294944 | tf_op jit(solution)/shard_map/all_to_all | solution.py:451
  33.8 0.7 copy-done.9
  34.5 3.1 %shard_map.173 = bf16[512,256]{1,0:T(8,128)(2,1)} custom-call(s32[1]{0:T(128)} %bitcast.5.place_ref, bf16[512,128]{1,0:T(8,128)(2,1)} %q_ref.1, bf16[512,128]{1,0:T(8,128)(2,1)} %k_ref.3, bf16[512,256]{1,0:T(8,128)(2,1)} %v_ref.3, f32[512,128]{1,0:T(8,128)} %get-tuple-element.17.within_ref, f32[8,128,128]{2,1,0:T(8,128)} %get-tuple-element.18.starts_ref, ...), custom_call_target="tpu_custom_call" | custom-call | tf_op jit(solution)/shard_map/pallas_call | solution.py:155
  37.6 9.4 %all_to_all.30.g_ref = bf16[4,128,256]{2,1,0:T(8,128)(2,1)S(1)} all-to-all(bf16[4,128,256]{2,1,0:T(8,128)(2,1)} %bitcast.26), channel_id=1, replica_groups=mesh['sp'=8,'tp'=4] {'tp'}, dimensions={0} | all-to-all | bytes 524288 | tf_op jit(solution)/shard_map/all_to_all | solution.py:469
  47.6 2.7 %tables.1 = (bf16[512,128]{1,0:T(8,128)(2,1)}, bf16[256,512]{1,0:T(8,128)(2,1)}, bf16[512,128]{1,0:T(8,128)(2,1)}, bf16[256,512]{1,0:T(8,128)(2,1)}) custom-call(s32[2]{0:T(128)} %pad_add_fusion.place_ref, s32[4,128]{1,0:T(4,128)} %bitcast.31, f32[4,128]{1,0:T(4,128)} %bitcast.33, bf16[8,144,128]{2,1,0:T(8,128)(2,1)} %copy-done.9), custom_call_target="tpu_custom_call" | custom-call | tf_op jit(solution)/shard_map/tables/pallas_call | solution.py:266
  50.3 10.6 %collective-permute-done.g_ref = bf16[4,128,256]{2,1,0:T(8,128)(2,1)S(1)} collective-permute-done((bf16[4,128,256]{2,1,0:T(8,128)(2,1)S(1)}, bf16[4,128,256]{2,1,0:T(8,128)(2,1)S(1)}, u32[]{:S(2)}, u32[]{:S(2)}) %collective-permute-start) | collective-permute-done | bytes 262176 | tf_op jit(solution)/shard_map/ppermute | solution.py:473
  61.6 6.2 %shard_map.177 = bf16[512,2048]{1,0:T(8,128)(2,1)} custom-call(bf16[4,128,256]{2,1,0:T(8,128)(2,1)} %copy-done.12, bf16[1024,2048]{1,0:T(8,128)(2,1)} %w_ref.3, bf16[128,2048]{1,0:T(8,128)(2,1)} %copy-done.11, f32[1,2048]{1,0:T(1,128)} %bitcast.28, bf16[512,128]{1,0:T(8,128)(2,1)} %get-tuple-element.24.held_ref), custom_call_target="tpu_custom_call" | custom-call | tf_op jit(solution)/shard_map/pallas_call | solution.py:322
  67.9 3.7 %all-to-all-start.4 = ((bf16[16,32,2048]{2,1,0:T(8,128)(2,1)}), bf16[16,32,2048]{2,1,0:T(8,128)(2,1)S(1)}, u32[]{:S(2)}, u32[]{:S(2)}) async-start(bf16[16,32,2048]{2,1,0:T(8,128)(2,1)} %bitcast.21), calls=%async_computation.4 | async-start | bytes 4194304 | tf_op jit(solution)/shard_map/all_to_all | solution.py:415
  71.6 6.7 %shard_map.174 = (bf16[512,2048]{1,0:T(8,128)(2,1)}, bf16[128,2048]{1,0:T(8,128)(2,1)}, bf16[128,2048]{1,0:T(8,128)(2,1)}) custom-call(bf16[4,128,256]{2,1,0:T(8,128)(2,1)} %copy-done.10, bf16[1024,2048]{1,0:T(8,128)(2,1)} %w_ref.3, bf16[128,2048]{1,0:T(8,128)(2,1)} %res_ref.1, f32[1,2048]{1,0:T(1,128)} %bitcast.29, bf16[512,128]{1,0:T(8,128)(2,1)} %get-tuple-element.19.held_ref), custom_call_target="tpu_custom_call" | custom-call | tf_op jit(solution)/shard_map/pallas_call | solution.py:322
  78.3 22.4 %all-to-all-done.4.x_ref = bf16[16,32,2048]{2,1,0:T(8,128)(2,1)S(1)} async-done(((bf16[16,32,2048]{2,1,0:T(8,128)(2,1)}), bf16[16,32,2048]{2,1,0:T(8,128)(2,1)S(1)}, u32[]{:S(2)}, u32[]{:S(2)}) %all-to-all-start.4) | async-done | bytes 2097184 | tf_op jit(solution)/shard_map/all_to_all | solution.py:415
  100.6 4.5 %all-to-all-start.2 = ((bf16[16,32,2048]{2,1,0:T(8,128)(2,1)}), bf16[16,32,2048]{2,1,0:T(8,128)(2,1)}, u32[]{:S(2)}, u32[]{:S(2)}) async-start(bf16[16,32,2048]{2,1,0:T(8,128)(2,1)} %bitcast.22), calls=%async_computation.2 | async-start | bytes 4194304 | tf_op jit(solution)/shard_map/all_to_all | solution.py:415
  105.1 2.2 %copy-done = bf16[2,2048,512]{2,1,0:T(8,128)(2,1)S(1)} copy-done((bf16[2,2048,512]{2,1,0:T(8,128)(2,1)S(1)}, bf16[2,2048,512]{2,1,0:T(8,128)(2,1)}, u32[]{:S(2)}) %copy-start) | copy-done | bytes 4194328
  107.3 2.2 %copy-done.2 = bf16[2,2048,512]{2,1,0:T(8,128)(2,1)S(1)} copy-done((bf16[2,2048,512]{2,1,0:T(8,128)(2,1)S(1)}, bf16[2,2048,512]{2,1,0:T(8,128)(2,1)}, u32[]{:S(2)}) %copy-start.2) | copy-done | bytes 4194328
  109.5 7.2 %shard_map.178 = bf16[16,32,2048]{2,1,0:T(8,128)(2,1)S(1)} custom-call(bf16[16,32,2048]{2,1,0:T(8,128)(2,1)S(1)} %all-to-all-done.4.x_ref, bf16[2,2048,512]{2,1,0:T(8,128)(2,1)S(1)} %copy-done, bf16[2,2048,512]{2,1,0:T(8,128)(2,1)S(1)} %copy-done.2, bf16[2,512,2048]{2,1,0:T(8,128)(2,1)} %down_ref.3), custom_call_target="tpu_custom_call" | custom-call | flops 3221225472 | bytes 16777216 | tf_op jit(solution)/shard_map/pallas_call | solution.py:206
  116.7 1.3 copy-done.5
  118.0 16.1 %all-to-all-done.2.x_ref = bf16[16,32,2048]{2,1,0:T(8,128)(2,1)} async-done(((bf16[16,32,2048]{2,1,0:T(8,128)(2,1)}), bf16[16,32,2048]{2,1,0:T(8,128)(2,1)}, u32[]{:S(2)}, u32[]{:S(2)}) %all-to-all-start.2) | async-done | bytes 2097184 | tf_op jit(solution)/shard_map/all_to_all | solution.py:415
  134.2 4.9 %all-to-all-start.5 = ((bf16[16,32,2048]{2,1,0:T(8,128)(2,1)}), bf16[16,32,2048]{2,1,0:T(8,128)(2,1)S(1)}, u32[]{:S(2)}, u32[]{:S(2)}) async-start(bf16[16,32,2048]{2,1,0:T(8,128)(2,1)} %copy-done.5), calls=%async_computation.5 | async-start | bytes 4194304 | tf_op jit(solution)/shard_map/all_to_all | solution.py:415
  139.1 2.2 %copy-done.1 = bf16[2,2048,512]{2,1,0:T(8,128)(2,1)S(1)} copy-done((bf16[2,2048,512]{2,1,0:T(8,128)(2,1)S(1)}, bf16[2,2048,512]{2,1,0:T(8,128)(2,1)}, u32[]{:S(2)}) %copy-start.1) | copy-done | bytes 4194328
  141.3 2.2 %copy-done.3 = bf16[2,2048,512]{2,1,0:T(8,128)(2,1)S(1)} copy-done((bf16[2,2048,512]{2,1,0:T(8,128)(2,1)S(1)}, bf16[2,2048,512]{2,1,0:T(8,128)(2,1)}, u32[]{:S(2)}) %copy-start.3) | copy-done | bytes 4194328
  143.5 7.3 %shard_map.175 = bf16[16,32,2048]{2,1,0:T(8,128)(2,1)S(1)} custom-call(bf16[16,32,2048]{2,1,0:T(8,128)(2,1)} %all-to-all-done.2.x_ref, bf16[2,2048,512]{2,1,0:T(8,128)(2,1)S(1)} %copy-done.1, bf16[2,2048,512]{2,1,0:T(8,128)(2,1)S(1)} %copy-done.3, bf16[2,512,2048]{2,1,0:T(8,128)(2,1)} %down_ref.3), custom_call_target="tpu_custom_call" | custom-call | flops 3221225472 | bytes 16777216 | tf_op jit(solution)/shard_map/pallas_call | solution.py:206
  150.8 1.3 copy-done.4
  152.2 16.0 %all-to-all-done.5 = bf16[16,32,2048]{2,1,0:T(8,128)(2,1)S(1)} async-done(((bf16[16,32,2048]{2,1,0:T(8,128)(2,1)}), bf16[16,32,2048]{2,1,0:T(8,128)(2,1)S(1)}, u32[]{:S(2)}, u32[]{:S(2)}) %all-to-all-start.5) | async-done | bytes 2097184 | tf_op jit(solution)/shard_map/all_to_all | solution.py:415
  168.2 1.3 copy-done.8
  169.5 4.9 %all-to-all-start.3 = ((bf16[16,32,2048]{2,1,0:T(8,128)(2,1)}), bf16[16,32,2048]{2,1,0:T(8,128)(2,1)S(1)}, u32[]{:S(2)}, u32[]{:S(2)}) async-start(bf16[16,32,2048]{2,1,0:T(8,128)(2,1)} %copy-done.4), calls=%async_computation.3 | async-start | bytes 4194304 | tf_op jit(solution)/shard_map/all_to_all | solution.py:415
  174.4 3.2 %shard_map.179 = bf16[128,2048]{1,0:T(8,128)(2,1)} custom-call(bf16[256,512]{1,0:T(8,128)(2,1)} %get-tuple-element.23.weight_ref, bf16[512,2048]{1,0:T(8,128)(2,1)} %bitcast.20), custom_call_target="tpu_custom_call" | custom-call | tf_op jit(solution)/shard_map/pallas_call | solution.py:366
  178.3 5.2 %shard_map.176 = f32[1,128,2048]{2,1,0:T(8,128)} custom-call(bf16[1,128,2048]{2,1,0:T(8,128)(2,1)} %bitcast.27, bf16[1,2048,512]{2,1,0:T(8,128)(2,1)} %bitcast.23, bf16[1,2048,512]{2,1,0:T(8,128)(2,1)} %bitcast.24, bf16[1,512,2048]{2,1,0:T(8,128)(2,1)} %bitcast.25, bf16[128,2048]{1,0:T(8,128)(2,1)} %get-tuple-element.22.rest_0_), custom_call_target="tpu_custom_call" | custom-call | flops 805306368 | bytes 7340032 | tf_op jit(solution)/shard_map/pallas_call | solution.py:206
  183.5 30.9 %all-to-all-done.3 = bf16[16,32,2048]{2,1,0:T(8,128)(2,1)S(1)} async-done(((bf16[16,32,2048]{2,1,0:T(8,128)(2,1)}), bf16[16,32,2048]{2,1,0:T(8,128)(2,1)S(1)}, u32[]{:S(2)}, u32[]{:S(2)}) %all-to-all-start.3) | async-done | bytes 2097184 | tf_op jit(solution)/shard_map/all_to_all | solution.py:415
  214.3 1.2 copy-done.6
  215.6 1.9 shard_map.180
  (22 shorter events, 2.0 us)
Async XLA Ops:
  4.3 29.6 %all-to-all-start = ((bf16[8,144,128]{2,1,0:T(8,128)(2,1)}), bf16[8,144,128]{2,1,0:T(8,128)(2,1)S(1)}, u32[]{:S(2)}, u32[]{:S(2)}) async-start(bf16[8,144,128]{2,1,0:T(8,128)(2,1)} %get-tuple-element.15), calls=%async_computation | async-start | bytes 589824 | tf_op jit(solution)/shard_map/all_to_all | solution.py:451
  11.6 38.7 %collective-permute-start.1 = (bf16[128,2048]{1,0:T(8,128)(2,1)}, bf16[128,2048]{1,0:T(8,128)(2,1)S(1)}, u32[]{:S(2)}, u32[]{:S(2)}) collective-permute-start(bf16[128,2048]{1,0:T(8,128)(2,1)} %res_ref.1), channel_id=1, source_target_pairs={{0,16},{4,20},{8,24},{12,28},{16,0},{20,4},{24,8},{28,12},{1,17},{... | collective-permute-start | bytes 1572872 | tf_op jit(solution)/shard_map/ppermute | solution.py:452
  33.8 0.7 copy-start.9
  47.0 20.9 %copy-start.10 = (bf16[4,128,256]{2,1,0:T(8,128)(2,1)}, bf16[4,128,256]{2,1,0:T(8,128)(2,1)S(1)}, u32[]{:S(2)}) copy-start(bf16[4,128,256]{2,1,0:T(8,128)(2,1)S(1)} %all_to_all.30.g_ref) | copy-start | bytes 786436
  47.0 13.9 %collective-permute-start = (bf16[4,128,256]{2,1,0:T(8,128)(2,1)S(1)}, bf16[4,128,256]{2,1,0:T(8,128)(2,1)S(1)}, u32[]{:S(2)}, u32[]{:S(2)}) collective-permute-start(bf16[4,128,256]{2,1,0:T(8,128)(2,1)S(1)} %all_to_all.30.g_ref), channel_id=1, source_target_pairs={{0,16},{4,20},{8,24},{12,28},{16,0},{20,4},{24,8},{28,12},{1,17},{... | collective-permute-start | bytes 786440 | tf_op jit(solution)/shard_map/ppermute | solution.py:473
  50.3 10.6 %copy-start.11 = (bf16[128,2048]{1,0:T(8,128)(2,1)}, bf16[128,2048]{1,0:T(8,128)(2,1)S(1)}, u32[]{:S(2)}) copy-start(bf16[128,2048]{1,0:T(8,128)(2,1)S(1)} %collective-permute-done.1.res_ref) | copy-start | bytes 1572868
  60.9 0.7 copy-start.12
  67.9 32.8 %all-to-all-start.4 = ((bf16[16,32,2048]{2,1,0:T(8,128)(2,1)}), bf16[16,32,2048]{2,1,0:T(8,128)(2,1)S(1)}, u32[]{:S(2)}, u32[]{:S(2)}) async-start(bf16[16,32,2048]{2,1,0:T(8,128)(2,1)} %bitcast.21), calls=%async_computation.4 | async-start | bytes 4194304 | tf_op jit(solution)/shard_map/all_to_all | solution.py:415
  100.6 33.5 %all-to-all-start.2 = ((bf16[16,32,2048]{2,1,0:T(8,128)(2,1)}), bf16[16,32,2048]{2,1,0:T(8,128)(2,1)}, u32[]{:S(2)}, u32[]{:S(2)}) async-start(bf16[16,32,2048]{2,1,0:T(8,128)(2,1)} %bitcast.22), calls=%async_computation.2 | async-start | bytes 4194304 | tf_op jit(solution)/shard_map/all_to_all | solution.py:415
  105.1 2.2 %copy-start = (bf16[2,2048,512]{2,1,0:T(8,128)(2,1)S(1)}, bf16[2,2048,512]{2,1,0:T(8,128)(2,1)}, u32[]{:S(2)}) copy-start(bf16[2,2048,512]{2,1,0:T(8,128)(2,1)} %gate_ref.5) | copy-start | bytes 12582916
  107.3 2.2 %copy-start.2 = (bf16[2,2048,512]{2,1,0:T(8,128)(2,1)S(1)}, bf16[2,2048,512]{2,1,0:T(8,128)(2,1)}, u32[]{:S(2)}) copy-start(bf16[2,2048,512]{2,1,0:T(8,128)(2,1)} %up_ref.3) | copy-start | bytes 12582916
  116.7 1.3 copy-start.5
  134.2 34.0 %all-to-all-start.5 = ((bf16[16,32,2048]{2,1,0:T(8,128)(2,1)}), bf16[16,32,2048]{2,1,0:T(8,128)(2,1)S(1)}, u32[]{:S(2)}, u32[]{:S(2)}) async-start(bf16[16,32,2048]{2,1,0:T(8,128)(2,1)} %copy-done.5), calls=%async_computation.5 | async-start | bytes 4194304 | tf_op jit(solution)/shard_map/all_to_all | solution.py:415
  139.1 2.2 %copy-start.1 = (bf16[2,2048,512]{2,1,0:T(8,128)(2,1)S(1)}, bf16[2,2048,512]{2,1,0:T(8,128)(2,1)}, u32[]{:S(2)}) copy-start(bf16[2,2048,512]{2,1,0:T(8,128)(2,1)} %gate_ref.5) | copy-start | bytes 12582916
  141.3 2.2 %copy-start.3 = (bf16[2,2048,512]{2,1,0:T(8,128)(2,1)S(1)}, bf16[2,2048,512]{2,1,0:T(8,128)(2,1)}, u32[]{:S(2)}) copy-start(bf16[2,2048,512]{2,1,0:T(8,128)(2,1)} %up_ref.3) | copy-start | bytes 12582916
  150.8 1.3 copy-start.4
  168.2 1.3 copy-start.8
  169.5 44.8 %all-to-all-start.3 = ((bf16[16,32,2048]{2,1,0:T(8,128)(2,1)}), bf16[16,32,2048]{2,1,0:T(8,128)(2,1)S(1)}, u32[]{:S(2)}, u32[]{:S(2)}) async-start(bf16[16,32,2048]{2,1,0:T(8,128)(2,1)} %copy-done.4), calls=%async_computation.3 | async-start | bytes 4194304 | tf_op jit(solution)/shard_map/all_to_all | solution.py:415
  177.6 36.8 %collective-permute-start.2 = (bf16[128,2048]{1,0:T(8,128)(2,1)}, bf16[128,2048]{1,0:T(8,128)(2,1)S(1)}, u32[]{:S(2)}, u32[]{:S(2)}) collective-permute-start(bf16[128,2048]{1,0:T(8,128)(2,1)} %shard_map.179), channel_id=1, source_target_pairs={{0,16},{4,20},{8,24},{12,28},{16,0},{20,4},{24,8},{28,12},{1,17},{... | collective-permute-start | bytes 1572872 | tf_op jit(solution)/shard_map/ppermute | solution.py:495
  178.3 36.1 %copy-start.7 = (bf16[256,512]{1,0:T(8,128)(2,1)S(1)}, bf16[256,512]{1,0:T(8,128)(2,1)}, u32[]{:S(2)}) copy-start(bf16[256,512]{1,0:T(8,128)(2,1)} %get-tuple-element.16.weight_ref) | copy-start | bytes 786436
  214.3 1.2 copy-start.6

commit v5 on v4

--- a/solution.py
+++ b/solution.py
@@ -11,7 +11,7 @@
 BLOCK = 64
 TOP_K = 4
 MSG_PAD = 16
-ROOM = 40 << 20
+ROOM = 48 << 20
 
 eps_norm = 1e-06
 decay_running = 16.0
@@ -148,12 +148,17 @@
     )
 
 
-def call(kernel, out, *args, scalars=0, loose=()):
+def call(kernel, out, *args, scalars=0, loose=(), room=None):
     in_specs = [pl.BlockSpec(memory_space=pltpu.SMEM)] * scalars + [
         whole(x, i in loose) for i, x in enumerate(args[scalars:])
     ]
     return pl.pallas_call(
-        kernel, grid=(1,), in_specs=in_specs, out_specs=jax.tree.map(whole, out), out_shape=out
+        kernel,
+        grid=(1,),
+        in_specs=in_specs,
+        out_specs=jax.tree.map(whole, out),
+        out_shape=out,
+        compiler_params=pltpu.CompilerParams(vmem_limit_bytes=room),
     )(*args)
 
 
@@ -193,9 +198,9 @@
     )
     in_specs = [
         pl.BlockSpec((sources, cap, width), lambda e, f: (0, e, 0)),
-        pl.BlockSpec((1, width, piece), lambda e, f: (e, 0, f), memory_space=pltpu.VMEM),
-        pl.BlockSpec((1, width, piece), lambda e, f: (e, 0, f), memory_space=pltpu.VMEM),
-        pl.BlockSpec((1, piece, width), lambda e, f: (e, f, 0), memory_space=pltpu.VMEM),
+        pl.BlockSpec((1, width, piece), lambda e, f: (e, 0, f)),
+        pl.BlockSpec((1, width, piece), lambda e, f: (e, 0, f)),
+        pl.BlockSpec((1, piece, width), lambda e, f: (e, f, 0)),
     ]
     args = [rows, gate_weight, up_weight, down_weight]
     dtype = jnp.bfloat16
@@ -286,8 +291,13 @@
     return jnp.dot(held, rows, preferred_element_type=jnp.float32).astype(jnp.bfloat16)
 
 
-def project_kernel(g_ref, w_ref, res_ref, gain_ref, held_ref, sent_ref, *rest):
-    acc_ref = rest[-1]
+def pack_kernel(held_ref, rows_ref, sent_ref):
+    sent_ref[...] = pick(held_ref[...], rows_ref[...])
+
+
+def project_kernel(
+    g_ref, w_ref, res_ref, gain_ref, held_ref, sent_ref, mid_ref, norm_ref, acc_ref
+):
     step = pl.program_id(0)
     part = jnp.dot(g_ref[0], w_ref[...], preferred_element_type=jnp.float32)
 
@@ -306,18 +316,16 @@
         scale = lax.rsqrt(jnp.mean(wide * wide, axis=-1, keepdims=True) + eps_norm)
         normed = (wide * scale * gain_ref[...]).astype(jnp.bfloat16)
         sent_ref[...] = pick(held_ref[...], normed)
-        if len(rest) == 3:
-            rest[0][...] = middle
-            rest[1][...] = normed
-
-
-def project(stacked, weight, residual, gain, held, keep_rows):
+        mid_ref[...] = middle
+        norm_ref[...] = normed
+
+
+def project(stacked, weight, residual, gain, held):
     count, tokens, cols = stacked.shape
     width = residual.shape[1]
     slots = held.shape[0]
-    out = [jax.ShapeDtypeStruct((slots, width), jnp.bfloat16)]
-    if keep_rows:
-        out += [jax.ShapeDtypeStruct((tokens, width), jnp.bfloat16)] * 2
+    rows = jax.ShapeDtypeStruct((tokens, width), jnp.bfloat16)
+    out = [jax.ShapeDtypeStruct((slots, width), jnp.bfloat16), rows, rows]
 
     return pl.pallas_call(
         project_kernel,
@@ -325,13 +333,14 @@
         in_specs=[
             pl.BlockSpec((1, tokens, cols), lambda t: (t, 0, 0)),
             pl.BlockSpec((cols, width), lambda t: (t, 0), memory_space=pltpu.VMEM),
-            whole(residual, not keep_rows),
+            whole(residual),
             whole(gain),
             whole(held),
         ],
         out_specs=[whole(x) for x in out],
         out_shape=out,
         scratch_shapes=[pltpu.VMEM((tokens, width), jnp.float32)],
+        name="project",
     )(stacked, weight, residual, gain, held)
 
 
@@ -449,7 +458,6 @@
         scores_t,
     )
     arrived = lax.all_to_all(message, "sp", split_axis=0, concat_axis=0, tiled=True)
-    residual_far = lax.ppermute(residual, "sp", swap)
     gated = call(
         mixer_kernel,
         like(value_matrix.shape),
@@ -470,10 +478,9 @@
     held_near, weights_near, held_far, weights_far = tables(
         jnp.stack([first_expert, far_place]), routes_t, scores_t, arrived, slots, cap
     )
-    stacked_far = lax.ppermute(stacked, "sp", swap)
     gain = expert_norm_gain.reshape(1, width)
     sent_near, middle, normed = project(
-        stacked, mixer_output_weight, residual, gain, held_near, True
+        stacked, mixer_output_weight, residual, gain, held_near
     )
     arrived_near = spread(sent_near)
     base = ffn(
@@ -484,7 +491,8 @@
         tok_count,
         add=middle,
     )[0]
-    (sent_far,) = project(stacked_far, mixer_output_weight, residual_far, gain, held_far, False)
+    normed_far = lax.ppermute(normed, "sp", swap)
+    sent_far = call(pack_kernel, like((slots, width)), held_far, normed_far, room=ROOM)
     arrived_far = spread(sent_far)
     done_near = experts(arrived_near)
     done_far = experts(arrived_far)

time: 219 us -> 214 us (0.977)
  blocking collectives: 9.38 us -> 30.7 us
  waiting for transfers between devices: 115 us -> 105 us
  local copies, waits for them, and re-layouts: 15.4 us -> 6.9 us
  Pallas kernels: 47.8 us -> 44.1 us
  starting transfers between devices: 29 us -> 25.7 us
    all_to_all x1, blocking collectives: 9.38 us -> 30.7 us  [spread(): lax.all_to_all(rows.reshape(half, exp_dev * cap, width), axes, split_axis...]
    all_to_all x4 -> x3, waiting for transfers between devices: 85.4 us -> 68.3 us  [spread(): lax.all_to_all(rows.reshape(half, exp_dev * cap, width), axes, split_axis...]
    ppermute x2 -> x1, waiting for transfers between devices: 10.6 us -> 24.6 us  [on_device(): normed_far = lax.ppermute(normed, 'sp', swap)]
    all_to_all x1, waiting for transfers between devices: 19.3 us -> 9.61 us  [on_device(): lax.all_to_all(message, 'sp', split_axis=0, concat_axis=0, tiled=True)]
    unnamed x26 -> x16, local copies, waits for them, and re-layouts: 15.4 us -> 6.9 us
    pallas_call x2 -> x1, Pallas kernels: 12.9 us -> 6.67 us  [project(): pl.pallas_call(project_kernel, grid=(count,), in_specs=[pl.BlockSpec((1,...]
    all_to_all x4 -> x3, starting transfers between devices: 18 us -> 13.1 us  [spread(): lax.all_to_all(rows.reshape(half, exp_dev * cap, width), axes, split_axis...]
    all_to_all x0 -> x1, starting transfers between devices: none -> 3.4 us  [on_device(): lax.all_to_all(stacked, 'tp', split_axis=0, concat_axis=0, tiled=True)]
  transfers between devices with their start and end apart: 8 -> 7, of which waited for: 6 -> 6; matrix products, arithmetic and copies ran while one was open for 0% -> 0% of each run, Pallas kernels for 16% -> 13%
where the time goes in v5:
time: 214 us; the launch traced here: 213 us
  waiting for transfers between devices  105 us (49%)
  Pallas kernels  44.1 us (21%)
  blocking collectives  30.7 us (14%)
  starting transfers between devices  25.7 us (12%)
  local copies, waits for them, and re-layouts  6.9 us (3%)
    all_to_all x3, waiting for transfers between devices, spread(): lax.all_to_all(rows.reshape(half, exp_dev * cap, width), axes, split_axis...  68.3 us
    all_to_all x1, blocking collectives, spread(): lax.all_to_all(rows.reshape(half, exp_dev * cap, width), axes, split_axis...  30.7 us
    ppermute x1, waiting for transfers between devices, on_device(): normed_far = lax.ppermute(normed, 'sp', swap)  24.6 us
    pallas_call x3, Pallas kernels, ffn(): pl.pallas_call(ffn_kernel, grid=(count, steps), in_specs=in_specs, out_sp...  21.6 us
    all_to_all x3, starting transfers between devices, spread(): lax.all_to_all(rows.reshape(half, exp_dev * cap, width), axes, split_axis...  13.1 us
    all_to_all x1, waiting for transfers between devices, on_device(): lax.all_to_all(message, 'sp', split_axis=0, concat_axis=0, tiled=True)  9.61 us
    pallas_call x3, Pallas kernels, call(): pl.pallas_call(kernel, grid=(1,), in_specs=in_specs, out_specs=jax.tree.m...  7.99 us
    all_to_all x1, starting transfers between devices, on_device(): lax.all_to_all(message, 'sp', split_axis=0, concat_axis=0, tiled=True)  7.31 us
  transfers between devices with their start and end apart: 7, of which 6 were waited for; matrix products, arithmetic and copies ran while one was open for 0% of the time, Pallas kernels for 13%

profile of v5, /device:TPU:0, one launch (start us, length us, event | category | flops | bytes accessed | tf_op | source)
XLA Modules:
  0.0 213.2 jit_solution(14625944906433195030)
XLA Ops:
  0.0 4.3 %shard_map.172 = (f32[512,128]{1,0:T(8,128)}, f32[8,128,128]{2,1,0:T(8,128)}, bf16[8,144,128]{2,1,0:T(8,128)(2,1)}) custom-call(bf16[512,128]{1,0:T(8,128)(2,1)} %k_ref.3, bf16[512,256]{1,0:T(8,128)(2,1)} %v_ref.3, bf16[512,128]{1,0:T(8,128)(2,1)} %c_ref.1, f32[2,512]{1,0:T(2,128)} %bitcast.32, s32[4,128]{1,0:T(4,128)} %bitcast.28, f32[4,128]{1,0:T(4,128)} %bitcast.30), custom_call_target="tpu_custom_call" | custom-call | tf_op jit(solution)/shard_map/pallas_call | solution.py:155
  4.3 7.3 %all-to-all-start = ((bf16[8,144,128]{2,1,0:T(8,128)(2,1)}), bf16[8,144,128]{2,1,0:T(8,128)(2,1)S(1)}, u32[]{:S(2)}, u32[]{:S(2)}) async-start(bf16[8,144,128]{2,1,0:T(8,128)(2,1)} %get-tuple-element.15), calls=%async_computation | async-start | bytes 589824 | tf_op jit(solution)/shard_map/all_to_all | solution.py:460
  11.6 9.6 %all-to-all-done.far_ref.msg_ref = bf16[8,144,128]{2,1,0:T(8,128)(2,1)S(1)} async-done(((bf16[8,144,128]{2,1,0:T(8,128)(2,1)}), bf16[8,144,128]{2,1,0:T(8,128)(2,1)S(1)}, u32[]{:S(2)}, u32[]{:S(2)}) %all-to-all-start) | async-done | bytes 294944 | tf_op jit(solution)/shard_map/all_to_all | solution.py:460
  21.2 0.7 copy-done.6
  21.9 3.0 %shard_map.173 = bf16[512,256]{1,0:T(8,128)(2,1)} custom-call(s32[1]{0:T(128)} %bitcast.5.place_ref, bf16[512,128]{1,0:T(8,128)(2,1)} %q_ref.1, bf16[512,128]{1,0:T(8,128)(2,1)} %k_ref.3, bf16[512,256]{1,0:T(8,128)(2,1)} %v_ref.3, f32[512,128]{1,0:T(8,128)} %get-tuple-element.17.within_ref, f32[8,128,128]{2,1,0:T(8,128)} %get-tuple-element.18.starts_ref, ...), custom_call_target="tpu_custom_call" | custom-call | tf_op jit(solution)/shard_map/pallas_call | solution.py:155
  24.9 3.4 %all-to-all-start.1 = ((bf16[4,128,256]{2,1,0:T(8,128)(2,1)}), bf16[4,128,256]{2,1,0:T(8,128)(2,1)S(1)}, u32[]{:S(2)}, u32[]{:S(2)}) async-start(bf16[4,128,256]{2,1,0:T(8,128)(2,1)} %bitcast.25), calls=%async_computation.1 | async-start | bytes 524288 | tf_op jit(solution)/shard_map/all_to_all | solution.py:477
  28.4 0.6 pad_add_fusion.place_ref
  29.0 2.7 %tables.1 = (bf16[512,128]{1,0:T(8,128)(2,1)}, bf16[256,512]{1,0:T(8,128)(2,1)}, bf16[512,128]{1,0:T(8,128)(2,1)}, bf16[256,512]{1,0:T(8,128)(2,1)}) custom-call(s32[2]{0:T(128)} %pad_add_fusion.place_ref, s32[4,128]{1,0:T(4,128)} %bitcast.29, f32[4,128]{1,0:T(4,128)} %bitcast.31, bf16[8,144,128]{2,1,0:T(8,128)(2,1)} %copy-done.6), custom_call_target="tpu_custom_call" | custom-call | tf_op jit(solution)/shard_map/tables/pallas_call | solution.py:271
  31.8 2.6 %all-to-all-done.1.g_ref = bf16[4,128,256]{2,1,0:T(8,128)(2,1)S(1)} async-done(((bf16[4,128,256]{2,1,0:T(8,128)(2,1)}), bf16[4,128,256]{2,1,0:T(8,128)(2,1)S(1)}, u32[]{:S(2)}, u32[]{:S(2)}) %all-to-all-start.1) | async-done | bytes 262176 | tf_op jit(solution)/shard_map/all_to_all | solution.py:477
  34.3 0.7 copy-done.7
  35.0 6.7 %project.1 = (bf16[512,2048]{1,0:T(8,128)(2,1)}, bf16[128,2048]{1,0:T(8,128)(2,1)}, bf16[128,2048]{1,0:T(8,128)(2,1)}) custom-call(bf16[4,128,256]{2,1,0:T(8,128)(2,1)} %copy-done.7, bf16[1024,2048]{1,0:T(8,128)(2,1)} %w_ref.1, bf16[128,2048]{1,0:T(8,128)(2,1)} %res_ref.1, f32[1,2048]{1,0:T(1,128)} %bitcast.27, bf16[512,128]{1,0:T(8,128)(2,1)} %get-tuple-element.19.held_ref), custom_call_target="tpu_custom_call" | custom-call | tf_op jit(solution)/shard_map/project/pallas_call | solution.py:330
  41.7 1.1 collective-permute-start
  42.8 24.6 %collective-permute-done.rows_ref = bf16[128,2048]{1,0:T(8,128)(2,1)S(1)} collective-permute-done((bf16[128,2048]{1,0:T(8,128)(2,1)}, bf16[128,2048]{1,0:T(8,128)(2,1)S(1)}, u32[]{:S(2)}, u32[]{:S(2)}) %collective-permute-start) | collective-permute-done | bytes 524320 | tf_op jit(solution)/shard_map/ppermute | solution.py:494
  67.4 0.7 shard_map.176
  68.1 30.7 %all_to_all.30.x_ref = bf16[16,32,2048]{2,1,0:T(8,128)(2,1)} all-to-all(bf16[16,32,2048]{2,1,0:T(8,128)(2,1)S(1)} %bitcast.19), channel_id=1, replica_groups={{0,1,2,3,4,5,6,7,8,9,10,11,12,13,14,15},{16,17,18,19,20,21,22,23,24,25,..., dimensions={0} | all-to-all | bytes 4194304 | tf_op jit(solution)/shard_map/all_to_all | solution.py:424
  98.8 3.7 %all-to-all-start.2 = ((bf16[16,32,2048]{2,1,0:T(8,128)(2,1)}), bf16[16,32,2048]{2,1,0:T(8,128)(2,1)S(1)}, u32[]{:S(2)}, u32[]{:S(2)}) async-start(bf16[16,32,2048]{2,1,0:T(8,128)(2,1)} %bitcast.21), calls=%async_computation.2 | async-start | bytes 4194304 | tf_op jit(solution)/shard_map/all_to_all | solution.py:424
  102.6 1.6 copy-done.2
  104.1 8.2 %shard_map.177 = bf16[16,32,2048]{2,1,0:T(8,128)(2,1)S(1)} custom-call(bf16[16,32,2048]{2,1,0:T(8,128)(2,1)S(1)} %copy-done.2, bf16[2,2048,512]{2,1,0:T(8,128)(2,1)} %gate_ref.5, bf16[2,2048,512]{2,1,0:T(8,128)(2,1)} %up_ref.3, bf16[2,512,2048]{2,1,0:T(8,128)(2,1)} %down_ref.3), custom_call_target="tpu_custom_call" | custom-call | flops 3221225472 | bytes 16777216 | tf_op jit(solution)/shard_map/pallas_call | solution.py:211
  112.3 1.3 copy-done.1
  113.7 17.9 %all-to-all-done.2.x_ref = bf16[16,32,2048]{2,1,0:T(8,128)(2,1)S(1)} async-done(((bf16[16,32,2048]{2,1,0:T(8,128)(2,1)}), bf16[16,32,2048]{2,1,0:T(8,128)(2,1)S(1)}, u32[]{:S(2)}, u32[]{:S(2)}) %all-to-all-start.2) | async-done | bytes 2097184 | tf_op jit(solution)/shard_map/all_to_all | solution.py:424
  131.6 4.5 %all-to-all-start.5 = ((bf16[16,32,2048]{2,1,0:T(8,128)(2,1)}), bf16[16,32,2048]{2,1,0:T(8,128)(2,1)}, u32[]{:S(2)}, u32[]{:S(2)}) async-start(bf16[16,32,2048]{2,1,0:T(8,128)(2,1)} %copy-done.1), calls=%async_computation.5 | async-start | bytes 4194304 | tf_op jit(solution)/shard_map/all_to_all | solution.py:424
  136.1 8.2 %shard_map.174 = bf16[16,32,2048]{2,1,0:T(8,128)(2,1)S(1)} custom-call(bf16[16,32,2048]{2,1,0:T(8,128)(2,1)S(1)} %all-to-all-done.2.x_ref, bf16[2,2048,512]{2,1,0:T(8,128)(2,1)} %gate_ref.5, bf16[2,2048,512]{2,1,0:T(8,128)(2,1)} %up_ref.3, bf16[2,512,2048]{2,1,0:T(8,128)(2,1)} %down_ref.3), custom_call_target="tpu_custom_call" | custom-call | flops 3221225472 | bytes 16777216 | tf_op jit(solution)/shard_map/pallas_call | solution.py:211
  144.3 1.3 copy-done
  145.6 19.5 %all-to-all-done.5 = bf16[16,32,2048]{2,1,0:T(8,128)(2,1)} async-done(((bf16[16,32,2048]{2,1,0:T(8,128)(2,1)}), bf16[16,32,2048]{2,1,0:T(8,128)(2,1)}, u32[]{:S(2)}, u32[]{:S(2)}) %all-to-all-start.5) | async-done | bytes 2097184 | tf_op jit(solution)/shard_map/all_to_all | solution.py:424
  165.2 4.9 %all-to-all-start.3 = ((bf16[16,32,2048]{2,1,0:T(8,128)(2,1)}), bf16[16,32,2048]{2,1,0:T(8,128)(2,1)S(1)}, u32[]{:S(2)}, u32[]{:S(2)}) async-start(bf16[16,32,2048]{2,1,0:T(8,128)(2,1)} %copy-done), calls=%async_computation.3 | async-start | bytes 4194304 | tf_op jit(solution)/shard_map/all_to_all | solution.py:424
  170.1 3.2 %shard_map.178 = bf16[128,2048]{1,0:T(8,128)(2,1)} custom-call(bf16[256,512]{1,0:T(8,128)(2,1)} %get-tuple-element.23.weight_ref, bf16[512,2048]{1,0:T(8,128)(2,1)} %bitcast.17.results_ref), custom_call_target="tpu_custom_call" | custom-call | tf_op jit(solution)/shard_map/pallas_call | solution.py:375
  173.2 0.8 collective-permute-start.1
  174.0 5.2 %shard_map.175 = f32[1,128,2048]{2,1,0:T(8,128)} custom-call(bf16[1,128,2048]{2,1,0:T(8,128)(2,1)} %bitcast.26, bf16[1,2048,512]{2,1,0:T(8,128)(2,1)} %bitcast.22, bf16[1,2048,512]{2,1,0:T(8,128)(2,1)} %bitcast.23, bf16[1,512,2048]{2,1,0:T(8,128)(2,1)} %bitcast.24, bf16[128,2048]{1,0:T(8,128)(2,1)} %get-tuple-element.22.rest_0_), custom_call_target="tpu_custom_call" | custom-call | flops 805306368 | bytes 7340032 | tf_op jit(solution)/shard_map/pallas_call | solution.py:211
  179.2 30.8 %all-to-all-done.3 = bf16[16,32,2048]{2,1,0:T(8,128)(2,1)S(1)} async-done(((bf16[16,32,2048]{2,1,0:T(8,128)(2,1)}), bf16[16,32,2048]{2,1,0:T(8,128)(2,1)S(1)}, u32[]{:S(2)}, u32[]{:S(2)}) %all-to-all-start.3) | async-done | bytes 2097184 | tf_op jit(solution)/shard_map/all_to_all | solution.py:424
  210.0 0.0 collective-permute-done.1.rest_1_
  210.0 1.2 copy-done.3
  211.3 1.9 shard_map.179
  (10 shorter events, 0.0 us)
Async XLA Ops:
  4.3 16.9 %all-to-all-start = ((bf16[8,144,128]{2,1,0:T(8,128)(2,1)}), bf16[8,144,128]{2,1,0:T(8,128)(2,1)S(1)}, u32[]{:S(2)}, u32[]{:S(2)}) async-start(bf16[8,144,128]{2,1,0:T(8,128)(2,1)} %get-tuple-element.15), calls=%async_computation | async-start | bytes 589824 | tf_op jit(solution)/shard_map/all_to_all | solution.py:460
  21.2 0.7 copy-start.6
  24.9 9.4 %all-to-all-start.1 = ((bf16[4,128,256]{2,1,0:T(8,128)(2,1)}), bf16[4,128,256]{2,1,0:T(8,128)(2,1)S(1)}, u32[]{:S(2)}, u32[]{:S(2)}) async-start(bf16[4,128,256]{2,1,0:T(8,128)(2,1)} %bitcast.25), calls=%async_computation.1 | async-start | bytes 524288 | tf_op jit(solution)/shard_map/all_to_all | solution.py:477
  34.3 0.7 copy-start.7
  35.0 32.4 %copy-start.5 = (bf16[512,128]{1,0:T(8,128)(2,1)S(1)}, bf16[512,128]{1,0:T(8,128)(2,1)}, u32[]{:S(2)}) copy-start(bf16[512,128]{1,0:T(8,128)(2,1)} %get-tuple-element.24.held_ref) | copy-start | bytes 393220
  41.7 25.7 %collective-permute-start = (bf16[128,2048]{1,0:T(8,128)(2,1)}, bf16[128,2048]{1,0:T(8,128)(2,1)S(1)}, u32[]{:S(2)}, u32[]{:S(2)}) collective-permute-start(bf16[128,2048]{1,0:T(8,128)(2,1)} %get-tuple-element.21), channel_id=1, source_target_pairs={{0,16},{4,20},{8,24},{12,28},{16,0},{20,4},{24,8},{28,12},{1,17},{... | collective-permute-start | bytes 1572872 | tf_op jit(solution)/shard_map/ppermute | solution.py:494
  98.8 32.8 %all-to-all-start.2 = ((bf16[16,32,2048]{2,1,0:T(8,128)(2,1)}), bf16[16,32,2048]{2,1,0:T(8,128)(2,1)S(1)}, u32[]{:S(2)}, u32[]{:S(2)}) async-start(bf16[16,32,2048]{2,1,0:T(8,128)(2,1)} %bitcast.21), calls=%async_computation.2 | async-start | bytes 4194304 | tf_op jit(solution)/shard_map/all_to_all | solution.py:424
  102.6 1.6 copy-start.2
  112.3 1.3 copy-start.1
  131.6 33.6 %all-to-all-start.5 = ((bf16[16,32,2048]{2,1,0:T(8,128)(2,1)}), bf16[16,32,2048]{2,1,0:T(8,128)(2,1)}, u32[]{:S(2)}, u32[]{:S(2)}) async-start(bf16[16,32,2048]{2,1,0:T(8,128)(2,1)} %copy-done.1), calls=%async_computation.5 | async-start | bytes 4194304 | tf_op jit(solution)/shard_map/all_to_all | solution.py:424
  144.3 1.3 copy-start
  165.2 44.9 %all-to-all-start.3 = ((bf16[16,32,2048]{2,1,0:T(8,128)(2,1)}), bf16[16,32,2048]{2,1,0:T(8,128)(2,1)S(1)}, u32[]{:S(2)}, u32[]{:S(2)}) async-start(bf16[16,32,2048]{2,1,0:T(8,128)(2,1)} %copy-done), calls=%async_computation.3 | async-start | bytes 4194304 | tf_op jit(solution)/shard_map/all_to_all | solution.py:424
  173.2 36.8 %collective-permute-start.1 = (bf16[128,2048]{1,0:T(8,128)(2,1)}, bf16[128,2048]{1,0:T(8,128)(2,1)S(1)}, u32[]{:S(2)}, u32[]{:S(2)}) collective-permute-start(bf16[128,2048]{1,0:T(8,128)(2,1)} %shard_map.178), channel_id=1, source_target_pairs={{0,16},{4,20},{8,24},{12,28},{16,0},{20,4},{24,8},{28,12},{1,17},{... | collective-permute-start | bytes 1572872 | tf_op jit(solution)/shard_map/ppermute | solution.py:503
  174.0 36.0 %copy-start.4 = (bf16[256,512]{1,0:T(8,128)(2,1)S(1)}, bf16[256,512]{1,0:T(8,128)(2,1)}, u32[]{:S(2)}) copy-start(bf16[256,512]{1,0:T(8,128)(2,1)} %get-tuple-element.16.weight_ref) | copy-start | bytes 786436
  210.0 1.2 copy-start.3

commit v6 on v5

--- a/solution.py
+++ b/solution.py
@@ -291,96 +291,141 @@
     return jnp.dot(held, rows, preferred_element_type=jnp.float32).astype(jnp.bfloat16)
 
 
-def pack_kernel(held_ref, rows_ref, sent_ref):
-    sent_ref[...] = pick(held_ref[...], rows_ref[...])
+def start_all(pairs, sems):
+    copies = [pltpu.make_async_copy(src, dst, sems.at[i]) for i, (src, dst) in enumerate(pairs)]
+    for copy in copies:
+        copy.start()
+    return copies
+
+
+def pieces_of(rows, count):
+    return [pl.ds(i * (rows // count), rows // count) for i in range(count)]
+
+
+def streamed(kernel, out, args, scratch, copies, room=None):
+    anywhere = pl.BlockSpec(memory_space=pl.ANY)
+    return pl.pallas_call(
+        kernel,
+        in_specs=[anywhere] * len(args),
+        out_specs=jax.tree.map(lambda _: anywhere, out),
+        out_shape=out,
+        scratch_shapes=[pltpu.VMEM(x.shape, x.dtype) for x in scratch]
+        + [pltpu.SemaphoreType.DMA((copies,))],
+        compiler_params=pltpu.CompilerParams(vmem_limit_bytes=room),
+    )(*args)
+
+
+PIECES = 4
+
+
+def store_slots(held, normed, sent, sent_out, sems, first):
+    copies = []
+    for i, at in enumerate(pieces_of(sent.shape[0], PIECES)):
+        sent[at, :] = pick(held[at, :], normed)
+        copies.append(
+            pltpu.make_async_copy(sent.at[at, :], sent_out.at[at, :], sems.at[first + i])
+        )
+        copies[-1].start()
+    return copies
+
+
+def pack_kernel(held_in, rows_in, sent_out, held, rows, sent, sems):
+    loads = start_all([(held_in, held), (rows_in, rows)], sems)
+    for copy in loads:
+        copy.wait()
+    for copy in store_slots(held, rows[...], sent, sent_out, sems, 2):
+        copy.wait()
+
+
+def pack(held, rows):
+    out = jax.ShapeDtypeStruct((held.shape[0], rows.shape[1]), rows.dtype)
+    args = (held, rows)
+    return streamed(pack_kernel, out, args, args + (out,), 2 + PIECES, ROOM)
 
 
 def project_kernel(
-    g_ref, w_ref, res_ref, gain_ref, held_ref, sent_ref, mid_ref, norm_ref, acc_ref
+    g_in, w_in, res_in, gain_in, held_in, sent_out, mid_out, norm_out, *buffers
 ):
-    step = pl.program_id(0)
-    part = jnp.dot(g_ref[0], w_ref[...], preferred_element_type=jnp.float32)
-
-    @pl.when(step == 0)
-    def _():
-        acc_ref[...] = res_ref[...].astype(jnp.float32) + part
-
-    @pl.when(step != 0)
-    def _():
-        acc_ref[...] += part
-
-    @pl.when(step == pl.num_programs(0) - 1)
-    def _():
-        middle = acc_ref[...].astype(jnp.bfloat16)
-        wide = middle.astype(jnp.float32)
-        scale = lax.rsqrt(jnp.mean(wide * wide, axis=-1, keepdims=True) + eps_norm)
-        normed = (wide * scale * gain_ref[...]).astype(jnp.bfloat16)
-        sent_ref[...] = pick(held_ref[...], normed)
-        mid_ref[...] = middle
-        norm_ref[...] = normed
+    g, w, res, gain, held, sent, mid, norm, sems = buffers
+    count, _, _ = g.shape
+    pieces = pieces_of(w.shape[0], count)
+    loads = start_all(
+        [(g_in, g)]
+        + [(w_in.at[at, :], w.at[at, :]) for at in pieces]
+        + [(res_in, res), (gain_in, gain), (held_in, held)],
+        sems,
+    )
+    loads[0].wait()
+    total = None
+    for t, at in enumerate(pieces):
+        loads[1 + t].wait()
+        part = jnp.dot(g[t], w[at, :], preferred_element_type=jnp.float32)
+        total = part if total is None else total + part
+    for copy in loads[1 + count :]:
+        copy.wait()
+    middle = (total + res[...].astype(jnp.float32)).astype(jnp.bfloat16)
+    wide = middle.astype(jnp.float32)
+    scale = lax.rsqrt(jnp.mean(wide * wide, axis=-1, keepdims=True) + eps_norm)
+    normed = (wide * scale * gain[...]).astype(jnp.bfloat16)
+    norm[...] = normed
+    mid[...] = middle
+    first = len(loads)
+    stores = [
+        pltpu.make_async_copy(norm, norm_out, sems.at[first]),
+        pltpu.make_async_copy(mid, mid_out, sems.at[first + 1]),
+    ]
+    for copy in stores:
+        copy.start()
+    for copy in stores + store_slots(held, normed, sent, sent_out, sems, first + 2):
+        copy.wait()
 
 
 def project(stacked, weight, residual, gain, held):
-    count, tokens, cols = stacked.shape
-    width = residual.shape[1]
-    slots = held.shape[0]
-    rows = jax.ShapeDtypeStruct((tokens, width), jnp.bfloat16)
-    out = [jax.ShapeDtypeStruct((slots, width), jnp.bfloat16), rows, rows]
-
-    return pl.pallas_call(
-        project_kernel,
-        grid=(count,),
-        in_specs=[
-            pl.BlockSpec((1, tokens, cols), lambda t: (t, 0, 0)),
-            pl.BlockSpec((cols, width), lambda t: (t, 0), memory_space=pltpu.VMEM),
-            whole(residual),
-            whole(gain),
-            whole(held),
-        ],
-        out_specs=[whole(x) for x in out],
-        out_shape=out,
-        scratch_shapes=[pltpu.VMEM((tokens, width), jnp.float32)],
-        name="project",
-    )(stacked, weight, residual, gain, held)
-
-
-def weigh_kernel(weight_ref, results_ref, *rest):
-    out_ref, acc_ref = rest[-2:]
-    step = pl.program_id(0)
-    tokens = out_ref.shape[0]
-    both = jnp.dot(weight_ref[...], results_ref[...], preferred_element_type=jnp.float32)
-    part = both[:tokens] + both[tokens:]
-
-    @pl.when(step == 0)
-    def _():
-        acc_ref[...] = part
-
-    @pl.when(step == pl.num_programs(0) - 1)
-    def _():
-        total = acc_ref[...] + part
-        if len(rest) == 4:
-            total = total + rest[0][...] + rest[1][...].astype(jnp.float32)
-        out_ref[...] = total.astype(jnp.bfloat16)
+    rows = jax.ShapeDtypeStruct(residual.shape, jnp.bfloat16)
+    out = (jax.ShapeDtypeStruct((held.shape[0], residual.shape[1]), jnp.bfloat16), rows, rows)
+    args = (stacked, weight, residual, gain, held)
+    return streamed(project_kernel, out, args, args + out, 6 + stacked.shape[0] + PIECES)
+
+
+def weigh_kernel(more, weight_in, results_in, *refs):
+    extra_in, out_ref = refs[:more], refs[more]
+    weight, results = refs[more + 1 : more + 3]
+    extra = refs[more + 3 : 2 * more + 3]
+    done, sems = refs[2 * more + 3 :]
+    tokens = done.shape[0]
+    pieces = pieces_of(results.shape[0], PIECES)
+    loads = start_all(
+        [(weight_in, weight)]
+        + [(results_in.at[at, :], results.at[at, :]) for at in pieces]
+        + list(zip(extra_in, extra)),
+        sems,
+    )
+    loads[0].wait()
+    total = None
+    for i, at in enumerate(pieces):
+        loads[1 + i].wait()
+        part = jnp.dot(weight[:, at], results[at, :], preferred_element_type=jnp.float32)
+        total = part if total is None else total + part
+    total = total[:tokens] + total[tokens:]
+    for copy, ref in zip(loads[1 + PIECES :], extra):
+        copy.wait()
+        total = total + ref[...].astype(jnp.float32)
+    done[...] = total.astype(jnp.bfloat16)
+    store = pltpu.make_async_copy(done, out_ref, sems.at[len(loads)])
+    store.start()
+    store.wait()
 
 
 def weigh(out, weights, results, *more):
-    slots, width = results.shape
-    piece = slots // 2
-    in_specs = [
-        pl.BlockSpec((weights.shape[0], piece), lambda k: (0, k), memory_space=pltpu.VMEM),
-        pl.BlockSpec((piece, width), lambda k: (k, 0)),
-    ]
-    if more:
-        in_specs += [whole(more[0]), whole(more[1], True)]
-    return pl.pallas_call(
-        weigh_kernel,
-        grid=(2,),
-        in_specs=in_specs,
-        out_specs=whole(out),
-        out_shape=out,
-        scratch_shapes=[pltpu.VMEM(out.shape, jnp.float32)],
-        compiler_params=pltpu.CompilerParams(vmem_limit_bytes=ROOM if more else None),
-    )(weights, results, *more)
+    args = (weights, results) + more
+    return streamed(
+        functools.partial(weigh_kernel, len(more)),
+        out,
+        args,
+        args + (out,),
+        2 + PIECES + len(more),
+        ROOM if more else None,
+    )
 
 
 def on_device(
@@ -492,7 +537,7 @@
         add=middle,
     )[0]
     normed_far = lax.ppermute(normed, "sp", swap)
-    sent_far = call(pack_kernel, like((slots, width)), held_far, normed_far, room=ROOM)
+    sent_far = pack(held_far, normed_far)
     arrived_far = spread(sent_far)
     done_near = experts(arrived_near)
     done_far = experts(arrived_far)

time: 214 us -> 214 us (level)
    pallas_call x3 -> x2, Pallas kernels: 7.99 us -> 7.3 us  [call(): pl.pallas_call(kernel, grid=(1,), in_specs=in_specs, out_specs=jax.tree.m...]
    pallas_call x3 -> x4, Pallas kernels: 11.8 us -> 12.4 us  [streamed(): pl.pallas_call(kernel, in_specs=[anywhere] * len(args), out_specs=jax.tre...]
where the time goes in v6:
time: 214 us; the launch traced here: 213 us
  waiting for transfers between devices  105 us (49%)
  Pallas kernels  44 us (21%)
  blocking collectives  30.7 us (14%)
  starting transfers between devices  25.8 us (12%)
  local copies, waits for them, and re-layouts  6.9 us (3%)
    all_to_all x3, waiting for transfers between devices, spread(): lax.all_to_all(rows.reshape(half, exp_dev * cap, width), axes, split_axis...  67.9 us
    all_to_all x1, blocking collectives, spread(): lax.all_to_all(rows.reshape(half, exp_dev * cap, width), axes, split_axis...  30.7 us
    ppermute x1, waiting for transfers between devices, on_device(): normed_far = lax.ppermute(normed, 'sp', swap)  24.6 us
    pallas_call x3, Pallas kernels, ffn(): pl.pallas_call(ffn_kernel, grid=(count, steps), in_specs=in_specs, out_sp...  21.6 us
    all_to_all x3, starting transfers between devices, spread(): lax.all_to_all(rows.reshape(half, exp_dev * cap, width), axes, split_axis...  13.1 us
    pallas_call x4, Pallas kernels, streamed(): pl.pallas_call(kernel, in_specs=[anywhere] * len(args), out_specs=jax.tre...  12.4 us
    all_to_all x1, waiting for transfers between devices, on_device(): lax.all_to_all(message, 'sp', split_axis=0, concat_axis=0, tiled=True)  9.61 us
    all_to_all x1, starting transfers between devices, on_device(): lax.all_to_all(message, 'sp', split_axis=0, concat_axis=0, tiled=True)  7.31 us
  transfers between devices with their start and end apart: 7, of which 6 were waited for; matrix products, arithmetic and copies ran while one was open for 0% of the time, Pallas kernels for 13%

profile of v6, /device:TPU:0, one launch (start us, length us, event | category | flops | bytes accessed | tf_op | source)
XLA Modules:
  0.0 213.1 jit_solution(9630016104809660109)
XLA Ops:
  0.0 4.3 %shard_map.172 = (f32[512,128]{1,0:T(8,128)}, f32[8,128,128]{2,1,0:T(8,128)}, bf16[8,144,128]{2,1,0:T(8,128)(2,1)}) custom-call(bf16[512,128]{1,0:T(8,128)(2,1)} %k_ref.3, bf16[512,256]{1,0:T(8,128)(2,1)} %v_ref.3, bf16[512,128]{1,0:T(8,128)(2,1)} %c_ref.1, f32[2,512]{1,0:T(2,128)} %bitcast.32, s32[4,128]{1,0:T(4,128)} %bitcast.28, f32[4,128]{1,0:T(4,128)} %bitcast.30), custom_call_target="tpu_custom_call" | custom-call | tf_op jit(solution)/shard_map/pallas_call | solution.py:155
  4.3 7.3 %all-to-all-start = ((bf16[8,144,128]{2,1,0:T(8,128)(2,1)}), bf16[8,144,128]{2,1,0:T(8,128)(2,1)S(1)}, u32[]{:S(2)}, u32[]{:S(2)}) async-start(bf16[8,144,128]{2,1,0:T(8,128)(2,1)} %get-tuple-element.15), calls=%async_computation | async-start | bytes 589824 | tf_op jit(solution)/shard_map/all_to_all | solution.py:505
  11.6 9.6 %all-to-all-done.far_ref.msg_ref = bf16[8,144,128]{2,1,0:T(8,128)(2,1)S(1)} async-done(((bf16[8,144,128]{2,1,0:T(8,128)(2,1)}), bf16[8,144,128]{2,1,0:T(8,128)(2,1)S(1)}, u32[]{:S(2)}, u32[]{:S(2)}) %all-to-all-start) | async-done | bytes 294944 | tf_op jit(solution)/shard_map/all_to_all | solution.py:505
  21.2 0.7 copy-done.6
  21.9 3.0 %shard_map.173 = bf16[512,256]{1,0:T(8,128)(2,1)} custom-call(s32[1]{0:T(128)} %bitcast.5.place_ref, bf16[512,128]{1,0:T(8,128)(2,1)} %q_ref.1, bf16[512,128]{1,0:T(8,128)(2,1)} %k_ref.3, bf16[512,256]{1,0:T(8,128)(2,1)} %v_ref.3, f32[512,128]{1,0:T(8,128)} %get-tuple-element.17.within_ref, f32[8,128,128]{2,1,0:T(8,128)} %get-tuple-element.18.starts_ref, ...), custom_call_target="tpu_custom_call" | custom-call | tf_op jit(solution)/shard_map/pallas_call | solution.py:155
  24.9 3.4 %all-to-all-start.1 = ((bf16[4,128,256]{2,1,0:T(8,128)(2,1)}), bf16[4,128,256]{2,1,0:T(8,128)(2,1)S(1)}, u32[]{:S(2)}, u32[]{:S(2)}) async-start(bf16[4,128,256]{2,1,0:T(8,128)(2,1)} %bitcast.25), calls=%async_computation.1 | async-start | bytes 524288 | tf_op jit(solution)/shard_map/all_to_all | solution.py:522
  28.4 0.6 pad_add_fusion.place_ref
  29.0 2.7 %tables.1 = (bf16[512,128]{1,0:T(8,128)(2,1)}, bf16[256,512]{1,0:T(8,128)(2,1)}, bf16[512,128]{1,0:T(8,128)(2,1)}, bf16[256,512]{1,0:T(8,128)(2,1)}) custom-call(s32[2]{0:T(128)} %pad_add_fusion.place_ref, s32[4,128]{1,0:T(4,128)} %bitcast.29, f32[4,128]{1,0:T(4,128)} %bitcast.31, bf16[8,144,128]{2,1,0:T(8,128)(2,1)} %copy-done.6), custom_call_target="tpu_custom_call" | custom-call | tf_op jit(solution)/shard_map/tables/pallas_call | solution.py:271
  31.8 2.6 %all-to-all-done.1.g_in = bf16[4,128,256]{2,1,0:T(8,128)(2,1)S(1)} async-done(((bf16[4,128,256]{2,1,0:T(8,128)(2,1)}), bf16[4,128,256]{2,1,0:T(8,128)(2,1)S(1)}, u32[]{:S(2)}, u32[]{:S(2)}) %all-to-all-start.1) | async-done | bytes 262176 | tf_op jit(solution)/shard_map/all_to_all | solution.py:522
  34.3 0.7 copy-done.7
  35.0 4.8 %shard_map.174 = (bf16[512,2048]{1,0:T(8,128)(2,1)}, bf16[128,2048]{1,0:T(8,128)(2,1)}, bf16[128,2048]{1,0:T(8,128)(2,1)}) custom-call(bf16[4,128,256]{2,1,0:T(8,128)(2,1)} %copy-done.7, bf16[1024,2048]{1,0:T(8,128)(2,1)} %w_in.1, bf16[128,2048]{1,0:T(8,128)(2,1)} %res_in.1, f32[1,2048]{1,0:T(1,128)} %bitcast.27, bf16[512,128]{1,0:T(8,128)(2,1)} %get-tuple-element.19.held_in), custom_call_target="tpu_custom_call" | custom-call | tf_op jit(solution)/shard_map/pallas_call | solution.py:307
  39.8 1.2 collective-permute-start
  41.0 24.6 %collective-permute-done.rows_in = bf16[128,2048]{1,0:T(8,128)(2,1)S(1)} collective-permute-done((bf16[128,2048]{1,0:T(8,128)(2,1)}, bf16[128,2048]{1,0:T(8,128)(2,1)S(1)}, u32[]{:S(2)}, u32[]{:S(2)}) %collective-permute-start) | collective-permute-done | bytes 524320 | tf_op jit(solution)/shard_map/ppermute | solution.py:539
  65.6 1.5 shard_map.177
  67.2 30.7 %all_to_all.30.x_ref = bf16[16,32,2048]{2,1,0:T(8,128)(2,1)} all-to-all(bf16[16,32,2048]{2,1,0:T(8,128)(2,1)S(1)} %bitcast.19), channel_id=1, replica_groups={{0,1,2,3,4,5,6,7,8,9,10,11,12,13,14,15},{16,17,18,19,20,21,22,23,24,25,..., dimensions={0} | all-to-all | bytes 4194304 | tf_op jit(solution)/shard_map/all_to_all | solution.py:469
  97.9 3.7 %all-to-all-start.2 = ((bf16[16,32,2048]{2,1,0:T(8,128)(2,1)}), bf16[16,32,2048]{2,1,0:T(8,128)(2,1)S(1)}, u32[]{:S(2)}, u32[]{:S(2)}) async-start(bf16[16,32,2048]{2,1,0:T(8,128)(2,1)} %bitcast.21), calls=%async_computation.2 | async-start | bytes 4194304 | tf_op jit(solution)/shard_map/all_to_all | solution.py:469
  101.6 1.6 copy-done.2
  103.2 8.2 %shard_map.178 = bf16[16,32,2048]{2,1,0:T(8,128)(2,1)S(1)} custom-call(bf16[16,32,2048]{2,1,0:T(8,128)(2,1)S(1)} %copy-done.2, bf16[2,2048,512]{2,1,0:T(8,128)(2,1)} %gate_ref.5, bf16[2,2048,512]{2,1,0:T(8,128)(2,1)} %up_ref.3, bf16[2,512,2048]{2,1,0:T(8,128)(2,1)} %down_ref.3), custom_call_target="tpu_custom_call" | custom-call | flops 3221225472 | bytes 16777216 | tf_op jit(solution)/shard_map/pallas_call | solution.py:211
  111.4 1.3 copy-done.1
  112.7 17.9 %all-to-all-done.2.x_ref = bf16[16,32,2048]{2,1,0:T(8,128)(2,1)S(1)} async-done(((bf16[16,32,2048]{2,1,0:T(8,128)(2,1)}), bf16[16,32,2048]{2,1,0:T(8,128)(2,1)S(1)}, u32[]{:S(2)}, u32[]{:S(2)}) %all-to-all-start.2) | async-done | bytes 2097184 | tf_op jit(solution)/shard_map/all_to_all | solution.py:469
  130.6 4.5 %all-to-all-start.5 = ((bf16[16,32,2048]{2,1,0:T(8,128)(2,1)}), bf16[16,32,2048]{2,1,0:T(8,128)(2,1)}, u32[]{:S(2)}, u32[]{:S(2)}) async-start(bf16[16,32,2048]{2,1,0:T(8,128)(2,1)} %copy-done.1), calls=%async_computation.5 | async-start | bytes 4194304 | tf_op jit(solution)/shard_map/all_to_all | solution.py:469
  135.1 8.2 %shard_map.175 = bf16[16,32,2048]{2,1,0:T(8,128)(2,1)S(1)} custom-call(bf16[16,32,2048]{2,1,0:T(8,128)(2,1)S(1)} %all-to-all-done.2.x_ref, bf16[2,2048,512]{2,1,0:T(8,128)(2,1)} %gate_ref.5, bf16[2,2048,512]{2,1,0:T(8,128)(2,1)} %up_ref.3, bf16[2,512,2048]{2,1,0:T(8,128)(2,1)} %down_ref.3), custom_call_target="tpu_custom_call" | custom-call | flops 3221225472 | bytes 16777216 | tf_op jit(solution)/shard_map/pallas_call | solution.py:211
  143.3 1.3 copy-done
  144.6 19.5 %all-to-all-done.5 = bf16[16,32,2048]{2,1,0:T(8,128)(2,1)} async-done(((bf16[16,32,2048]{2,1,0:T(8,128)(2,1)}), bf16[16,32,2048]{2,1,0:T(8,128)(2,1)}, u32[]{:S(2)}, u32[]{:S(2)}) %all-to-all-start.5) | async-done | bytes 2097184 | tf_op jit(solution)/shard_map/all_to_all | solution.py:469
  164.2 4.9 %all-to-all-start.3 = ((bf16[16,32,2048]{2,1,0:T(8,128)(2,1)}), bf16[16,32,2048]{2,1,0:T(8,128)(2,1)S(1)}, u32[]{:S(2)}, u32[]{:S(2)}) async-start(bf16[16,32,2048]{2,1,0:T(8,128)(2,1)} %copy-done), calls=%async_computation.3 | async-start | bytes 4194304 | tf_op jit(solution)/shard_map/all_to_all | solution.py:469
  169.1 3.4 %shard_map.179 = bf16[128,2048]{1,0:T(8,128)(2,1)} custom-call(bf16[256,512]{1,0:T(8,128)(2,1)} %get-tuple-element.23.weight_in, bf16[512,2048]{1,0:T(8,128)(2,1)} %bitcast.17.results_in), custom_call_target="tpu_custom_call" | custom-call | tf_op jit(solution)/shard_map/pallas_call | solution.py:307
  172.6 0.8 collective-permute-start.1
  173.4 5.2 %shard_map.176 = f32[1,128,2048]{2,1,0:T(8,128)} custom-call(bf16[1,128,2048]{2,1,0:T(8,128)(2,1)} %bitcast.26, bf16[1,2048,512]{2,1,0:T(8,128)(2,1)} %bitcast.22, bf16[1,2048,512]{2,1,0:T(8,128)(2,1)} %bitcast.23, bf16[1,512,2048]{2,1,0:T(8,128)(2,1)} %bitcast.24, bf16[128,2048]{1,0:T(8,128)(2,1)} %get-tuple-element.22.rest_0_), custom_call_target="tpu_custom_call" | custom-call | flops 805306368 | bytes 7340032 | tf_op jit(solution)/shard_map/pallas_call | solution.py:211
  178.6 30.5 %all-to-all-done.3 = bf16[16,32,2048]{2,1,0:T(8,128)(2,1)S(1)} async-done(((bf16[16,32,2048]{2,1,0:T(8,128)(2,1)}), bf16[16,32,2048]{2,1,0:T(8,128)(2,1)S(1)}, u32[]{:S(2)}, u32[]{:S(2)}) %all-to-all-start.3) | async-done | bytes 2097184 | tf_op jit(solution)/shard_map/all_to_all | solution.py:469
  209.0 0.0 collective-permute-done.1.refs_1_
  209.1 1.2 copy-done.3
  210.3 2.6 %shard_map.180 = bf16[128,2048]{1,0:T(8,128)(2,1)} custom-call(bf16[256,512]{1,0:T(8,128)(2,1)S(1)} %copy-done.4, bf16[512,2048]{1,0:T(8,128)(2,1)S(1)} %bitcast.18, f32[128,2048]{1,0:T(8,128)S(1)} %bitcast.20, bf16[128,2048]{1,0:T(8,128)(2,1)S(1)} %collective-permute-done.1.refs_1_), custom_call_target="tpu_custom_call" | custom-call | tf_op jit(solution)/shard_map/pallas_call | solution.py:307
  (10 shorter events, 0.0 us)
Async XLA Ops:
  4.3 16.9 %all-to-all-start = ((bf16[8,144,128]{2,1,0:T(8,128)(2,1)}), bf16[8,144,128]{2,1,0:T(8,128)(2,1)S(1)}, u32[]{:S(2)}, u32[]{:S(2)}) async-start(bf16[8,144,128]{2,1,0:T(8,128)(2,1)} %get-tuple-element.15), calls=%async_computation | async-start | bytes 589824 | tf_op jit(solution)/shard_map/all_to_all | solution.py:505
  21.2 0.7 copy-start.6
  24.9 9.4 %all-to-all-start.1 = ((bf16[4,128,256]{2,1,0:T(8,128)(2,1)}), bf16[4,128,256]{2,1,0:T(8,128)(2,1)S(1)}, u32[]{:S(2)}, u32[]{:S(2)}) async-start(bf16[4,128,256]{2,1,0:T(8,128)(2,1)} %bitcast.25), calls=%async_computation.1 | async-start | bytes 524288 | tf_op jit(solution)/shard_map/all_to_all | solution.py:522
  34.3 0.7 copy-start.7
  35.0 30.6 %copy-start.5 = (bf16[512,128]{1,0:T(8,128)(2,1)S(1)}, bf16[512,128]{1,0:T(8,128)(2,1)}, u32[]{:S(2)}) copy-start(bf16[512,128]{1,0:T(8,128)(2,1)} %get-tuple-element.24.held_in) | copy-start | bytes 393220
  39.8 25.8 %collective-permute-start = (bf16[128,2048]{1,0:T(8,128)(2,1)}, bf16[128,2048]{1,0:T(8,128)(2,1)S(1)}, u32[]{:S(2)}, u32[]{:S(2)}) collective-permute-start(bf16[128,2048]{1,0:T(8,128)(2,1)} %get-tuple-element.21), channel_id=1, source_target_pairs={{0,16},{4,20},{8,24},{12,28},{16,0},{20,4},{24,8},{28,12},{1,17},{... | collective-permute-start | bytes 1572872 | tf_op jit(solution)/shard_map/ppermute | solution.py:539
  97.9 32.8 %all-to-all-start.2 = ((bf16[16,32,2048]{2,1,0:T(8,128)(2,1)}), bf16[16,32,2048]{2,1,0:T(8,128)(2,1)S(1)}, u32[]{:S(2)}, u32[]{:S(2)}) async-start(bf16[16,32,2048]{2,1,0:T(8,128)(2,1)} %bitcast.21), calls=%async_computation.2 | async-start | bytes 4194304 | tf_op jit(solution)/shard_map/all_to_all | solution.py:469
  101.6 1.6 copy-start.2
  111.4 1.3 copy-start.1
  130.6 33.6 %all-to-all-start.5 = ((bf16[16,32,2048]{2,1,0:T(8,128)(2,1)}), bf16[16,32,2048]{2,1,0:T(8,128)(2,1)}, u32[]{:S(2)}, u32[]{:S(2)}) async-start(bf16[16,32,2048]{2,1,0:T(8,128)(2,1)} %copy-done.1), calls=%async_computation.5 | async-start | bytes 4194304 | tf_op jit(solution)/shard_map/all_to_all | solution.py:469
  143.3 1.3 copy-start
  164.2 44.9 %all-to-all-start.3 = ((bf16[16,32,2048]{2,1,0:T(8,128)(2,1)}), bf16[16,32,2048]{2,1,0:T(8,128)(2,1)S(1)}, u32[]{:S(2)}, u32[]{:S(2)}) async-start(bf16[16,32,2048]{2,1,0:T(8,128)(2,1)} %copy-done), calls=%async_computation.3 | async-start | bytes 4194304 | tf_op jit(solution)/shard_map/all_to_all | solution.py:469
  172.6 36.5 %collective-permute-start.1 = (bf16[128,2048]{1,0:T(8,128)(2,1)}, bf16[128,2048]{1,0:T(8,128)(2,1)S(1)}, u32[]{:S(2)}, u32[]{:S(2)}) collective-permute-start(bf16[128,2048]{1,0:T(8,128)(2,1)} %shard_map.179), channel_id=1, source_target_pairs={{0,16},{4,20},{8,24},{12,28},{16,0},{20,4},{24,8},{28,12},{1,17},{... | collective-permute-start | bytes 1572872 | tf_op jit(solution)/shard_map/ppermute | solution.py:548
  173.4 35.7 %copy-start.4 = (bf16[256,512]{1,0:T(8,128)(2,1)S(1)}, bf16[256,512]{1,0:T(8,128)(2,1)}, u32[]{:S(2)}) copy-start(bf16[256,512]{1,0:T(8,128)(2,1)} %get-tuple-element.16.weight_in) | copy-start | bytes 786436
  209.1 1.2 copy-start.3

commit v7 on v6

--- a/solution.py
+++ b/solution.py
@@ -16,6 +16,35 @@
 eps_norm = 1e-06
 decay_running = 16.0
 routed_scale = 2.5
+
+
+def start_all(pairs, sems):
+    copies = [pltpu.make_async_copy(src, dst, sems.at[i]) for i, (src, dst) in enumerate(pairs)]
+    for copy in copies:
+        copy.start()
+    return copies
+
+
+def pieces_of(rows, count):
+    return [pl.ds(i * (rows // count), rows // count) for i in range(count)]
+
+
+def streamed(kernel, out, args, scratch, copies, scalars=0, room=None):
+    anywhere = pl.BlockSpec(memory_space=pl.ANY)
+    smem = pl.BlockSpec(memory_space=pltpu.SMEM)
+    return pl.pallas_call(
+        kernel,
+        in_specs=[smem] * scalars + [anywhere] * (len(args) - scalars),
+        out_specs=jax.tree.map(lambda _: anywhere, out),
+        out_shape=out,
+        scratch_shapes=[pltpu.VMEM(x.shape, x.dtype) for x in scratch]
+        + [pltpu.SemaphoreType.DMA((copies,))],
+        compiler_params=pltpu.CompilerParams(vmem_limit_bytes=room),
+    )(*args)
+
+
+PIECES = 4
+DEEP = 2
 
 
 def lane_head(shape):
@@ -92,17 +121,55 @@
 
 
 def mixer_kernel(
-    place_ref, q_ref, k_ref, v_ref, within_ref, starts_ref, msg_ref, gate_ref, gain_ref, out_ref
+    place_ref,
+    gain_in,
+    msg_in,
+    q_in,
+    k_in,
+    v_in,
+    within_in,
+    gate_in,
+    starts_in,
+    out_ref,
+    gain_ref,
+    msg_ref,
+    q_ref,
+    k_ref,
+    v_ref,
+    within_ref,
+    gate_ref,
+    starts_ref,
+    done_ref,
+    sems,
 ):
     rows, width = k_ref.shape
     heads = width // KEY_CHANNELS
     vdim = v_ref.shape[1] // heads
+    blocks = rows // BLOCK
+    each = blocks // PIECES
+    by_rows = pieces_of(rows, PIECES)
+    pairs = [(msg_in, msg_ref), (gain_in, gain_ref)]
+    for p, at in enumerate(by_rows):
+        for src, dst in (
+            (q_in, q_ref),
+            (k_in, k_ref),
+            (v_in, v_ref),
+            (within_in, within_ref),
+            (gate_in, gate_ref),
+        ):
+            pairs.append((src.at[at, :], dst.at[at, :]))
+        part = pl.ds(p * each, each)
+        pairs.append((starts_in.at[part], starts_ref.at[part]))
+    loads = start_all(pairs, sems)
+    per_piece = 6
 
     def hop(j, carried):
         message = msg_ref[j].astype(jnp.float32)
         factor = message[vdim : vdim + 1] + message[vdim + 1 : vdim + 2]
         return carried * factor + message[:vdim]
 
+    loads[0].wait()
+    loads[1].wait()
     carried = lax.fori_loop(0, place_ref[0], hop, jnp.zeros((vdim, width), jnp.float32))
     head_of = lane_head((BLOCK, width))
     causal = lax.broadcasted_iota(jnp.int32, (heads * BLOCK, BLOCK), 0) % BLOCK >= (
@@ -110,7 +177,12 @@
     )
     gain = gain_ref[...]
     before = jnp.zeros((1, width), jnp.float32)
-    for n in range(rows // BLOCK):
+    stores = []
+    for n in range(blocks):
+        if n % each == 0:
+            first = 2 + n // each * per_piece
+            for copy in loads[first : first + per_piece]:
+                copy.wait()
         at = slice(n * BLOCK, (n + 1) * BLOCK)
         within = within_ref[at, :]
         queries = q_ref[at, :].astype(jnp.float32) * (KEY_CHANNELS**-0.5) * jnp.exp(within)
@@ -134,10 +206,22 @@
             )
             scale = lax.rsqrt(jnp.mean(output * output, axis=-1, keepdims=True) + eps_norm)
             gate = gate_ref[at, cols].astype(jnp.float32)
-            out_ref[at, cols] = (
+            done_ref[at, cols] = (
                 output * scale * gain * (gate / (1.0 + jnp.exp(-gate)))
             ).astype(jnp.bfloat16)
         before = before + within[BLOCK - 1 : BLOCK]
+        if (n + 1) % each == 0:
+            p = n // each
+            stores.append(
+                pltpu.make_async_copy(
+                    done_ref.at[by_rows[p], :],
+                    out_ref.at[by_rows[p], :],
+                    sems.at[len(loads) + p],
+                )
+            )
+            stores[-1].start()
+    for copy in stores:
+        copy.wait()
 
 
 def whole(x, loose=False):
@@ -291,33 +375,6 @@
     return jnp.dot(held, rows, preferred_element_type=jnp.float32).astype(jnp.bfloat16)
 
 
-def start_all(pairs, sems):
-    copies = [pltpu.make_async_copy(src, dst, sems.at[i]) for i, (src, dst) in enumerate(pairs)]
-    for copy in copies:
-        copy.start()
-    return copies
-
-
-def pieces_of(rows, count):
-    return [pl.ds(i * (rows // count), rows // count) for i in range(count)]
-
-
-def streamed(kernel, out, args, scratch, copies, room=None):
-    anywhere = pl.BlockSpec(memory_space=pl.ANY)
-    return pl.pallas_call(
-        kernel,
-        in_specs=[anywhere] * len(args),
-        out_specs=jax.tree.map(lambda _: anywhere, out),
-        out_shape=out,
-        scratch_shapes=[pltpu.VMEM(x.shape, x.dtype) for x in scratch]
-        + [pltpu.SemaphoreType.DMA((copies,))],
-        compiler_params=pltpu.CompilerParams(vmem_limit_bytes=room),
-    )(*args)
-
-
-PIECES = 4
-
-
 def store_slots(held, normed, sent, sent_out, sems, first):
     copies = []
     for i, at in enumerate(pieces_of(sent.shape[0], PIECES)):
@@ -340,7 +397,7 @@
 def pack(held, rows):
     out = jax.ShapeDtypeStruct((held.shape[0], rows.shape[1]), rows.dtype)
     args = (held, rows)
-    return streamed(pack_kernel, out, args, args + (out,), 2 + PIECES, ROOM)
+    return streamed(pack_kernel, out, args, args + (out,), 2 + PIECES, room=ROOM)
 
 
 def project_kernel(
@@ -393,7 +450,7 @@
     extra = refs[more + 3 : 2 * more + 3]
     done, sems = refs[2 * more + 3 :]
     tokens = done.shape[0]
-    pieces = pieces_of(results.shape[0], PIECES)
+    pieces = pieces_of(results.shape[0], DEEP)
     loads = start_all(
         [(weight_in, weight)]
         + [(results_in.at[at, :], results.at[at, :]) for at in pieces]
@@ -407,7 +464,7 @@
         part = jnp.dot(weight[:, at], results[at, :], preferred_element_type=jnp.float32)
         total = part if total is None else total + part
     total = total[:tokens] + total[tokens:]
-    for copy, ref in zip(loads[1 + PIECES :], extra):
+    for copy, ref in zip(loads[1 + DEEP :], extra):
         copy.wait()
         total = total + ref[...].astype(jnp.float32)
     done[...] = total.astype(jnp.bfloat16)
@@ -423,8 +480,8 @@
         out,
         args,
         args + (out,),
-        2 + PIECES + len(more),
-        ROOM if more else None,
+        2 + DEEP + len(more),
+        room=ROOM if more else None,
     )
 
 
@@ -503,20 +560,25 @@
         scores_t,
     )
     arrived = lax.all_to_all(message, "sp", split_axis=0, concat_axis=0, tiled=True)
-    gated = call(
-        mixer_kernel,
-        like(value_matrix.shape),
+    gated_args = (
         place.reshape(1),
+        head_norm_gain.reshape(1, vdim),
+        arrived,
         queries,
         key_matrix,
         value_matrix,
         within,
+        output_gate_input,
         starts,
-        arrived,
-        output_gate_input,
-        head_norm_gain.reshape(1, vdim),
+    )
+    gated_like = like(value_matrix.shape)
+    gated = streamed(
+        mixer_kernel,
+        gated_like,
+        gated_args,
+        gated_args[1:] + (gated_like,),
+        2 + 7 * PIECES,
         scalars=1,
-        loose=(5,),
     )
     stacked = gated.reshape(heads_axis, tok_count, gated.shape[1])
     stacked = lax.all_to_all(stacked, "tp", split_axis=0, concat_axis=0, tiled=True)

time: 214 us -> 214 us (level)
    pallas_call x2 -> x1, Pallas kernels: 7.3 us -> 4.25 us  [call(): pl.pallas_call(kernel, grid=(1,), in_specs=in_specs, out_specs=jax.tree.m...]
    pallas_call x4 -> x5, Pallas kernels: 12.4 us -> 15.2 us  [streamed(): pl.pallas_call(kernel, in_specs=[smem] * scalars + [anywhere] * (len(args...]
where the time goes in v7:
time: 214 us; the launch traced here: 213 us
  waiting for transfers between devices  105 us (49%)
  Pallas kernels  43.7 us (20%)
  blocking collectives  30.7 us (14%)
  starting transfers between devices  25.8 us (12%)
  local copies, waits for them, and re-layouts  6.9 us (3%)
    all_to_all x3, waiting for transfers between devices, spread(): lax.all_to_all(rows.reshape(half, exp_dev * cap, width), axes, split_axis...  68.2 us
    all_to_all x1, blocking collectives, spread(): lax.all_to_all(rows.reshape(half, exp_dev * cap, width), axes, split_axis...  30.7 us
    ppermute x1, waiting for transfers between devices, on_device(): normed_far = lax.ppermute(normed, 'sp', swap)  24.7 us
    pallas_call x3, Pallas kernels, ffn(): pl.pallas_call(ffn_kernel, grid=(count, steps), in_specs=in_specs, out_sp...  21.5 us
    pallas_call x5, Pallas kernels, streamed(): pl.pallas_call(kernel, in_specs=[smem] * scalars + [anywhere] * (len(args...  15.2 us
    all_to_all x3, starting transfers between devices, spread(): lax.all_to_all(rows.reshape(half, exp_dev * cap, width), axes, split_axis...  13.1 us
    all_to_all x1, waiting for transfers between devices, on_device(): lax.all_to_all(message, 'sp', split_axis=0, concat_axis=0, tiled=True)  9.61 us
    all_to_all x1, starting transfers between devices, on_device(): lax.all_to_all(message, 'sp', split_axis=0, concat_axis=0, tiled=True)  7.31 us
  transfers between devices with their start and end apart: 7, of which 6 were waited for; matrix products, arithmetic and copies ran while one was open for 0% of the time, Pallas kernels for 13%

profile of v7, /device:TPU:0, one launch (start us, length us, event | category | flops | bytes accessed | tf_op | source)
XLA Modules:
  0.0 213.0 jit_solution(13620705460310013444)
XLA Ops:
  0.0 4.3 %shard_map.172 = (f32[512,128]{1,0:T(8,128)}, f32[8,128,128]{2,1,0:T(8,128)}, bf16[8,144,128]{2,1,0:T(8,128)(2,1)}) custom-call(bf16[512,128]{1,0:T(8,128)(2,1)} %k_in.1, bf16[512,256]{1,0:T(8,128)(2,1)} %v_in.1, bf16[512,128]{1,0:T(8,128)(2,1)} %c_ref.1, f32[2,512]{1,0:T(2,128)} %bitcast.32, s32[4,128]{1,0:T(4,128)} %bitcast.28, f32[4,128]{1,0:T(4,128)} %bitcast.30), custom_call_target="tpu_custom_call" | custom-call | tf_op jit(solution)/shard_map/pallas_call | solution.py:239
  4.3 7.3 %all-to-all-start = ((bf16[8,144,128]{2,1,0:T(8,128)(2,1)}), bf16[8,144,128]{2,1,0:T(8,128)(2,1)S(1)}, u32[]{:S(2)}, u32[]{:S(2)}) async-start(bf16[8,144,128]{2,1,0:T(8,128)(2,1)} %get-tuple-element.15), calls=%async_computation | async-start | bytes 589824 | tf_op jit(solution)/shard_map/all_to_all | solution.py:562
  11.6 9.6 %all-to-all-done.far_ref.msg_in = bf16[8,144,128]{2,1,0:T(8,128)(2,1)S(1)} async-done(((bf16[8,144,128]{2,1,0:T(8,128)(2,1)}), bf16[8,144,128]{2,1,0:T(8,128)(2,1)S(1)}, u32[]{:S(2)}, u32[]{:S(2)}) %all-to-all-start) | async-done | bytes 294944 | tf_op jit(solution)/shard_map/all_to_all | solution.py:562
  21.2 0.7 copy-done.6
  21.9 3.6 %shard_map.173 = bf16[512,256]{1,0:T(8,128)(2,1)} custom-call(s32[1]{0:T(128)} %bitcast.5.place_ref, f32[1,128]{1,0:T(1,128)} %bitcast.33, bf16[8,144,128]{2,1,0:T(8,128)(2,1)} %copy-done.6, bf16[512,128]{1,0:T(8,128)(2,1)} %q_in.1, bf16[512,128]{1,0:T(8,128)(2,1)} %k_in.1, bf16[512,256]{1,0:T(8,128)(2,1)} %v_in.1, f32[512,128]{1,0:T(8,128)} %get-tuple-element.17.within_in, ...), custom_call_target="tpu_custom_call" | custom-call | tf_op jit(solution)/shard_map/pallas_call | solution.py:35
  25.5 3.4 %all-to-all-start.1 = ((bf16[4,128,256]{2,1,0:T(8,128)(2,1)}), bf16[4,128,256]{2,1,0:T(8,128)(2,1)S(1)}, u32[]{:S(2)}, u32[]{:S(2)}) async-start(bf16[4,128,256]{2,1,0:T(8,128)(2,1)} %bitcast.25), calls=%async_computation.1 | async-start | bytes 524288 | tf_op jit(solution)/shard_map/all_to_all | solution.py:584
  29.0 0.6 pad_add_fusion.place_ref
  29.6 2.7 %tables.1 = (bf16[512,128]{1,0:T(8,128)(2,1)}, bf16[256,512]{1,0:T(8,128)(2,1)}, bf16[512,128]{1,0:T(8,128)(2,1)}, bf16[256,512]{1,0:T(8,128)(2,1)}) custom-call(s32[2]{0:T(128)} %pad_add_fusion.place_ref, s32[4,128]{1,0:T(4,128)} %bitcast.29, f32[4,128]{1,0:T(4,128)} %bitcast.31, bf16[8,144,128]{2,1,0:T(8,128)(2,1)} %copy-done.6), custom_call_target="tpu_custom_call" | custom-call | tf_op jit(solution)/shard_map/tables/pallas_call | solution.py:355
  32.4 2.6 %all-to-all-done.1.g_in = bf16[4,128,256]{2,1,0:T(8,128)(2,1)S(1)} async-done(((bf16[4,128,256]{2,1,0:T(8,128)(2,1)}), bf16[4,128,256]{2,1,0:T(8,128)(2,1)S(1)}, u32[]{:S(2)}, u32[]{:S(2)}) %all-to-all-start.1) | async-done | bytes 262176 | tf_op jit(solution)/shard_map/all_to_all | solution.py:584
  34.9 0.7 copy-done.7
  35.7 4.8 %shard_map.174 = (bf16[512,2048]{1,0:T(8,128)(2,1)}, bf16[128,2048]{1,0:T(8,128)(2,1)}, bf16[128,2048]{1,0:T(8,128)(2,1)}) custom-call(bf16[4,128,256]{2,1,0:T(8,128)(2,1)} %copy-done.7, bf16[1024,2048]{1,0:T(8,128)(2,1)} %w_in.1, bf16[128,2048]{1,0:T(8,128)(2,1)} %res_in.1, f32[1,2048]{1,0:T(1,128)} %bitcast.27, bf16[512,128]{1,0:T(8,128)(2,1)} %get-tuple-element.19.held_in), custom_call_target="tpu_custom_call" | custom-call | tf_op jit(solution)/shard_map/pallas_call | solution.py:35
  40.4 1.1 collective-permute-start
  41.6 24.7 %collective-permute-done.rows_in = bf16[128,2048]{1,0:T(8,128)(2,1)S(1)} collective-permute-done((bf16[128,2048]{1,0:T(8,128)(2,1)}, bf16[128,2048]{1,0:T(8,128)(2,1)S(1)}, u32[]{:S(2)}, u32[]{:S(2)}) %collective-permute-start) | collective-permute-done | bytes 524320 | tf_op jit(solution)/shard_map/ppermute | solution.py:601
  66.2 1.5 shard_map.177
  67.8 30.7 %all_to_all.30.x_ref = bf16[16,32,2048]{2,1,0:T(8,128)(2,1)} all-to-all(bf16[16,32,2048]{2,1,0:T(8,128)(2,1)S(1)} %bitcast.19), channel_id=1, replica_groups={{0,1,2,3,4,5,6,7,8,9,10,11,12,13,14,15},{16,17,18,19,20,21,22,23,24,25,..., dimensions={0} | all-to-all | bytes 4194304 | tf_op jit(solution)/shard_map/all_to_all | solution.py:526
  98.5 3.7 %all-to-all-start.2 = ((bf16[16,32,2048]{2,1,0:T(8,128)(2,1)}), bf16[16,32,2048]{2,1,0:T(8,128)(2,1)S(1)}, u32[]{:S(2)}, u32[]{:S(2)}) async-start(bf16[16,32,2048]{2,1,0:T(8,128)(2,1)} %bitcast.21), calls=%async_computation.2 | async-start | bytes 4194304 | tf_op jit(solution)/shard_map/all_to_all | solution.py:526
  102.2 1.6 copy-done.2
  103.8 8.2 %shard_map.178 = bf16[16,32,2048]{2,1,0:T(8,128)(2,1)S(1)} custom-call(bf16[16,32,2048]{2,1,0:T(8,128)(2,1)S(1)} %copy-done.2, bf16[2,2048,512]{2,1,0:T(8,128)(2,1)} %gate_ref.3, bf16[2,2048,512]{2,1,0:T(8,128)(2,1)} %up_ref.3, bf16[2,512,2048]{2,1,0:T(8,128)(2,1)} %down_ref.3), custom_call_target="tpu_custom_call" | custom-call | flops 3221225472 | bytes 16777216 | tf_op jit(solution)/shard_map/pallas_call | solution.py:295
  112.0 1.3 copy-done.1
  113.3 17.9 %all-to-all-done.2.x_ref = bf16[16,32,2048]{2,1,0:T(8,128)(2,1)S(1)} async-done(((bf16[16,32,2048]{2,1,0:T(8,128)(2,1)}), bf16[16,32,2048]{2,1,0:T(8,128)(2,1)S(1)}, u32[]{:S(2)}, u32[]{:S(2)}) %all-to-all-start.2) | async-done | bytes 2097184 | tf_op jit(solution)/shard_map/all_to_all | solution.py:526
  131.2 4.5 %all-to-all-start.5 = ((bf16[16,32,2048]{2,1,0:T(8,128)(2,1)}), bf16[16,32,2048]{2,1,0:T(8,128)(2,1)}, u32[]{:S(2)}, u32[]{:S(2)}) async-start(bf16[16,32,2048]{2,1,0:T(8,128)(2,1)} %copy-done.1), calls=%async_computation.5 | async-start | bytes 4194304 | tf_op jit(solution)/shard_map/all_to_all | solution.py:526
  135.7 8.2 %shard_map.175 = bf16[16,32,2048]{2,1,0:T(8,128)(2,1)S(1)} custom-call(bf16[16,32,2048]{2,1,0:T(8,128)(2,1)S(1)} %all-to-all-done.2.x_ref, bf16[2,2048,512]{2,1,0:T(8,128)(2,1)} %gate_ref.3, bf16[2,2048,512]{2,1,0:T(8,128)(2,1)} %up_ref.3, bf16[2,512,2048]{2,1,0:T(8,128)(2,1)} %down_ref.3), custom_call_target="tpu_custom_call" | custom-call | flops 3221225472 | bytes 16777216 | tf_op jit(solution)/shard_map/pallas_call | solution.py:295
  143.9 1.3 copy-done
  145.2 19.6 %all-to-all-done.5 = bf16[16,32,2048]{2,1,0:T(8,128)(2,1)} async-done(((bf16[16,32,2048]{2,1,0:T(8,128)(2,1)}), bf16[16,32,2048]{2,1,0:T(8,128)(2,1)}, u32[]{:S(2)}, u32[]{:S(2)}) %all-to-all-start.5) | async-done | bytes 2097184 | tf_op jit(solution)/shard_map/all_to_all | solution.py:526
  164.8 4.9 %all-to-all-start.3 = ((bf16[16,32,2048]{2,1,0:T(8,128)(2,1)}), bf16[16,32,2048]{2,1,0:T(8,128)(2,1)S(1)}, u32[]{:S(2)}, u32[]{:S(2)}) async-start(bf16[16,32,2048]{2,1,0:T(8,128)(2,1)} %copy-done), calls=%async_computation.3 | async-start | bytes 4194304 | tf_op jit(solution)/shard_map/all_to_all | solution.py:526
  169.7 3.2 %shard_map.179 = bf16[128,2048]{1,0:T(8,128)(2,1)} custom-call(bf16[256,512]{1,0:T(8,128)(2,1)} %get-tuple-element.23.weight_in, bf16[512,2048]{1,0:T(8,128)(2,1)} %bitcast.17.results_in), custom_call_target="tpu_custom_call" | custom-call | tf_op jit(solution)/shard_map/pallas_call | solution.py:35
  172.9 0.8 collective-permute-start.1
  173.7 5.2 %shard_map.176 = f32[1,128,2048]{2,1,0:T(8,128)} custom-call(bf16[1,128,2048]{2,1,0:T(8,128)(2,1)} %bitcast.26, bf16[1,2048,512]{2,1,0:T(8,128)(2,1)} %bitcast.22, bf16[1,2048,512]{2,1,0:T(8,128)(2,1)} %bitcast.23, bf16[1,512,2048]{2,1,0:T(8,128)(2,1)} %bitcast.24, bf16[128,2048]{1,0:T(8,128)(2,1)} %get-tuple-element.22.rest_0_), custom_call_target="tpu_custom_call" | custom-call | flops 805306368 | bytes 7340032 | tf_op jit(solution)/shard_map/pallas_call | solution.py:295
  178.9 30.7 %all-to-all-done.3 = bf16[16,32,2048]{2,1,0:T(8,128)(2,1)S(1)} async-done(((bf16[16,32,2048]{2,1,0:T(8,128)(2,1)}), bf16[16,32,2048]{2,1,0:T(8,128)(2,1)S(1)}, u32[]{:S(2)}, u32[]{:S(2)}) %all-to-all-start.3) | async-done | bytes 2097184 | tf_op jit(solution)/shard_map/all_to_all | solution.py:526
  209.6 0.0 collective-permute-done.1.refs_1_
  209.7 1.2 copy-done.3
  210.9 2.1 shard_map.180
  (10 shorter events, 0.0 us)
Async XLA Ops:
  4.3 16.9 %all-to-all-start = ((bf16[8,144,128]{2,1,0:T(8,128)(2,1)}), bf16[8,144,128]{2,1,0:T(8,128)(2,1)S(1)}, u32[]{:S(2)}, u32[]{:S(2)}) async-start(bf16[8,144,128]{2,1,0:T(8,128)(2,1)} %get-tuple-element.15), calls=%async_computation | async-start | bytes 589824 | tf_op jit(solution)/shard_map/all_to_all | solution.py:562
  21.2 0.7 copy-start.6
  25.5 9.4 %all-to-all-start.1 = ((bf16[4,128,256]{2,1,0:T(8,128)(2,1)}), bf16[4,128,256]{2,1,0:T(8,128)(2,1)S(1)}, u32[]{:S(2)}, u32[]{:S(2)}) async-start(bf16[4,128,256]{2,1,0:T(8,128)(2,1)} %bitcast.25), calls=%async_computation.1 | async-start | bytes 524288 | tf_op jit(solution)/shard_map/all_to_all | solution.py:584
  34.9 0.7 copy-start.7
  35.6 30.6 %copy-start.5 = (bf16[512,128]{1,0:T(8,128)(2,1)S(1)}, bf16[512,128]{1,0:T(8,128)(2,1)}, u32[]{:S(2)}) copy-start(bf16[512,128]{1,0:T(8,128)(2,1)} %get-tuple-element.24.held_in) | copy-start | bytes 393220
  40.4 25.8 %collective-permute-start = (bf16[128,2048]{1,0:T(8,128)(2,1)}, bf16[128,2048]{1,0:T(8,128)(2,1)S(1)}, u32[]{:S(2)}, u32[]{:S(2)}) collective-permute-start(bf16[128,2048]{1,0:T(8,128)(2,1)} %get-tuple-element.21), channel_id=1, source_target_pairs={{0,16},{4,20},{8,24},{12,28},{16,0},{20,4},{24,8},{28,12},{1,17},{... | collective-permute-start | bytes 1572872 | tf_op jit(solution)/shard_map/ppermute | solution.py:601
  98.5 32.8 %all-to-all-start.2 = ((bf16[16,32,2048]{2,1,0:T(8,128)(2,1)}), bf16[16,32,2048]{2,1,0:T(8,128)(2,1)S(1)}, u32[]{:S(2)}, u32[]{:S(2)}) async-start(bf16[16,32,2048]{2,1,0:T(8,128)(2,1)} %bitcast.21), calls=%async_computation.2 | async-start | bytes 4194304 | tf_op jit(solution)/shard_map/all_to_all | solution.py:526
  102.2 1.6 copy-start.2
  111.9 1.3 copy-start.1
  131.2 33.6 %all-to-all-start.5 = ((bf16[16,32,2048]{2,1,0:T(8,128)(2,1)}), bf16[16,32,2048]{2,1,0:T(8,128)(2,1)}, u32[]{:S(2)}, u32[]{:S(2)}) async-start(bf16[16,32,2048]{2,1,0:T(8,128)(2,1)} %copy-done.1), calls=%async_computation.5 | async-start | bytes 4194304 | tf_op jit(solution)/shard_map/all_to_all | solution.py:526
  143.9 1.3 copy-start
  164.8 44.9 %all-to-all-start.3 = ((bf16[16,32,2048]{2,1,0:T(8,128)(2,1)}), bf16[16,32,2048]{2,1,0:T(8,128)(2,1)S(1)}, u32[]{:S(2)}, u32[]{:S(2)}) async-start(bf16[16,32,2048]{2,1,0:T(8,128)(2,1)} %copy-done), calls=%async_computation.3 | async-start | bytes 4194304 | tf_op jit(solution)/shard_map/all_to_all | solution.py:526
  172.9 36.7 %collective-permute-start.1 = (bf16[128,2048]{1,0:T(8,128)(2,1)}, bf16[128,2048]{1,0:T(8,128)(2,1)S(1)}, u32[]{:S(2)}, u32[]{:S(2)}) collective-permute-start(bf16[128,2048]{1,0:T(8,128)(2,1)} %shard_map.179), channel_id=1, source_target_pairs={{0,16},{4,20},{8,24},{12,28},{16,0},{20,4},{24,8},{28,12},{1,17},{... | collective-permute-start | bytes 1572872 | tf_op jit(solution)/shard_map/ppermute | solution.py:610
  173.7 35.9 %copy-start.4 = (bf16[256,512]{1,0:T(8,128)(2,1)S(1)}, bf16[256,512]{1,0:T(8,128)(2,1)}, u32[]{:S(2)}) copy-start(bf16[256,512]{1,0:T(8,128)(2,1)} %get-tuple-element.16.weight_in) | copy-start | bytes 786436
  209.7 1.2 copy-start.3

commit v8 on v6

--- a/solution.py
+++ b/solution.py
@@ -16,6 +16,35 @@
 eps_norm = 1e-06
 decay_running = 16.0
 routed_scale = 2.5
+
+
+def start_all(pairs, sems):
+    copies = [pltpu.make_async_copy(src, dst, sems.at[i]) for i, (src, dst) in enumerate(pairs)]
+    for copy in copies:
+        copy.start()
+    return copies
+
+
+def pieces_of(rows, count):
+    return [pl.ds(i * (rows // count), rows // count) for i in range(count)]
+
+
+def streamed(kernel, out, args, scratch, copies, scalars=0, room=None):
+    anywhere = pl.BlockSpec(memory_space=pl.ANY)
+    smem = pl.BlockSpec(memory_space=pltpu.SMEM)
+    return pl.pallas_call(
+        kernel,
+        in_specs=[smem] * scalars + [anywhere] * (len(args) - scalars),
+        out_specs=jax.tree.map(lambda _: anywhere, out),
+        out_shape=out,
+        scratch_shapes=[pltpu.VMEM(x.shape, x.dtype) for x in scratch]
+        + [pltpu.SemaphoreType.DMA((copies,))],
+        compiler_params=pltpu.CompilerParams(vmem_limit_bytes=room),
+    )(*args)
+
+
+PIECES = 4
+DEEP = 2
 
 
 def lane_head(shape):
@@ -291,33 +320,6 @@
     return jnp.dot(held, rows, preferred_element_type=jnp.float32).astype(jnp.bfloat16)
 
 
-def start_all(pairs, sems):
-    copies = [pltpu.make_async_copy(src, dst, sems.at[i]) for i, (src, dst) in enumerate(pairs)]
-    for copy in copies:
-        copy.start()
-    return copies
-
-
-def pieces_of(rows, count):
-    return [pl.ds(i * (rows // count), rows // count) for i in range(count)]
-
-
-def streamed(kernel, out, args, scratch, copies, room=None):
-    anywhere = pl.BlockSpec(memory_space=pl.ANY)
-    return pl.pallas_call(
-        kernel,
-        in_specs=[anywhere] * len(args),
-        out_specs=jax.tree.map(lambda _: anywhere, out),
-        out_shape=out,
-        scratch_shapes=[pltpu.VMEM(x.shape, x.dtype) for x in scratch]
-        + [pltpu.SemaphoreType.DMA((copies,))],
-        compiler_params=pltpu.CompilerParams(vmem_limit_bytes=room),
-    )(*args)
-
-
-PIECES = 4
-
-
 def store_slots(held, normed, sent, sent_out, sems, first):
     copies = []
     for i, at in enumerate(pieces_of(sent.shape[0], PIECES)):
@@ -340,7 +342,7 @@
 def pack(held, rows):
     out = jax.ShapeDtypeStruct((held.shape[0], rows.shape[1]), rows.dtype)
     args = (held, rows)
-    return streamed(pack_kernel, out, args, args + (out,), 2 + PIECES, ROOM)
+    return streamed(pack_kernel, out, args, args + (out,), 2 + PIECES, room=ROOM)
 
 
 def project_kernel(
@@ -393,7 +395,7 @@
     extra = refs[more + 3 : 2 * more + 3]
     done, sems = refs[2 * more + 3 :]
     tokens = done.shape[0]
-    pieces = pieces_of(results.shape[0], PIECES)
+    pieces = pieces_of(results.shape[0], DEEP)
     loads = start_all(
         [(weight_in, weight)]
         + [(results_in.at[at, :], results.at[at, :]) for at in pieces]
@@ -407,7 +409,7 @@
         part = jnp.dot(weight[:, at], results[at, :], preferred_element_type=jnp.float32)
         total = part if total is None else total + part
     total = total[:tokens] + total[tokens:]
-    for copy, ref in zip(loads[1 + PIECES :], extra):
+    for copy, ref in zip(loads[1 + DEEP :], extra):
         copy.wait()
         total = total + ref[...].astype(jnp.float32)
     done[...] = total.astype(jnp.bfloat16)
@@ -423,8 +425,8 @@
         out,
         args,
         args + (out,),
-        2 + PIECES + len(more),
-        ROOM if more else None,
+        2 + DEEP + len(more),
+        room=ROOM if more else None,
     )
 
 

time: 214 us -> 213 us (level)
  no operation moved by 1% of the time
where the time goes in v8:
time: 213 us; the launch traced here: 212 us
  waiting for transfers between devices  105 us (49%)
  Pallas kernels  43.2 us (20%)
  blocking collectives  30.7 us (14%)
  starting transfers between devices  25.8 us (12%)
  local copies, waits for them, and re-layouts  6.9 us (3%)
    all_to_all x3, waiting for transfers between devices, spread(): lax.all_to_all(rows.reshape(half, exp_dev * cap, width), axes, split_axis...  68.2 us
    all_to_all x1, blocking collectives, spread(): lax.all_to_all(rows.reshape(half, exp_dev * cap, width), axes, split_axis...  30.7 us
    ppermute x1, waiting for transfers between devices, on_device(): normed_far = lax.ppermute(normed, 'sp', swap)  24.6 us
    pallas_call x3, Pallas kernels, ffn(): pl.pallas_call(ffn_kernel, grid=(count, steps), in_specs=in_specs, out_sp...  21.6 us
    all_to_all x3, starting transfers between devices, spread(): lax.all_to_all(rows.reshape(half, exp_dev * cap, width), axes, split_axis...  13.1 us
    pallas_call x4, Pallas kernels, streamed(): pl.pallas_call(kernel, in_specs=[smem] * scalars + [anywhere] * (len(args...  11.6 us
    all_to_all x1, waiting for transfers between devices, on_device(): lax.all_to_all(message, 'sp', split_axis=0, concat_axis=0, tiled=True)  9.61 us
    all_to_all x1, starting transfers between devices, on_device(): lax.all_to_all(message, 'sp', split_axis=0, concat_axis=0, tiled=True)  7.31 us
  transfers between devices with their start and end apart: 7, of which 6 were waited for; matrix products, arithmetic and copies ran while one was open for 0% of the time, Pallas kernels for 13%

profile of v8, /device:TPU:0, one launch (start us, length us, event | category | flops | bytes accessed | tf_op | source)
XLA Modules:
  0.0 212.4 jit_solution(4395153070182537212)
XLA Ops:
  0.0 4.3 %shard_map.172 = (f32[512,128]{1,0:T(8,128)}, f32[8,128,128]{2,1,0:T(8,128)}, bf16[8,144,128]{2,1,0:T(8,128)(2,1)}) custom-call(bf16[512,128]{1,0:T(8,128)(2,1)} %k_ref.3, bf16[512,256]{1,0:T(8,128)(2,1)} %v_ref.3, bf16[512,128]{1,0:T(8,128)(2,1)} %c_ref.1, f32[2,512]{1,0:T(2,128)} %bitcast.32, s32[4,128]{1,0:T(4,128)} %bitcast.28, f32[4,128]{1,0:T(4,128)} %bitcast.30), custom_call_target="tpu_custom_call" | custom-call | tf_op jit(solution)/shard_map/pallas_call | solution.py:184
  4.3 7.3 %all-to-all-start = ((bf16[8,144,128]{2,1,0:T(8,128)(2,1)}), bf16[8,144,128]{2,1,0:T(8,128)(2,1)S(1)}, u32[]{:S(2)}, u32[]{:S(2)}) async-start(bf16[8,144,128]{2,1,0:T(8,128)(2,1)} %get-tuple-element.15), calls=%async_computation | async-start | bytes 589824 | tf_op jit(solution)/shard_map/all_to_all | solution.py:507
  11.6 9.6 %all-to-all-done.far_ref.msg_ref = bf16[8,144,128]{2,1,0:T(8,128)(2,1)S(1)} async-done(((bf16[8,144,128]{2,1,0:T(8,128)(2,1)}), bf16[8,144,128]{2,1,0:T(8,128)(2,1)S(1)}, u32[]{:S(2)}, u32[]{:S(2)}) %all-to-all-start) | async-done | bytes 294944 | tf_op jit(solution)/shard_map/all_to_all | solution.py:507
  21.2 0.7 copy-done.6
  21.9 3.0 %shard_map.173 = bf16[512,256]{1,0:T(8,128)(2,1)} custom-call(s32[1]{0:T(128)} %bitcast.5.place_ref, bf16[512,128]{1,0:T(8,128)(2,1)} %q_ref.1, bf16[512,128]{1,0:T(8,128)(2,1)} %k_ref.3, bf16[512,256]{1,0:T(8,128)(2,1)} %v_ref.3, f32[512,128]{1,0:T(8,128)} %get-tuple-element.17.within_ref, f32[8,128,128]{2,1,0:T(8,128)} %get-tuple-element.18.starts_ref, ...), custom_call_target="tpu_custom_call" | custom-call | tf_op jit(solution)/shard_map/pallas_call | solution.py:184
  24.9 3.4 %all-to-all-start.1 = ((bf16[4,128,256]{2,1,0:T(8,128)(2,1)}), bf16[4,128,256]{2,1,0:T(8,128)(2,1)S(1)}, u32[]{:S(2)}, u32[]{:S(2)}) async-start(bf16[4,128,256]{2,1,0:T(8,128)(2,1)} %bitcast.25), calls=%async_computation.1 | async-start | bytes 524288 | tf_op jit(solution)/shard_map/all_to_all | solution.py:524
  28.4 0.6 pad_add_fusion.place_ref
  29.0 2.7 %tables.1 = (bf16[512,128]{1,0:T(8,128)(2,1)}, bf16[256,512]{1,0:T(8,128)(2,1)}, bf16[512,128]{1,0:T(8,128)(2,1)}, bf16[256,512]{1,0:T(8,128)(2,1)}) custom-call(s32[2]{0:T(128)} %pad_add_fusion.place_ref, s32[4,128]{1,0:T(4,128)} %bitcast.29, f32[4,128]{1,0:T(4,128)} %bitcast.31, bf16[8,144,128]{2,1,0:T(8,128)(2,1)} %copy-done.6), custom_call_target="tpu_custom_call" | custom-call | tf_op jit(solution)/shard_map/tables/pallas_call | solution.py:300
  31.8 2.6 %all-to-all-done.1.g_in = bf16[4,128,256]{2,1,0:T(8,128)(2,1)S(1)} async-done(((bf16[4,128,256]{2,1,0:T(8,128)(2,1)}), bf16[4,128,256]{2,1,0:T(8,128)(2,1)S(1)}, u32[]{:S(2)}, u32[]{:S(2)}) %all-to-all-start.1) | async-done | bytes 262176 | tf_op jit(solution)/shard_map/all_to_all | solution.py:524
  34.3 0.7 copy-done.7
  35.0 4.8 %shard_map.174 = (bf16[512,2048]{1,0:T(8,128)(2,1)}, bf16[128,2048]{1,0:T(8,128)(2,1)}, bf16[128,2048]{1,0:T(8,128)(2,1)}) custom-call(bf16[4,128,256]{2,1,0:T(8,128)(2,1)} %copy-done.7, bf16[1024,2048]{1,0:T(8,128)(2,1)} %w_in.1, bf16[128,2048]{1,0:T(8,128)(2,1)} %res_in.1, f32[1,2048]{1,0:T(1,128)} %bitcast.27, bf16[512,128]{1,0:T(8,128)(2,1)} %get-tuple-element.19.held_in), custom_call_target="tpu_custom_call" | custom-call | tf_op jit(solution)/shard_map/pallas_call | solution.py:35
  39.8 1.2 collective-permute-start
  41.0 24.6 %collective-permute-done.rows_in = bf16[128,2048]{1,0:T(8,128)(2,1)S(1)} collective-permute-done((bf16[128,2048]{1,0:T(8,128)(2,1)}, bf16[128,2048]{1,0:T(8,128)(2,1)S(1)}, u32[]{:S(2)}, u32[]{:S(2)}) %collective-permute-start) | collective-permute-done | bytes 524320 | tf_op jit(solution)/shard_map/ppermute | solution.py:541
  65.6 1.5 shard_map.177
  67.1 30.7 %all_to_all.30.x_ref = bf16[16,32,2048]{2,1,0:T(8,128)(2,1)} all-to-all(bf16[16,32,2048]{2,1,0:T(8,128)(2,1)S(1)} %bitcast.19), channel_id=1, replica_groups={{0,1,2,3,4,5,6,7,8,9,10,11,12,13,14,15},{16,17,18,19,20,21,22,23,24,25,..., dimensions={0} | all-to-all | bytes 4194304 | tf_op jit(solution)/shard_map/all_to_all | solution.py:471
  97.8 3.7 %all-to-all-start.2 = ((bf16[16,32,2048]{2,1,0:T(8,128)(2,1)}), bf16[16,32,2048]{2,1,0:T(8,128)(2,1)S(1)}, u32[]{:S(2)}, u32[]{:S(2)}) async-start(bf16[16,32,2048]{2,1,0:T(8,128)(2,1)} %bitcast.21), calls=%async_computation.2 | async-start | bytes 4194304 | tf_op jit(solution)/shard_map/all_to_all | solution.py:471
  101.6 1.6 copy-done.2
  103.2 8.2 %shard_map.178 = bf16[16,32,2048]{2,1,0:T(8,128)(2,1)S(1)} custom-call(bf16[16,32,2048]{2,1,0:T(8,128)(2,1)S(1)} %copy-done.2, bf16[2,2048,512]{2,1,0:T(8,128)(2,1)} %gate_ref.5, bf16[2,2048,512]{2,1,0:T(8,128)(2,1)} %up_ref.3, bf16[2,512,2048]{2,1,0:T(8,128)(2,1)} %down_ref.3), custom_call_target="tpu_custom_call" | custom-call | flops 3221225472 | bytes 16777216 | tf_op jit(solution)/shard_map/pallas_call | solution.py:240
  111.4 1.3 copy-done.1
  112.7 17.9 %all-to-all-done.2.x_ref = bf16[16,32,2048]{2,1,0:T(8,128)(2,1)S(1)} async-done(((bf16[16,32,2048]{2,1,0:T(8,128)(2,1)}), bf16[16,32,2048]{2,1,0:T(8,128)(2,1)S(1)}, u32[]{:S(2)}, u32[]{:S(2)}) %all-to-all-start.2) | async-done | bytes 2097184 | tf_op jit(solution)/shard_map/all_to_all | solution.py:471
  130.6 4.5 %all-to-all-start.5 = ((bf16[16,32,2048]{2,1,0:T(8,128)(2,1)}), bf16[16,32,2048]{2,1,0:T(8,128)(2,1)}, u32[]{:S(2)}, u32[]{:S(2)}) async-start(bf16[16,32,2048]{2,1,0:T(8,128)(2,1)} %copy-done.1), calls=%async_computation.5 | async-start | bytes 4194304 | tf_op jit(solution)/shard_map/all_to_all | solution.py:471
  135.1 8.2 %shard_map.175 = bf16[16,32,2048]{2,1,0:T(8,128)(2,1)S(1)} custom-call(bf16[16,32,2048]{2,1,0:T(8,128)(2,1)S(1)} %all-to-all-done.2.x_ref, bf16[2,2048,512]{2,1,0:T(8,128)(2,1)} %gate_ref.5, bf16[2,2048,512]{2,1,0:T(8,128)(2,1)} %up_ref.3, bf16[2,512,2048]{2,1,0:T(8,128)(2,1)} %down_ref.3), custom_call_target="tpu_custom_call" | custom-call | flops 3221225472 | bytes 16777216 | tf_op jit(solution)/shard_map/pallas_call | solution.py:240
  143.3 1.3 copy-done
  144.6 19.5 %all-to-all-done.5 = bf16[16,32,2048]{2,1,0:T(8,128)(2,1)} async-done(((bf16[16,32,2048]{2,1,0:T(8,128)(2,1)}), bf16[16,32,2048]{2,1,0:T(8,128)(2,1)}, u32[]{:S(2)}, u32[]{:S(2)}) %all-to-all-start.5) | async-done | bytes 2097184 | tf_op jit(solution)/shard_map/all_to_all | solution.py:471
  164.2 4.9 %all-to-all-start.3 = ((bf16[16,32,2048]{2,1,0:T(8,128)(2,1)}), bf16[16,32,2048]{2,1,0:T(8,128)(2,1)S(1)}, u32[]{:S(2)}, u32[]{:S(2)}) async-start(bf16[16,32,2048]{2,1,0:T(8,128)(2,1)} %copy-done), calls=%async_computation.3 | async-start | bytes 4194304 | tf_op jit(solution)/shard_map/all_to_all | solution.py:471
  169.1 3.2 %shard_map.179 = bf16[128,2048]{1,0:T(8,128)(2,1)} custom-call(bf16[256,512]{1,0:T(8,128)(2,1)} %get-tuple-element.23.weight_in, bf16[512,2048]{1,0:T(8,128)(2,1)} %bitcast.17.results_in), custom_call_target="tpu_custom_call" | custom-call | tf_op jit(solution)/shard_map/pallas_call | solution.py:35
  172.3 0.8 collective-permute-start.1
  173.1 5.2 %shard_map.176 = f32[1,128,2048]{2,1,0:T(8,128)} custom-call(bf16[1,128,2048]{2,1,0:T(8,128)(2,1)} %bitcast.26, bf16[1,2048,512]{2,1,0:T(8,128)(2,1)} %bitcast.22, bf16[1,2048,512]{2,1,0:T(8,128)(2,1)} %bitcast.23, bf16[1,512,2048]{2,1,0:T(8,128)(2,1)} %bitcast.24, bf16[128,2048]{1,0:T(8,128)(2,1)} %get-tuple-element.22.rest_0_), custom_call_target="tpu_custom_call" | custom-call | flops 805306368 | bytes 7340032 | tf_op jit(solution)/shard_map/pallas_call | solution.py:240
  178.3 30.7 %all-to-all-done.3 = bf16[16,32,2048]{2,1,0:T(8,128)(2,1)S(1)} async-done(((bf16[16,32,2048]{2,1,0:T(8,128)(2,1)}), bf16[16,32,2048]{2,1,0:T(8,128)(2,1)S(1)}, u32[]{:S(2)}, u32[]{:S(2)}) %all-to-all-start.3) | async-done | bytes 2097184 | tf_op jit(solution)/shard_map/all_to_all | solution.py:471
  209.0 0.0 collective-permute-done.1.refs_1_
  209.1 1.2 copy-done.3
  210.3 2.1 shard_map.180
  (10 shorter events, 0.0 us)
Async XLA Ops:
  4.3 16.9 %all-to-all-start = ((bf16[8,144,128]{2,1,0:T(8,128)(2,1)}), bf16[8,144,128]{2,1,0:T(8,128)(2,1)S(1)}, u32[]{:S(2)}, u32[]{:S(2)}) async-start(bf16[8,144,128]{2,1,0:T(8,128)(2,1)} %get-tuple-element.15), calls=%async_computation | async-start | bytes 589824 | tf_op jit(solution)/shard_map/all_to_all | solution.py:507
  21.2 0.7 copy-start.6
  24.9 9.4 %all-to-all-start.1 = ((bf16[4,128,256]{2,1,0:T(8,128)(2,1)}), bf16[4,128,256]{2,1,0:T(8,128)(2,1)S(1)}, u32[]{:S(2)}, u32[]{:S(2)}) async-start(bf16[4,128,256]{2,1,0:T(8,128)(2,1)} %bitcast.25), calls=%async_computation.1 | async-start | bytes 524288 | tf_op jit(solution)/shard_map/all_to_all | solution.py:524
  34.3 0.7 copy-start.7
  35.0 30.6 %copy-start.5 = (bf16[512,128]{1,0:T(8,128)(2,1)S(1)}, bf16[512,128]{1,0:T(8,128)(2,1)}, u32[]{:S(2)}) copy-start(bf16[512,128]{1,0:T(8,128)(2,1)} %get-tuple-element.24.held_in) | copy-start | bytes 393220
  39.8 25.8 %collective-permute-start = (bf16[128,2048]{1,0:T(8,128)(2,1)}, bf16[128,2048]{1,0:T(8,128)(2,1)S(1)}, u32[]{:S(2)}, u32[]{:S(2)}) collective-permute-start(bf16[128,2048]{1,0:T(8,128)(2,1)} %get-tuple-element.21), channel_id=1, source_target_pairs={{0,16},{4,20},{8,24},{12,28},{16,0},{20,4},{24,8},{28,12},{1,17},{... | collective-permute-start | bytes 1572872 | tf_op jit(solution)/shard_map/ppermute | solution.py:541
  97.8 32.8 %all-to-all-start.2 = ((bf16[16,32,2048]{2,1,0:T(8,128)(2,1)}), bf16[16,32,2048]{2,1,0:T(8,128)(2,1)S(1)}, u32[]{:S(2)}, u32[]{:S(2)}) async-start(bf16[16,32,2048]{2,1,0:T(8,128)(2,1)} %bitcast.21), calls=%async_computation.2 | async-start | bytes 4194304 | tf_op jit(solution)/shard_map/all_to_all | solution.py:471
  101.6 1.6 copy-start.2
  111.4 1.3 copy-start.1
  130.6 33.6 %all-to-all-start.5 = ((bf16[16,32,2048]{2,1,0:T(8,128)(2,1)}), bf16[16,32,2048]{2,1,0:T(8,128)(2,1)}, u32[]{:S(2)}, u32[]{:S(2)}) async-start(bf16[16,32,2048]{2,1,0:T(8,128)(2,1)} %copy-done.1), calls=%async_computation.5 | async-start | bytes 4194304 | tf_op jit(solution)/shard_map/all_to_all | solution.py:471
  143.3 1.3 copy-start
  164.2 44.9 %all-to-all-start.3 = ((bf16[16,32,2048]{2,1,0:T(8,128)(2,1)}), bf16[16,32,2048]{2,1,0:T(8,128)(2,1)S(1)}, u32[]{:S(2)}, u32[]{:S(2)}) async-start(bf16[16,32,2048]{2,1,0:T(8,128)(2,1)} %copy-done), calls=%async_computation.3 | async-start | bytes 4194304 | tf_op jit(solution)/shard_map/all_to_all | solution.py:471
  172.3 36.7 %collective-permute-start.1 = (bf16[128,2048]{1,0:T(8,128)(2,1)}, bf16[128,2048]{1,0:T(8,128)(2,1)S(1)}, u32[]{:S(2)}, u32[]{:S(2)}) collective-permute-start(bf16[128,2048]{1,0:T(8,128)(2,1)} %shard_map.179), channel_id=1, source_target_pairs={{0,16},{4,20},{8,24},{12,28},{16,0},{20,4},{24,8},{28,12},{1,17},{... | collective-permute-start | bytes 1572872 | tf_op jit(solution)/shard_map/ppermute | solution.py:550
  173.1 35.9 %copy-start.4 = (bf16[256,512]{1,0:T(8,128)(2,1)S(1)}, bf16[256,512]{1,0:T(8,128)(2,1)}, u32[]{:S(2)}) copy-start(bf16[256,512]{1,0:T(8,128)(2,1)} %get-tuple-element.16.weight_in) | copy-start | bytes 786436
  209.0 1.2 copy-start.3

commit v9 on v8

--- a/solution.py
+++ b/solution.py
@@ -331,18 +331,19 @@
     return copies
 
 
-def pack_kernel(held_in, rows_in, sent_out, held, rows, sent, sems):
-    loads = start_all([(held_in, held), (rows_in, rows)], sems)
+def pack_kernel(held_in, outer_in, inner_in, sent_out, held, outer, inner, sent, sems):
+    loads = start_all([(held_in, held), (outer_in, outer), (inner_in, inner)], sems)
     for copy in loads:
         copy.wait()
-    for copy in store_slots(held, rows[...], sent, sent_out, sems, 2):
+    rows = outer[...] + inner[...]
+    for copy in store_slots(held, rows, sent, sent_out, sems, 3):
         copy.wait()
 
 
-def pack(held, rows):
-    out = jax.ShapeDtypeStruct((held.shape[0], rows.shape[1]), rows.dtype)
-    args = (held, rows)
-    return streamed(pack_kernel, out, args, args + (out,), 2 + PIECES, room=ROOM)
+def pack(held, outer, inner):
+    out = jax.ShapeDtypeStruct((held.shape[0], outer.shape[1]), outer.dtype)
+    args = (held, outer, inner)
+    return streamed(pack_kernel, out, args, args + (out,), 3 + PIECES, room=ROOM)
 
 
 def project_kernel(
@@ -538,8 +539,12 @@
         tok_count,
         add=middle,
     )[0]
-    normed_far = lax.ppermute(normed, "sp", swap)
-    sent_far = pack(held_far, normed_far)
+    quarter = seq // 4
+    outer = [pair for pair in swap if pair[0] < quarter or pair[0] >= seq - quarter]
+    inner = [pair for pair in swap if pair not in outer]
+    outer_rows = lax.ppermute(normed, "sp", outer)
+    inner_rows = lax.ppermute(normed, "sp", inner)
+    sent_far = pack(held_far, outer_rows, inner_rows)
     arrived_far = spread(sent_far)
     done_near = experts(arrived_near)
     done_far = experts(arrived_far)

time: 213 us -> 215 us (level)
  starting transfers between devices: 25.8 us -> 31.8 us
  waiting for transfers between devices: 105 us -> 101 us
    ppermute x1 -> x2, starting transfers between devices: 1.18 us -> 6.8 us  [the longest x1 5.51 us: on_device(): outer_rows = lax.ppermute(normed, 'sp', outer)]
    ppermute x1 -> x2, waiting for transfers between devices: 24.6 us -> 20.8 us  [the longest x1 20.8 us: on_device(): inner_rows = lax.ppermute(normed, 'sp', inner)]
  transfers between devices with their start and end apart: 7 -> 8, of which waited for: 6 -> 6; matrix products, arithmetic and copies ran while one was open for 0% -> 0% of each run, Pallas kernels for 13% -> 13%
where the time goes in v9:
time: 215 us; the launch traced here: 214 us
  waiting for transfers between devices  101 us (47%)
  Pallas kernels  43.2 us (20%)
  starting transfers between devices  31.8 us (15%)
  blocking collectives  30.7 us (14%)
  local copies, waits for them, and re-layouts  6.89 us (3%)
    all_to_all x3, waiting for transfers between devices, spread(): lax.all_to_all(rows.reshape(half, exp_dev * cap, width), axes, split_axis...  67.8 us
    all_to_all x1, blocking collectives, spread(): lax.all_to_all(rows.reshape(half, exp_dev * cap, width), axes, split_axis...  30.7 us
    pallas_call x3, Pallas kernels, ffn(): pl.pallas_call(ffn_kernel, grid=(count, steps), in_specs=in_specs, out_sp...  21.6 us
    ppermute x1, waiting for transfers between devices, on_device(): inner_rows = lax.ppermute(normed, 'sp', inner)  20.8 us
    all_to_all x3, starting transfers between devices, spread(): lax.all_to_all(rows.reshape(half, exp_dev * cap, width), axes, split_axis...  13.1 us
    pallas_call x4, Pallas kernels, streamed(): pl.pallas_call(kernel, in_specs=[smem] * scalars + [anywhere] * (len(args...  11.6 us
    all_to_all x1, waiting for transfers between devices, on_device(): lax.all_to_all(message, 'sp', split_axis=0, concat_axis=0, tiled=True)  9.61 us
    all_to_all x1, starting transfers between devices, on_device(): lax.all_to_all(message, 'sp', split_axis=0, concat_axis=0, tiled=True)  7.31 us
  transfers between devices with their start and end apart: 8, of which 6 were waited for; matrix products, arithmetic and copies ran while one was open for 0% of the time, Pallas kernels for 13%

profile of v9, /device:TPU:0, one launch (start us, length us, event | category | flops | bytes accessed | tf_op | source)
XLA Modules:
  0.0 214.2 jit_solution(11366225497736290974)
XLA Ops:
  0.0 4.2 %shard_map.172 = (f32[512,128]{1,0:T(8,128)}, f32[8,128,128]{2,1,0:T(8,128)}, bf16[8,144,128]{2,1,0:T(8,128)(2,1)}) custom-call(bf16[512,128]{1,0:T(8,128)(2,1)} %k_ref.3, bf16[512,256]{1,0:T(8,128)(2,1)} %v_ref.3, bf16[512,128]{1,0:T(8,128)(2,1)} %c_ref.1, f32[2,512]{1,0:T(2,128)} %bitcast.32, s32[4,128]{1,0:T(4,128)} %bitcast.28, f32[4,128]{1,0:T(4,128)} %bitcast.30), custom_call_target="tpu_custom_call" | custom-call | tf_op jit(solution)/shard_map/pallas_call | solution.py:184
  4.3 7.3 %all-to-all-start = ((bf16[8,144,128]{2,1,0:T(8,128)(2,1)}), bf16[8,144,128]{2,1,0:T(8,128)(2,1)S(1)}, u32[]{:S(2)}, u32[]{:S(2)}) async-start(bf16[8,144,128]{2,1,0:T(8,128)(2,1)} %get-tuple-element.15), calls=%async_computation | async-start | bytes 589824 | tf_op jit(solution)/shard_map/all_to_all | solution.py:508
  11.6 9.6 %all-to-all-done.far_ref.msg_ref = bf16[8,144,128]{2,1,0:T(8,128)(2,1)S(1)} async-done(((bf16[8,144,128]{2,1,0:T(8,128)(2,1)}), bf16[8,144,128]{2,1,0:T(8,128)(2,1)S(1)}, u32[]{:S(2)}, u32[]{:S(2)}) %all-to-all-start) | async-done | bytes 294944 | tf_op jit(solution)/shard_map/all_to_all | solution.py:508
  21.2 0.7 copy-done.6
  21.9 3.0 %shard_map.173 = bf16[512,256]{1,0:T(8,128)(2,1)} custom-call(s32[1]{0:T(128)} %bitcast.5.place_ref, bf16[512,128]{1,0:T(8,128)(2,1)} %q_ref.1, bf16[512,128]{1,0:T(8,128)(2,1)} %k_ref.3, bf16[512,256]{1,0:T(8,128)(2,1)} %v_ref.3, f32[512,128]{1,0:T(8,128)} %get-tuple-element.17.within_ref, f32[8,128,128]{2,1,0:T(8,128)} %get-tuple-element.18.starts_ref, ...), custom_call_target="tpu_custom_call" | custom-call | tf_op jit(solution)/shard_map/pallas_call | solution.py:184
  24.9 3.4 %all-to-all-start.1 = ((bf16[4,128,256]{2,1,0:T(8,128)(2,1)}), bf16[4,128,256]{2,1,0:T(8,128)(2,1)S(1)}, u32[]{:S(2)}, u32[]{:S(2)}) async-start(bf16[4,128,256]{2,1,0:T(8,128)(2,1)} %bitcast.25), calls=%async_computation.1 | async-start | bytes 524288 | tf_op jit(solution)/shard_map/all_to_all | solution.py:525
  28.4 0.6 pad_add_fusion.place_ref
  29.0 2.7 %tables.1 = (bf16[512,128]{1,0:T(8,128)(2,1)}, bf16[256,512]{1,0:T(8,128)(2,1)}, bf16[512,128]{1,0:T(8,128)(2,1)}, bf16[256,512]{1,0:T(8,128)(2,1)}) custom-call(s32[2]{0:T(128)} %pad_add_fusion.place_ref, s32[4,128]{1,0:T(4,128)} %bitcast.29, f32[4,128]{1,0:T(4,128)} %bitcast.31, bf16[8,144,128]{2,1,0:T(8,128)(2,1)} %copy-done.6), custom_call_target="tpu_custom_call" | custom-call | tf_op jit(solution)/shard_map/tables/pallas_call | solution.py:300
  31.7 2.6 %all-to-all-done.1.g_in = bf16[4,128,256]{2,1,0:T(8,128)(2,1)S(1)} async-done(((bf16[4,128,256]{2,1,0:T(8,128)(2,1)}), bf16[4,128,256]{2,1,0:T(8,128)(2,1)S(1)}, u32[]{:S(2)}, u32[]{:S(2)}) %all-to-all-start.1) | async-done | bytes 262176 | tf_op jit(solution)/shard_map/all_to_all | solution.py:525
  34.3 0.7 copy-done.7
  35.0 4.8 %shard_map.174 = (bf16[512,2048]{1,0:T(8,128)(2,1)}, bf16[128,2048]{1,0:T(8,128)(2,1)}, bf16[128,2048]{1,0:T(8,128)(2,1)}) custom-call(bf16[4,128,256]{2,1,0:T(8,128)(2,1)} %copy-done.7, bf16[1024,2048]{1,0:T(8,128)(2,1)} %w_in.1, bf16[128,2048]{1,0:T(8,128)(2,1)} %res_in.1, f32[1,2048]{1,0:T(1,128)} %bitcast.27, bf16[512,128]{1,0:T(8,128)(2,1)} %get-tuple-element.19.held_in), custom_call_target="tpu_custom_call" | custom-call | tf_op jit(solution)/shard_map/pallas_call | solution.py:35
  39.8 1.3 collective-permute-start.1
  41.1 5.5 %collective-permute-start = (bf16[128,2048]{1,0:T(8,128)(2,1)}, bf16[128,2048]{1,0:T(8,128)(2,1)S(1)}, u32[]{:S(2)}, u32[]{:S(2)}) collective-permute-start(bf16[128,2048]{1,0:T(8,128)(2,1)} %get-tuple-element.21), channel_id=1, source_target_pairs={{0,16},{4,20},{24,8},{28,12},{1,17},{5,21},{25,9},{29,13},{2,18},{... | collective-permute-start | bytes 1572872 | tf_op jit(solution)/shard_map/ppermute | solution.py:545
  46.6 20.8 %collective-permute-done.1.inner_in = bf16[128,2048]{1,0:T(8,128)(2,1)S(1)} collective-permute-done((bf16[128,2048]{1,0:T(8,128)(2,1)}, bf16[128,2048]{1,0:T(8,128)(2,1)S(1)}, u32[]{:S(2)}, u32[]{:S(2)}) %collective-permute-start.1) | collective-permute-done | bytes 524320 | tf_op jit(solution)/shard_map/ppermute | solution.py:546
  67.4 1.6 shard_map.177
  69.0 30.7 %all_to_all.30.x_ref = bf16[16,32,2048]{2,1,0:T(8,128)(2,1)} all-to-all(bf16[16,32,2048]{2,1,0:T(8,128)(2,1)S(1)} %bitcast.19), channel_id=1, replica_groups={{0,1,2,3,4,5,6,7,8,9,10,11,12,13,14,15},{16,17,18,19,20,21,22,23,24,25,..., dimensions={0} | all-to-all | bytes 4194304 | tf_op jit(solution)/shard_map/all_to_all | solution.py:472
  99.7 3.7 %all-to-all-start.2 = ((bf16[16,32,2048]{2,1,0:T(8,128)(2,1)}), bf16[16,32,2048]{2,1,0:T(8,128)(2,1)S(1)}, u32[]{:S(2)}, u32[]{:S(2)}) async-start(bf16[16,32,2048]{2,1,0:T(8,128)(2,1)} %bitcast.21), calls=%async_computation.2 | async-start | bytes 4194304 | tf_op jit(solution)/shard_map/all_to_all | solution.py:472
  103.5 1.6 copy-done.2
  105.0 8.2 %shard_map.178 = bf16[16,32,2048]{2,1,0:T(8,128)(2,1)S(1)} custom-call(bf16[16,32,2048]{2,1,0:T(8,128)(2,1)S(1)} %copy-done.2, bf16[2,2048,512]{2,1,0:T(8,128)(2,1)} %gate_ref.5, bf16[2,2048,512]{2,1,0:T(8,128)(2,1)} %up_ref.3, bf16[2,512,2048]{2,1,0:T(8,128)(2,1)} %down_ref.3), custom_call_target="tpu_custom_call" | custom-call | flops 3221225472 | bytes 16777216 | tf_op jit(solution)/shard_map/pallas_call | solution.py:240
  113.2 1.3 copy-done.1
  114.6 17.9 %all-to-all-done.2.x_ref = bf16[16,32,2048]{2,1,0:T(8,128)(2,1)S(1)} async-done(((bf16[16,32,2048]{2,1,0:T(8,128)(2,1)}), bf16[16,32,2048]{2,1,0:T(8,128)(2,1)S(1)}, u32[]{:S(2)}, u32[]{:S(2)}) %all-to-all-start.2) | async-done | bytes 2097184 | tf_op jit(solution)/shard_map/all_to_all | solution.py:472
  132.5 4.5 %all-to-all-start.5 = ((bf16[16,32,2048]{2,1,0:T(8,128)(2,1)}), bf16[16,32,2048]{2,1,0:T(8,128)(2,1)}, u32[]{:S(2)}, u32[]{:S(2)}) async-start(bf16[16,32,2048]{2,1,0:T(8,128)(2,1)} %copy-done.1), calls=%async_computation.5 | async-start | bytes 4194304 | tf_op jit(solution)/shard_map/all_to_all | solution.py:472
  137.0 8.2 %shard_map.175 = bf16[16,32,2048]{2,1,0:T(8,128)(2,1)S(1)} custom-call(bf16[16,32,2048]{2,1,0:T(8,128)(2,1)S(1)} %all-to-all-done.2.x_ref, bf16[2,2048,512]{2,1,0:T(8,128)(2,1)} %gate_ref.5, bf16[2,2048,512]{2,1,0:T(8,128)(2,1)} %up_ref.3, bf16[2,512,2048]{2,1,0:T(8,128)(2,1)} %down_ref.3), custom_call_target="tpu_custom_call" | custom-call | flops 3221225472 | bytes 16777216 | tf_op jit(solution)/shard_map/pallas_call | solution.py:240
  145.2 1.3 copy-done
  146.5 19.6 %all-to-all-done.5 = bf16[16,32,2048]{2,1,0:T(8,128)(2,1)} async-done(((bf16[16,32,2048]{2,1,0:T(8,128)(2,1)}), bf16[16,32,2048]{2,1,0:T(8,128)(2,1)}, u32[]{:S(2)}, u32[]{:S(2)}) %all-to-all-start.5) | async-done | bytes 2097184 | tf_op jit(solution)/shard_map/all_to_all | solution.py:472
  166.0 4.9 %all-to-all-start.3 = ((bf16[16,32,2048]{2,1,0:T(8,128)(2,1)}), bf16[16,32,2048]{2,1,0:T(8,128)(2,1)S(1)}, u32[]{:S(2)}, u32[]{:S(2)}) async-start(bf16[16,32,2048]{2,1,0:T(8,128)(2,1)} %copy-done), calls=%async_computation.3 | async-start | bytes 4194304 | tf_op jit(solution)/shard_map/all_to_all | solution.py:472
  171.0 3.2 %shard_map.179 = bf16[128,2048]{1,0:T(8,128)(2,1)} custom-call(bf16[256,512]{1,0:T(8,128)(2,1)} %get-tuple-element.23.weight_in, bf16[512,2048]{1,0:T(8,128)(2,1)} %bitcast.17.results_in), custom_call_target="tpu_custom_call" | custom-call | tf_op jit(solution)/shard_map/pallas_call | solution.py:35
  174.2 1.2 collective-permute-start.2
  175.4 5.2 %shard_map.176 = f32[1,128,2048]{2,1,0:T(8,128)} custom-call(bf16[1,128,2048]{2,1,0:T(8,128)(2,1)} %bitcast.26, bf16[1,2048,512]{2,1,0:T(8,128)(2,1)} %bitcast.22, bf16[1,2048,512]{2,1,0:T(8,128)(2,1)} %bitcast.23, bf16[1,512,2048]{2,1,0:T(8,128)(2,1)} %bitcast.24, bf16[128,2048]{1,0:T(8,128)(2,1)} %get-tuple-element.22.rest_0_), custom_call_target="tpu_custom_call" | custom-call | flops 805306368 | bytes 7340032 | tf_op jit(solution)/shard_map/pallas_call | solution.py:240
  180.6 30.3 %all-to-all-done.3 = bf16[16,32,2048]{2,1,0:T(8,128)(2,1)S(1)} async-done(((bf16[16,32,2048]{2,1,0:T(8,128)(2,1)}), bf16[16,32,2048]{2,1,0:T(8,128)(2,1)S(1)}, u32[]{:S(2)}, u32[]{:S(2)}) %all-to-all-start.3) | async-done | bytes 2097184 | tf_op jit(solution)/shard_map/all_to_all | solution.py:472
  210.9 1.2 copy-done.3
  212.1 2.1 shard_map.180
  (12 shorter events, 0.0 us)
Async XLA Ops:
  4.3 16.9 %all-to-all-start = ((bf16[8,144,128]{2,1,0:T(8,128)(2,1)}), bf16[8,144,128]{2,1,0:T(8,128)(2,1)S(1)}, u32[]{:S(2)}, u32[]{:S(2)}) async-start(bf16[8,144,128]{2,1,0:T(8,128)(2,1)} %get-tuple-element.15), calls=%async_computation | async-start | bytes 589824 | tf_op jit(solution)/shard_map/all_to_all | solution.py:508
  21.2 0.7 copy-start.6
  24.9 9.4 %all-to-all-start.1 = ((bf16[4,128,256]{2,1,0:T(8,128)(2,1)}), bf16[4,128,256]{2,1,0:T(8,128)(2,1)S(1)}, u32[]{:S(2)}, u32[]{:S(2)}) async-start(bf16[4,128,256]{2,1,0:T(8,128)(2,1)} %bitcast.25), calls=%async_computation.1 | async-start | bytes 524288 | tf_op jit(solution)/shard_map/all_to_all | solution.py:525
  34.3 0.7 copy-start.7
  35.0 32.4 %copy-start.5 = (bf16[512,128]{1,0:T(8,128)(2,1)S(1)}, bf16[512,128]{1,0:T(8,128)(2,1)}, u32[]{:S(2)}) copy-start(bf16[512,128]{1,0:T(8,128)(2,1)} %get-tuple-element.24.held_in) | copy-start | bytes 393220
  39.8 27.6 %collective-permute-start.1 = (bf16[128,2048]{1,0:T(8,128)(2,1)}, bf16[128,2048]{1,0:T(8,128)(2,1)S(1)}, u32[]{:S(2)}, u32[]{:S(2)}) collective-permute-start(bf16[128,2048]{1,0:T(8,128)(2,1)} %get-tuple-element.21), channel_id=1, source_target_pairs={{8,24},{12,28},{16,0},{20,4},{9,25},{13,29},{17,1},{21,5},{10,26},... | collective-permute-start | bytes 1572872 | tf_op jit(solution)/shard_map/ppermute | solution.py:546
  41.1 26.3 %collective-permute-start = (bf16[128,2048]{1,0:T(8,128)(2,1)}, bf16[128,2048]{1,0:T(8,128)(2,1)S(1)}, u32[]{:S(2)}, u32[]{:S(2)}) collective-permute-start(bf16[128,2048]{1,0:T(8,128)(2,1)} %get-tuple-element.21), channel_id=1, source_target_pairs={{0,16},{4,20},{24,8},{28,12},{1,17},{5,21},{25,9},{29,13},{2,18},{... | collective-permute-start | bytes 1572872 | tf_op jit(solution)/shard_map/ppermute | solution.py:545
  99.7 32.8 %all-to-all-start.2 = ((bf16[16,32,2048]{2,1,0:T(8,128)(2,1)}), bf16[16,32,2048]{2,1,0:T(8,128)(2,1)S(1)}, u32[]{:S(2)}, u32[]{:S(2)}) async-start(bf16[16,32,2048]{2,1,0:T(8,128)(2,1)} %bitcast.21), calls=%async_computation.2 | async-start | bytes 4194304 | tf_op jit(solution)/shard_map/all_to_all | solution.py:472
  103.4 1.6 copy-start.2
  113.2 1.3 copy-start.1
  132.5 33.5 %all-to-all-start.5 = ((bf16[16,32,2048]{2,1,0:T(8,128)(2,1)}), bf16[16,32,2048]{2,1,0:T(8,128)(2,1)}, u32[]{:S(2)}, u32[]{:S(2)}) async-start(bf16[16,32,2048]{2,1,0:T(8,128)(2,1)} %copy-done.1), calls=%async_computation.5 | async-start | bytes 4194304 | tf_op jit(solution)/shard_map/all_to_all | solution.py:472
  145.2 1.3 copy-start
  166.0 44.9 %all-to-all-start.3 = ((bf16[16,32,2048]{2,1,0:T(8,128)(2,1)}), bf16[16,32,2048]{2,1,0:T(8,128)(2,1)S(1)}, u32[]{:S(2)}, u32[]{:S(2)}) async-start(bf16[16,32,2048]{2,1,0:T(8,128)(2,1)} %copy-done), calls=%async_computation.3 | async-start | bytes 4194304 | tf_op jit(solution)/shard_map/all_to_all | solution.py:472
  174.2 36.7 %collective-permute-start.2 = (bf16[128,2048]{1,0:T(8,128)(2,1)}, bf16[128,2048]{1,0:T(8,128)(2,1)S(1)}, u32[]{:S(2)}, u32[]{:S(2)}) collective-permute-start(bf16[128,2048]{1,0:T(8,128)(2,1)} %shard_map.179), channel_id=1, source_target_pairs={{0,16},{4,20},{8,24},{12,28},{16,0},{20,4},{24,8},{28,12},{1,17},{... | collective-permute-start | bytes 1572872 | tf_op jit(solution)/shard_map/ppermute | solution.py:555
  175.4 35.5 %copy-start.4 = (bf16[256,512]{1,0:T(8,128)(2,1)S(1)}, bf16[256,512]{1,0:T(8,128)(2,1)}, u32[]{:S(2)}) copy-start(bf16[256,512]{1,0:T(8,128)(2,1)} %get-tuple-element.16.weight_in) | copy-start | bytes 786436
  210.9 1.2 copy-start.3

commit v10 on v8

--- a/solution.py
+++ b/solution.py
@@ -77,20 +77,26 @@
     lower = lax.broadcasted_iota(jnp.int32, (BLOCK, BLOCK), 0) >= lax.broadcasted_iota(
         jnp.int32, (BLOCK, BLOCK), 1
     )
-    lower = lower.astype(jnp.float32)
+    lower = lower.astype(jnp.float32).astype(jnp.bfloat16)
+    blocks = rows // BLOCK
+    high, rest = two_pieces(decay)
+    middle, low = two_pieces(rest)
+    summed = None
+    for piece in (high, middle, low):
+        piece = piece.astype(jnp.bfloat16)
+        wide = jnp.concatenate(
+            [piece[n * BLOCK : (n + 1) * BLOCK] for n in range(blocks)], axis=1
+        )
+        part = jnp.dot(lower, wide, preferred_element_type=jnp.float32)
+        summed = part if summed is None else summed + part
     state_head = lane_head((vdim, width))
     state = jnp.zeros((vdim, width), jnp.float32)
     total = jnp.zeros((1, width), jnp.float32)
-    for n in range(rows // BLOCK):
+    for n in range(blocks):
         at = slice(n * BLOCK, (n + 1) * BLOCK)
-        within = jnp.dot(
-            lower,
-            decay[at],
-            precision=lax.Precision.HIGHEST,
-            preferred_element_type=jnp.float32,
-        )
+        within = summed[:, n * width : (n + 1) * width]
         within_ref[at, :] = within
-        starts_ref[n] = state
+        starts_ref[n] = state.astype(jnp.bfloat16)
         last = within[BLOCK - 1 : BLOCK]
         tail = (k_ref[at, :].astype(jnp.float32) * jnp.exp(last - within)).astype(jnp.bfloat16)
         added = jnp.zeros((vdim, width), jnp.float32)
@@ -151,7 +157,7 @@
             split, grown, (((1,), (1,)), ((), ())), preferred_element_type=jnp.float32
         )
         scores = jnp.where(causal, scores, 0.0).astype(jnp.bfloat16)
-        entering = (starts_ref[n] + jnp.exp(before) * carried).astype(jnp.bfloat16)
+        entering = (starts_ref[n].astype(jnp.float32) + jnp.exp(before) * carried).astype(jnp.bfloat16)
         crossed = lax.dot_general(
             split, entering, (((1,), (1,)), ((), ())), preferred_element_type=jnp.float32
         )
@@ -494,7 +500,7 @@
         state_kernel,
         (
             like((key_rows, key_cols), jnp.float32),
-            like((key_rows // BLOCK, vdim, key_cols), jnp.float32),
+            like((key_rows // BLOCK, vdim, key_cols)),
             like((seq, vdim + MSG_PAD, key_cols)),
         ),
         key_matrix,

time: 213 us -> 212 us (level)
  no operation moved by 1% of the time
where the time goes in v10:
time: 212 us; the launch traced here: 211 us
  waiting for transfers between devices  105 us (50%)
  Pallas kernels  42 us (20%)
  blocking collectives  30.7 us (14%)
  starting transfers between devices  25.8 us (12%)
  local copies, waits for them, and re-layouts  6.9 us (3%)
    all_to_all x3, waiting for transfers between devices, spread(): lax.all_to_all(rows.reshape(half, exp_dev * cap, width), axes, split_axis...  68.2 us
    all_to_all x1, blocking collectives, spread(): lax.all_to_all(rows.reshape(half, exp_dev * cap, width), axes, split_axis...  30.7 us
    ppermute x1, waiting for transfers between devices, on_device(): normed_far = lax.ppermute(normed, 'sp', swap)  24.6 us
    pallas_call x3, Pallas kernels, ffn(): pl.pallas_call(ffn_kernel, grid=(count, steps), in_specs=in_specs, out_sp...  21.6 us
    all_to_all x3, starting transfers between devices, spread(): lax.all_to_all(rows.reshape(half, exp_dev * cap, width), axes, split_axis...  13.1 us
    pallas_call x4, Pallas kernels, streamed(): pl.pallas_call(kernel, in_specs=[smem] * scalars + [anywhere] * (len(args...  11.6 us
    all_to_all x1, waiting for transfers between devices, on_device(): lax.all_to_all(message, 'sp', split_axis=0, concat_axis=0, tiled=True)  9.61 us
    all_to_all x1, starting transfers between devices, on_device(): lax.all_to_all(message, 'sp', split_axis=0, concat_axis=0, tiled=True)  7.31 us
  transfers between devices with their start and end apart: 7, of which 6 were waited for; matrix products, arithmetic and copies ran while one was open for 0% of the time, Pallas kernels for 13%

profile of v10, /device:TPU:0, one launch (start us, length us, event | category | flops | bytes accessed | tf_op | source)
XLA Modules:
  0.0 211.1 jit_solution(5236116646201858538)
XLA Ops:
  0.0 3.1 %shard_map.172 = (f32[512,128]{1,0:T(8,128)}, bf16[8,128,128]{2,1,0:T(8,128)(2,1)}, bf16[8,144,128]{2,1,0:T(8,128)(2,1)}) custom-call(bf16[512,128]{1,0:T(8,128)(2,1)} %k_ref.3, bf16[512,256]{1,0:T(8,128)(2,1)} %v_ref.3, bf16[512,128]{1,0:T(8,128)(2,1)} %c_ref.1, f32[2,512]{1,0:T(2,128)} %bitcast.32, s32[4,128]{1,0:T(4,128)} %bitcast.28, f32[4,128]{1,0:T(4,128)} %bitcast.30), custom_call_target="tpu_custom_call" | custom-call | tf_op jit(solution)/shard_map/pallas_call | solution.py:190
  3.1 7.3 %all-to-all-start = ((bf16[8,144,128]{2,1,0:T(8,128)(2,1)}), bf16[8,144,128]{2,1,0:T(8,128)(2,1)S(1)}, u32[]{:S(2)}, u32[]{:S(2)}) async-start(bf16[8,144,128]{2,1,0:T(8,128)(2,1)} %get-tuple-element.15), calls=%async_computation | async-start | bytes 589824 | tf_op jit(solution)/shard_map/all_to_all | solution.py:513
  10.4 9.6 %all-to-all-done.far_ref.msg_ref = bf16[8,144,128]{2,1,0:T(8,128)(2,1)S(1)} async-done(((bf16[8,144,128]{2,1,0:T(8,128)(2,1)}), bf16[8,144,128]{2,1,0:T(8,128)(2,1)S(1)}, u32[]{:S(2)}, u32[]{:S(2)}) %all-to-all-start) | async-done | bytes 294944 | tf_op jit(solution)/shard_map/all_to_all | solution.py:513
  20.1 0.7 copy-done.6
  20.8 3.0 %shard_map.173 = bf16[512,256]{1,0:T(8,128)(2,1)} custom-call(s32[1]{0:T(128)} %bitcast.5.place_ref, bf16[512,128]{1,0:T(8,128)(2,1)} %q_ref.1, bf16[512,128]{1,0:T(8,128)(2,1)} %k_ref.3, bf16[512,256]{1,0:T(8,128)(2,1)} %v_ref.3, f32[512,128]{1,0:T(8,128)} %get-tuple-element.17.within_ref, bf16[8,128,128]{2,1,0:T(8,128)(2,1)} %get-tuple-element.18.starts_ref, ...), custom_call_target="tpu_custom_call" | custom-call | tf_op jit(solution)/shard_map/pallas_call | solution.py:190
  23.7 3.4 %all-to-all-start.1 = ((bf16[4,128,256]{2,1,0:T(8,128)(2,1)}), bf16[4,128,256]{2,1,0:T(8,128)(2,1)S(1)}, u32[]{:S(2)}, u32[]{:S(2)}) async-start(bf16[4,128,256]{2,1,0:T(8,128)(2,1)} %bitcast.25), calls=%async_computation.1 | async-start | bytes 524288 | tf_op jit(solution)/shard_map/all_to_all | solution.py:530
  27.1 0.6 pad_add_fusion.place_ref
  27.7 2.8 %tables.1 = (bf16[512,128]{1,0:T(8,128)(2,1)}, bf16[256,512]{1,0:T(8,128)(2,1)}, bf16[512,128]{1,0:T(8,128)(2,1)}, bf16[256,512]{1,0:T(8,128)(2,1)}) custom-call(s32[2]{0:T(128)} %pad_add_fusion.place_ref, s32[4,128]{1,0:T(4,128)} %bitcast.29, f32[4,128]{1,0:T(4,128)} %bitcast.31, bf16[8,144,128]{2,1,0:T(8,128)(2,1)} %copy-done.6), custom_call_target="tpu_custom_call" | custom-call | tf_op jit(solution)/shard_map/tables/pallas_call | solution.py:306
  30.5 2.6 %all-to-all-done.1.g_in = bf16[4,128,256]{2,1,0:T(8,128)(2,1)S(1)} async-done(((bf16[4,128,256]{2,1,0:T(8,128)(2,1)}), bf16[4,128,256]{2,1,0:T(8,128)(2,1)S(1)}, u32[]{:S(2)}, u32[]{:S(2)}) %all-to-all-start.1) | async-done | bytes 262176 | tf_op jit(solution)/shard_map/all_to_all | solution.py:530
  33.1 0.7 copy-done.7
  33.8 4.8 %shard_map.174 = (bf16[512,2048]{1,0:T(8,128)(2,1)}, bf16[128,2048]{1,0:T(8,128)(2,1)}, bf16[128,2048]{1,0:T(8,128)(2,1)}) custom-call(bf16[4,128,256]{2,1,0:T(8,128)(2,1)} %copy-done.7, bf16[1024,2048]{1,0:T(8,128)(2,1)} %w_in.1, bf16[128,2048]{1,0:T(8,128)(2,1)} %res_in.1, f32[1,2048]{1,0:T(1,128)} %bitcast.27, bf16[512,128]{1,0:T(8,128)(2,1)} %get-tuple-element.19.held_in), custom_call_target="tpu_custom_call" | custom-call | tf_op jit(solution)/shard_map/pallas_call | solution.py:35
  38.6 1.2 collective-permute-start
  39.8 24.6 %collective-permute-done.rows_in = bf16[128,2048]{1,0:T(8,128)(2,1)S(1)} collective-permute-done((bf16[128,2048]{1,0:T(8,128)(2,1)}, bf16[128,2048]{1,0:T(8,128)(2,1)S(1)}, u32[]{:S(2)}, u32[]{:S(2)}) %collective-permute-start) | collective-permute-done | bytes 524320 | tf_op jit(solution)/shard_map/ppermute | solution.py:547
  64.4 1.5 shard_map.177
  65.9 30.7 %all_to_all.30.x_ref = bf16[16,32,2048]{2,1,0:T(8,128)(2,1)} all-to-all(bf16[16,32,2048]{2,1,0:T(8,128)(2,1)S(1)} %bitcast.19), channel_id=1, replica_groups={{0,1,2,3,4,5,6,7,8,9,10,11,12,13,14,15},{16,17,18,19,20,21,22,23,24,25,..., dimensions={0} | all-to-all | bytes 4194304 | tf_op jit(solution)/shard_map/all_to_all | solution.py:477
  96.6 3.7 %all-to-all-start.2 = ((bf16[16,32,2048]{2,1,0:T(8,128)(2,1)}), bf16[16,32,2048]{2,1,0:T(8,128)(2,1)S(1)}, u32[]{:S(2)}, u32[]{:S(2)}) async-start(bf16[16,32,2048]{2,1,0:T(8,128)(2,1)} %bitcast.21), calls=%async_computation.2 | async-start | bytes 4194304 | tf_op jit(solution)/shard_map/all_to_all | solution.py:477
  100.4 1.6 copy-done.2
  101.9 8.2 %shard_map.178 = bf16[16,32,2048]{2,1,0:T(8,128)(2,1)S(1)} custom-call(bf16[16,32,2048]{2,1,0:T(8,128)(2,1)S(1)} %copy-done.2, bf16[2,2048,512]{2,1,0:T(8,128)(2,1)} %gate_ref.5, bf16[2,2048,512]{2,1,0:T(8,128)(2,1)} %up_ref.3, bf16[2,512,2048]{2,1,0:T(8,128)(2,1)} %down_ref.3), custom_call_target="tpu_custom_call" | custom-call | flops 3221225472 | bytes 16777216 | tf_op jit(solution)/shard_map/pallas_call | solution.py:246
  110.1 1.3 copy-done.1
  111.5 17.9 %all-to-all-done.2.x_ref = bf16[16,32,2048]{2,1,0:T(8,128)(2,1)S(1)} async-done(((bf16[16,32,2048]{2,1,0:T(8,128)(2,1)}), bf16[16,32,2048]{2,1,0:T(8,128)(2,1)S(1)}, u32[]{:S(2)}, u32[]{:S(2)}) %all-to-all-start.2) | async-done | bytes 2097184 | tf_op jit(solution)/shard_map/all_to_all | solution.py:477
  129.4 4.5 %all-to-all-start.5 = ((bf16[16,32,2048]{2,1,0:T(8,128)(2,1)}), bf16[16,32,2048]{2,1,0:T(8,128)(2,1)}, u32[]{:S(2)}, u32[]{:S(2)}) async-start(bf16[16,32,2048]{2,1,0:T(8,128)(2,1)} %copy-done.1), calls=%async_computation.5 | async-start | bytes 4194304 | tf_op jit(solution)/shard_map/all_to_all | solution.py:477
  133.9 8.2 %shard_map.175 = bf16[16,32,2048]{2,1,0:T(8,128)(2,1)S(1)} custom-call(bf16[16,32,2048]{2,1,0:T(8,128)(2,1)S(1)} %all-to-all-done.2.x_ref, bf16[2,2048,512]{2,1,0:T(8,128)(2,1)} %gate_ref.5, bf16[2,2048,512]{2,1,0:T(8,128)(2,1)} %up_ref.3, bf16[2,512,2048]{2,1,0:T(8,128)(2,1)} %down_ref.3), custom_call_target="tpu_custom_call" | custom-call | flops 3221225472 | bytes 16777216 | tf_op jit(solution)/shard_map/pallas_call | solution.py:246
  142.1 1.3 copy-done
  143.4 19.5 %all-to-all-done.5 = bf16[16,32,2048]{2,1,0:T(8,128)(2,1)} async-done(((bf16[16,32,2048]{2,1,0:T(8,128)(2,1)}), bf16[16,32,2048]{2,1,0:T(8,128)(2,1)}, u32[]{:S(2)}, u32[]{:S(2)}) %all-to-all-start.5) | async-done | bytes 2097184 | tf_op jit(solution)/shard_map/all_to_all | solution.py:477
  163.0 4.9 %all-to-all-start.3 = ((bf16[16,32,2048]{2,1,0:T(8,128)(2,1)}), bf16[16,32,2048]{2,1,0:T(8,128)(2,1)S(1)}, u32[]{:S(2)}, u32[]{:S(2)}) async-start(bf16[16,32,2048]{2,1,0:T(8,128)(2,1)} %copy-done), calls=%async_computation.3 | async-start | bytes 4194304 | tf_op jit(solution)/shard_map/all_to_all | solution.py:477
  167.9 3.2 %shard_map.179 = bf16[128,2048]{1,0:T(8,128)(2,1)} custom-call(bf16[256,512]{1,0:T(8,128)(2,1)} %get-tuple-element.23.weight_in, bf16[512,2048]{1,0:T(8,128)(2,1)} %bitcast.17.results_in), custom_call_target="tpu_custom_call" | custom-call | tf_op jit(solution)/shard_map/pallas_call | solution.py:35
  171.1 0.8 collective-permute-start.1
  171.9 5.2 %shard_map.176 = f32[1,128,2048]{2,1,0:T(8,128)} custom-call(bf16[1,128,2048]{2,1,0:T(8,128)(2,1)} %bitcast.26, bf16[1,2048,512]{2,1,0:T(8,128)(2,1)} %bitcast.22, bf16[1,2048,512]{2,1,0:T(8,128)(2,1)} %bitcast.23, bf16[1,512,2048]{2,1,0:T(8,128)(2,1)} %bitcast.24, bf16[128,2048]{1,0:T(8,128)(2,1)} %get-tuple-element.22.rest_0_), custom_call_target="tpu_custom_call" | custom-call | flops 805306368 | bytes 7340032 | tf_op jit(solution)/shard_map/pallas_call | solution.py:246
  177.1 30.7 %all-to-all-done.3 = bf16[16,32,2048]{2,1,0:T(8,128)(2,1)S(1)} async-done(((bf16[16,32,2048]{2,1,0:T(8,128)(2,1)}), bf16[16,32,2048]{2,1,0:T(8,128)(2,1)S(1)}, u32[]{:S(2)}, u32[]{:S(2)}) %all-to-all-start.3) | async-done | bytes 2097184 | tf_op jit(solution)/shard_map/all_to_all | solution.py:477
  207.8 0.0 collective-permute-done.1.refs_1_
  207.8 1.2 copy-done.3
  209.1 2.1 shard_map.180
  (10 shorter events, 0.0 us)
Async XLA Ops:
  3.1 16.9 %all-to-all-start = ((bf16[8,144,128]{2,1,0:T(8,128)(2,1)}), bf16[8,144,128]{2,1,0:T(8,128)(2,1)S(1)}, u32[]{:S(2)}, u32[]{:S(2)}) async-start(bf16[8,144,128]{2,1,0:T(8,128)(2,1)} %get-tuple-element.15), calls=%async_computation | async-start | bytes 589824 | tf_op jit(solution)/shard_map/all_to_all | solution.py:513
  20.1 0.7 copy-start.6
  23.7 9.4 %all-to-all-start.1 = ((bf16[4,128,256]{2,1,0:T(8,128)(2,1)}), bf16[4,128,256]{2,1,0:T(8,128)(2,1)S(1)}, u32[]{:S(2)}, u32[]{:S(2)}) async-start(bf16[4,128,256]{2,1,0:T(8,128)(2,1)} %bitcast.25), calls=%async_computation.1 | async-start | bytes 524288 | tf_op jit(solution)/shard_map/all_to_all | solution.py:530
  33.1 0.7 copy-start.7
  33.8 30.6 %copy-start.5 = (bf16[512,128]{1,0:T(8,128)(2,1)S(1)}, bf16[512,128]{1,0:T(8,128)(2,1)}, u32[]{:S(2)}) copy-start(bf16[512,128]{1,0:T(8,128)(2,1)} %get-tuple-element.24.held_in) | copy-start | bytes 393220
  38.6 25.8 %collective-permute-start = (bf16[128,2048]{1,0:T(8,128)(2,1)}, bf16[128,2048]{1,0:T(8,128)(2,1)S(1)}, u32[]{:S(2)}, u32[]{:S(2)}) collective-permute-start(bf16[128,2048]{1,0:T(8,128)(2,1)} %get-tuple-element.21), channel_id=1, source_target_pairs={{0,16},{4,20},{8,24},{12,28},{16,0},{20,4},{24,8},{28,12},{1,17},{... | collective-permute-start | bytes 1572872 | tf_op jit(solution)/shard_map/ppermute | solution.py:547
  96.6 32.8 %all-to-all-start.2 = ((bf16[16,32,2048]{2,1,0:T(8,128)(2,1)}), bf16[16,32,2048]{2,1,0:T(8,128)(2,1)S(1)}, u32[]{:S(2)}, u32[]{:S(2)}) async-start(bf16[16,32,2048]{2,1,0:T(8,128)(2,1)} %bitcast.21), calls=%async_computation.2 | async-start | bytes 4194304 | tf_op jit(solution)/shard_map/all_to_all | solution.py:477
  100.4 1.6 copy-start.2
  110.1 1.3 copy-start.1
  129.4 33.6 %all-to-all-start.5 = ((bf16[16,32,2048]{2,1,0:T(8,128)(2,1)}), bf16[16,32,2048]{2,1,0:T(8,128)(2,1)}, u32[]{:S(2)}, u32[]{:S(2)}) async-start(bf16[16,32,2048]{2,1,0:T(8,128)(2,1)} %copy-done.1), calls=%async_computation.5 | async-start | bytes 4194304 | tf_op jit(solution)/shard_map/all_to_all | solution.py:477
  142.1 1.3 copy-start
  163.0 44.9 %all-to-all-start.3 = ((bf16[16,32,2048]{2,1,0:T(8,128)(2,1)}), bf16[16,32,2048]{2,1,0:T(8,128)(2,1)S(1)}, u32[]{:S(2)}, u32[]{:S(2)}) async-start(bf16[16,32,2048]{2,1,0:T(8,128)(2,1)} %copy-done), calls=%async_computation.3 | async-start | bytes 4194304 | tf_op jit(solution)/shard_map/all_to_all | solution.py:477
  171.1 36.7 %collective-permute-start.1 = (bf16[128,2048]{1,0:T(8,128)(2,1)}, bf16[128,2048]{1,0:T(8,128)(2,1)S(1)}, u32[]{:S(2)}, u32[]{:S(2)}) collective-permute-start(bf16[128,2048]{1,0:T(8,128)(2,1)} %shard_map.179), channel_id=1, source_target_pairs={{0,16},{4,20},{8,24},{12,28},{16,0},{20,4},{24,8},{28,12},{1,17},{... | collective-permute-start | bytes 1572872 | tf_op jit(solution)/shard_map/ppermute | solution.py:556
  171.9 35.9 %copy-start.4 = (bf16[256,512]{1,0:T(8,128)(2,1)S(1)}, bf16[256,512]{1,0:T(8,128)(2,1)}, u32[]{:S(2)}) copy-start(bf16[256,512]{1,0:T(8,128)(2,1)} %get-tuple-element.16.weight_in) | copy-start | bytes 786436
  207.8 1.2 copy-start.3
